TPU v7x, 256 devices: a whole 4x4x8 slice. The times are simulated.
256 devices in a mesh: ep: 32 (over z, x), tp: 8 (over y, core).
Axes of the slice: x: 4, y: 4, z: 8, core: 2. Of those that a mesh axis runs over, the one named last changes fastest.
Arguments:
- queries: bfloat16 [32768, 2048], P('ep', 'tp'), may hold values from -6 to 6
- key_vectors: bfloat16 [32768, 2048], P('ep', 'tp'), may hold values from -6 to 6
- value_vectors: bfloat16 [32768, 4096], P('ep', 'tp'), may hold values from -6 to 6
- decay_logit: float32 [32768, 2048], P('ep', 'tp'), may hold values from -11 to 16
- head_gain: float32 [256], replicated, may hold values from 0.1 to 1.9
- routed_rows: bfloat16 [8192, 4096], P('ep'), may hold values from -6 to 6
- pre_gain: float32 [4096], replicated, may hold values from 0.1 to 1.9
- expert_pick: int32 [8192, 2], P('ep'), may hold values from 0 to 31, as said below
- route_weight: float32 [8192, 2], P('ep'), may hold values from 0.2 to 1
- gate_weight: bfloat16 [32, 4096, 2048], P('ep', None, 'tp'), may hold values from -0.09375 to 0.09375
- up_weight: bfloat16 [32, 4096, 2048], P('ep', None, 'tp'), may hold values from -0.09375 to 0.09375
- down_weight: bfloat16 [32, 2048, 4096], P('ep', 'tp'), may hold values from -0.125 to 0.125
- post_gain: float32 [4096], replicated, may hold values from 0.1 to 1.9
Outputs:
- mixed_heads: bfloat16 [32768, 4096], P('ep', 'tp')
- routed_out: bfloat16 [8192, 4096], P(('ep', 'tp'))
Inputs may be any that keep to these rules, and one draw needn't show every extreme that they name: `expert_pick`: each row names 2 different experts, both in the same one of 4 equal groups of consecutive expert numbers. In every aligned block of 32 rows no expert is named more than 4 times, and some expert exactly 4 times.
All inputs are finite; a program needn't handle non-finite values.
Results may differ from a plain program's by a relative error of at most 0.015.
Values may be sent and summed in bfloat16 or wider, within the bound.
No kernel may reach another device: no remote copies, remote signals or barrier semaphores. Data moves between devices by JAX's collectives and lax.ppermute only.
A program may use at most 128 MiB of HBM per device.

v0:
```python
import functools

import jax
import jax.numpy as jnp
from jax import lax
from jax.experimental import pallas as pl
from jax.experimental.pallas import tpu as pltpu
from jax.sharding import Mesh
from jax.sharding import PartitionSpec as P


DK = 128
DV = 256
BLK = 64
VROWS = 16
CAP = 4
NY = 4
EP = ("z", "x")
F32 = jnp.float32
BF16 = jnp.bfloat16


def ring(size, step):
    return [(i, (i + step) % size) for i in range(size)]


def contract(a, b, dim_a, dim_b):
    return lax.dot_general(
        a, b, (((dim_a,), (dim_b,)), ((), ())), preferred_element_type=F32
    )


def attn_local_kernel(q_ref, k_ref, v_ref, g_ref, o_ref, qc_ref, st_ref, state, decay):
    step = pl.program_id(0)
    heads = state.shape[0]

    @pl.when(step == 0)
    def _():
        state[...] = jnp.zeros_like(state)
        decay[...] = jnp.zeros_like(decay)

    row = lax.broadcasted_iota(jnp.int32, (BLK, BLK), 0)
    col = lax.broadcasted_iota(jnp.int32, (BLK, BLK), 1)
    causal = row >= col
    before = decay[0:1, :]
    old = [state[h] for h in range(heads)]
    for b in range(q_ref.shape[0] // BLK):
        rows = slice(b * BLK, (b + 1) * BLK)
        logit = g_ref[rows, :]
        rate = (jnp.minimum(logit, 0.0) - jnp.log1p(jnp.exp(-jnp.abs(logit)))) * (1.0 / 16.0)
        cumulative = jnp.dot(
            causal.astype(F32), rate, precision=lax.Precision.HIGHEST, preferred_element_type=F32
        )
        ending = cumulative[BLK - 1 : BLK, :]
        q = q_ref[rows, :].astype(F32)
        k = k_ref[rows, :].astype(F32)
        query_decay = (q * jnp.exp(cumulative)).astype(BF16)
        key_decay = (k * jnp.exp(-cumulative)).astype(BF16)
        key_to_end = (k * jnp.exp(ending - cumulative)).astype(BF16)
        qc_ref[rows, :] = (q * jnp.exp(cumulative + before)).astype(BF16)
        before = before + ending
        step_decay = jnp.exp(ending)
        for h in range(heads):
            ks = slice(h * DK, (h + 1) * DK)
            vs = slice(h * DV, (h + 1) * DV)
            v = v_ref[rows, vs]
            scores = contract(query_decay[:, ks], key_decay[:, ks], 1, 1)
            weights = jnp.where(causal, scores, 0.0).astype(BF16)
            inside = contract(weights, v, 1, 0)
            o_ref[rows, vs] = inside + contract(query_decay[:, ks], old[h].astype(BF16), 1, 1)
            old[h] = old[h] * step_decay[:, ks] + contract(v, key_to_end[:, ks], 0, 0)
    decay[...] = jnp.broadcast_to(before, decay.shape)
    for h in range(heads):
        state[h] = old[h]

    @pl.when(step == pl.num_programs(0) - 1)
    def _():
        for h in range(heads):
            total = jnp.exp(decay[0:1, h * DK : (h + 1) * DK])
            chunks = DV // VROWS
            own = slice(h * chunks, (h + 1) * chunks)
            st_ref[own, 0:VROWS, :] = state[h].astype(BF16).reshape(chunks, VROWS, DK)
            st_ref[own, VROWS:, :] = jnp.broadcast_to(total, (chunks, 8, DK)).astype(BF16)


def attn_local(q, k, v, g):
    rows, keys = q.shape
    values = v.shape[1]
    heads = keys // DK
    tile = 4 * BLK
    return pl.pallas_call(
        attn_local_kernel,
        grid=(rows // tile,),
        in_specs=[
            pl.BlockSpec((tile, keys), lambda n: (n, 0)),
            pl.BlockSpec((tile, keys), lambda n: (n, 0)),
            pl.BlockSpec((tile, values), lambda n: (n, 0)),
            pl.BlockSpec((tile, keys), lambda n: (n, 0)),
        ],
        out_specs=[
            pl.BlockSpec((tile, values), lambda n: (n, 0)),
            pl.BlockSpec((tile, keys), lambda n: (n, 0)),
            pl.BlockSpec((heads * DV // VROWS, VROWS + 8, DK), lambda n: (0, 0, 0)),
        ],
        out_shape=[
            jax.ShapeDtypeStruct((rows, values), F32),
            jax.ShapeDtypeStruct((rows, keys), BF16),
            jax.ShapeDtypeStruct((heads * DV // VROWS, VROWS + 8, DK), BF16),
        ],
        scratch_shapes=[
            pltpu.VMEM((heads, DV, DK), F32),
            pltpu.VMEM((8, keys), F32),
        ],
        compiler_params=pltpu.CompilerParams(dimension_semantics=("arbitrary",)),
        cost_estimate=pl.CostEstimate(
            flops=8 * 10**9, transcendentals=10**6, bytes_accessed=6 * 10**6
        ),
        name="attn_local",
    )(q, k, v, g)


def attn_out_kernel(o_ref, qc_ref, in_ref, gain_ref, out_ref):
    gain = gain_ref[...]
    for h in range(in_ref.shape[0] // DV):
        vs = slice(h * DV, (h + 1) * DV)
        carried = contract(qc_ref[:, h * DK : (h + 1) * DK], in_ref[h * DV : (h + 1) * DV, :], 1, 1)
        total = o_ref[:, vs] + carried
        mean = jnp.mean(total * total, axis=-1, keepdims=True)
        out_ref[:, vs] = (total * lax.rsqrt(mean + 1e-06) * gain).astype(BF16)


def attn_out(o, qc, returned, gain, column):
    rows, values = o.shape
    tile = 256
    return pl.pallas_call(
        attn_out_kernel,
        grid=(rows // tile,),
        in_specs=[
            pl.BlockSpec((tile, values), lambda n: (n, 0)),
            pl.BlockSpec((tile, qc.shape[1]), lambda n: (n, 0)),
            pl.BlockSpec((returned.shape[0], DK), lambda n: (0, column)),
            pl.BlockSpec((1, DV), lambda n: (0, 0)),
        ],
        out_specs=pl.BlockSpec((tile, values), lambda n: (n, 0)),
        out_shape=jax.ShapeDtypeStruct((rows, values), BF16),
        compiler_params=pltpu.CompilerParams(dimension_semantics=("arbitrary",)),
        cost_estimate=pl.CostEstimate(
            flops=3 * 10**9, transcendentals=2048, bytes_accessed=4 * 10**6
        ),
        name="attn_out",
    )(o, qc, returned, gain.reshape(1, DV))


def prefix_kernel(in_ref, out_ref):
    carry = jnp.zeros((VROWS, DK), F32)
    for s in range(in_ref.shape[0]):
        out_ref[s] = carry.astype(BF16)
        decay = in_ref[s, VROWS:, :].astype(F32)[0:1, :]
        carry = carry * decay + in_ref[s, 0:VROWS, :].astype(F32)


def exchange(x):
    return lax.all_to_all(x, EP, split_axis=0, concat_axis=0, tiled=True)


def prefix(arrived):
    return pl.pallas_call(
        prefix_kernel,
        out_shape=jax.ShapeDtypeStruct((arrived.shape[0], VROWS, DK), BF16),
        name="prefix",
    )(arrived)


def own_columns(slots, first_rows, part):
    rows = slots.shape[1]
    wide = jnp.concatenate([slots] * 4, axis=0).astype(F32).astype(BF16)
    count = part * len(first_rows)
    row = lax.broadcasted_iota(jnp.int32, (rows, count), 0)
    col = lax.broadcasted_iota(jnp.int32, (rows, count), 1)
    source = col % part
    for i, first in enumerate(first_rows):
        source += jnp.where(col // part == i, first, 0)
    pick = jnp.where(row == source, 1.0, 0.0).astype(BF16)
    return contract(wide, pick, 1, 0)[0:2].astype(jnp.int32)


def dispatch_kernel(idx_ref, rows_ref, gain_ref, pick_ref, out_ref, slot_ref, *, part, experts):
    total = pick_ref.shape[1]
    pick = pick_ref[...]
    first = pick[0:1]
    second = pick[1:2]
    expert = lax.broadcasted_iota(jnp.int32, (experts, total), 0)
    hit0 = first == expert
    hit1 = second == expert
    named = jnp.where(hit0 | hit1, 1.0, 0.0).astype(BF16)
    row = lax.broadcasted_iota(jnp.int32, (total, total), 0)
    col = lax.broadcasted_iota(jnp.int32, (total, total), 1)
    earlier = (row < col) & (col // part == row // part)
    before = contract(named, jnp.where(earlier, 1.0, 0.0).astype(BF16), 1, 0)
    rank0 = jnp.sum(jnp.where(hit0, before, 0.0), axis=0, keepdims=True)
    rank1 = jnp.sum(jnp.where(hit1, before, 0.0), axis=0, keepdims=True)
    slots = pick * CAP + jnp.concatenate([rank0, rank1], axis=0).astype(jnp.int32)
    slot_ref[...] = slots
    values = rows_ref[...].astype(F32)
    mean = jnp.mean(values * values, axis=-1, keepdims=True)
    normed = (values * lax.rsqrt(mean + 1e-06) * gain_ref[...]).astype(BF16)
    own = own_columns(slots, [idx_ref[0] * part], part)
    place = lax.broadcasted_iota(jnp.int32, (out_ref.shape[0], part), 0)
    target = (place // (2 * CAP)) * CAP + place % CAP
    chosen = (own[0:1] == target) | (own[1:2] == target)
    half = out_ref.shape[1]
    total_out = None
    for h in range(2):
        mine = chosen & (place // CAP % 2 == h)
        piece = contract(
            jnp.where(mine, 1.0, 0.0).astype(BF16), normed[:, h * half : (h + 1) * half], 1, 0
        )
        total_out = piece if total_out is None else total_out + piece
    out_ref[...] = total_out.astype(BF16)


def dispatch(index, rows, gain, pick, part, experts):
    total, width = rows.shape
    return pl.pallas_call(
        functools.partial(dispatch_kernel, part=part, experts=experts),
        grid_spec=pltpu.PrefetchScalarGridSpec(
            num_scalar_prefetch=1,
            grid=(1,),
            in_specs=[
                pl.BlockSpec((part, width), lambda n, idx: (idx[0], 0)),
                pl.BlockSpec((1, width), lambda n, idx: (0, 0)),
                pl.BlockSpec((2, total), lambda n, idx: (0, 0)),
            ],
            out_specs=[
                pl.BlockSpec((experts * CAP * 2, width // 2), lambda n, idx: (0, 0)),
                pl.BlockSpec((2, total), lambda n, idx: (0, 0)),
            ],
        ),
        out_shape=[
            jax.ShapeDtypeStruct((experts * CAP * 2, width // 2), BF16),
            jax.ShapeDtypeStruct((2, total), jnp.int32),
        ],
        name="dispatch",
    )(index, rows, gain.reshape(1, width), pick.T)


def hidden_kernel(*refs, parts):
    xs = refs[:parts]
    weights = refs[parts : parts + 8]
    out_ref = refs[parts + 8]
    acc = refs[parts + 9]
    step = pl.program_id(0)
    rows = xs[0].shape[0]
    new = lax.broadcasted_iota(jnp.int32, (rows // 2, rows), 0)
    old = lax.broadcasted_iota(jnp.int32, (rows // 2, rows), 1)
    spread = (new // CAP) * (2 * CAP) + new % CAP
    x = []
    for h in range(2):
        order = jnp.where(old == spread + h * CAP, 1.0, 0.0).astype(BF16)
        x.append(
            jnp.concatenate([contract(order, r[...], 1, 0).astype(BF16) for r in xs], axis=0)
        )

    @pl.when(step == 0)
    def _():
        acc[...] = jnp.zeros_like(acc)

    width = weights[0].shape[1]
    for j in range(4):
        acc[:, j * width : (j + 1) * width] += contract(x[0], weights[2 * j][...], 1, 0) + contract(
            x[1], weights[2 * j + 1][...], 1, 0
        )

    @pl.when(step == pl.num_programs(0) - 1)
    def _():
        for j in range(2):
            gate = acc[:, 2 * j * width : (2 * j + 1) * width]
            up = acc[:, (2 * j + 1) * width : (2 * j + 2) * width]
            value = gate / (1.0 + jnp.exp(-gate)) * up
            out_ref[:, j * width : (j + 1) * width] = value.astype(BF16)


def hidden_units(xs, weights, ktile=512):
    rows = sum(x.shape[0] for x in xs) // 2
    depth, width = weights[0].shape
    steps = depth // 2 // ktile
    specs, doubled = [], []
    for w in weights:
        doubled += [w, w]
        specs += [
            pl.BlockSpec((ktile, width), lambda n: (n, 0)),
            pl.BlockSpec((ktile, width), lambda n: (n + steps, 0)),
        ]
    return pl.pallas_call(
        functools.partial(hidden_kernel, parts=len(xs)),
        grid=(steps,),
        in_specs=[pl.BlockSpec((x.shape[0], ktile), lambda n: (0, n)) for x in xs] + specs,
        out_specs=pl.BlockSpec((rows, 2 * width), lambda n: (0, 0)),
        out_shape=jax.ShapeDtypeStruct((rows, 2 * width), BF16),
        scratch_shapes=[pltpu.VMEM((rows, 4 * width), F32)],
        compiler_params=pltpu.CompilerParams(dimension_semantics=("arbitrary",)),
        cost_estimate=pl.CostEstimate(
            flops=8 * rows * depth * width,
            transcendentals=2 * rows * width,
            bytes_accessed=8 * depth * width + 2 * rows * depth,
        ),
        name="hidden_units",
    )(*xs, *doubled)


def in_blocks(near, far, shift):
    ordered = (near[0], near[1], far[...], near[2])
    return jnp.concatenate([ordered[(i - shift) % NY] for i in range(NY)], axis=0)


def down_sides_kernel(n0, f0, n1, f1, n3, f3, *rest):
    weights = rest[:6]
    out_ref = rest[6]
    width = weights[0].shape[0]
    total = None
    for m, act in enumerate((in_blocks(n0, f0, 0), in_blocks(n1, f1, 1), in_blocks(n3, f3, 3))):
        for c in range(2):
            term = contract(act[:, c * width : (c + 1) * width], weights[2 * m + c][...], 1, 0)
            total = term if total is None else total + term
    out_ref[...] = total


def down_far_kernel(n2, f2, *rest):
    weights = rest[:4]
    partial_ref, state_ref, out_ref = rest[4:7]
    width, depth = weights[0].shape
    group = f2.shape[0]
    rows = NY * group
    total = partial_ref[...]
    act = in_blocks(n2, f2, 2)
    for c in range(4):
        total += contract(act[:, c * width : (c + 1) * width], weights[c][...], 1, 0)
    new = lax.broadcasted_iota(jnp.int32, (rows, rows), 0)
    old = lax.broadcasted_iota(jnp.int32, (rows, rows), 1)
    want = (new // CAP % NY) * group + (new // (CAP * NY)) * CAP + new % CAP
    order = jnp.where(old == want, 1.0, 0.0).astype(BF16)
    out_ref[:, 0:depth] = contract(order, total.astype(BF16), 1, 0).astype(BF16)
    out_ref[:, depth:] = state_ref[...]


def expert_down(body, hs, weights, extra, columns, dtype, tiles=2):
    rows, units = hs[1].shape
    group = rows // tiles
    out_rows = NY * rows

    def spec(h):
        if h.ndim == 2:
            return pl.BlockSpec((group, units), lambda n: (n, 0))
        return pl.BlockSpec((h.shape[0], group, units), lambda n: (0, n, 0))

    return pl.pallas_call(
        body,
        grid=(tiles,),
        in_specs=[spec(h) for h in hs]
        + [pl.BlockSpec(w.shape, lambda n: (0, 0)) for w in weights]
        + [pl.BlockSpec((out_rows // tiles, x.shape[1]), lambda n: (n, 0)) for x in extra],
        out_specs=pl.BlockSpec((out_rows // tiles, columns), lambda n: (n, 0)),
        out_shape=jax.ShapeDtypeStruct((out_rows, columns), dtype),
        compiler_params=pltpu.CompilerParams(dimension_semantics=("arbitrary",)),
        cost_estimate=pl.CostEstimate(
            flops=2 * out_rows * columns * sum(w.shape[0] for w in weights),
            transcendentals=0,
            bytes_accessed=8 * 10**6,
        ),
    )(*hs, *weights, *extra)


def combine_kernel(idx_ref, back_ref, slot_ref, weight_ref, o0, o1, o2, o3, *, part):
    y = idx_ref[0] // 2
    core = idx_ref[0] % 2
    firsts = [(((y + i) % NY) * 2 + core) * part for i in range(NY)]
    own = own_columns(slot_ref[...], firsts, part)
    block = lax.broadcasted_iota(jnp.int32, own.shape, 1) // part
    spot = (own // CAP) * (CAP * NY) + block * CAP + own % CAP
    place = lax.broadcasted_iota(jnp.int32, (back_ref.shape[0], NY * part), 0)
    weight = jnp.concatenate(
        [weight_ref[pl.ds(pl.multiple_of(first, part), part), :] for first in firsts], axis=0
    )
    back = back_ref[...]
    mixed = None
    for j in range(2):
        chosen = jnp.where(place == spot[j : j + 1], 1.0, 0.0).astype(BF16)
        term = contract(chosen, back, 0, 0) * weight[:, j : j + 1]
        mixed = term if mixed is None else mixed + term
    for i, out in enumerate((o0, o1, o2, o3)):
        out[...] = mixed[i * part : (i + 1) * part].astype(out.dtype)


def combine(index, back, slots, weight, part, width):
    total = weight.shape[0]
    return pl.pallas_call(
        functools.partial(combine_kernel, part=part),
        grid_spec=pltpu.PrefetchScalarGridSpec(
            num_scalar_prefetch=1,
            grid=(1,),
            in_specs=[
                pl.BlockSpec((back.shape[0], width), lambda n, idx: (0, 0)),
                pl.BlockSpec((2, total), lambda n, idx: (0, 0)),
                pl.BlockSpec((total, 2), lambda n, idx: (0, 0)),
            ],
            out_specs=[pl.BlockSpec((part, width), lambda n, idx: (0, 0)) for _ in range(NY)],
        ),
        out_shape=[jax.ShapeDtypeStruct((part, width), BF16) for _ in range(NY)],
        name="combine",
    )(index, back, slots, weight)


def finish_kernel(idx_ref, p0, p1, p2, p3, gain_ref, out_ref):
    y = idx_ref[0] // 2
    width = p0.shape[1]
    pieces = [p[...].astype(F32) for p in (p0, p1, p2, p3)]
    square = sum(jnp.sum(p * p, axis=-1, keepdims=True) for p in pieces)
    scale = lax.rsqrt(square / (width * NY) + 1e-06)
    for i, piece in enumerate(pieces):
        columns = pl.ds(pl.multiple_of(((y + i) % NY) * width, width), width)
        out_ref[:, columns] = (piece * scale * gain_ref[:, columns]).astype(BF16)


def finish(index, pieces, gain):
    part, width = pieces[0].shape
    full = width * NY
    return pl.pallas_call(
        finish_kernel,
        grid_spec=pltpu.PrefetchScalarGridSpec(
            num_scalar_prefetch=1,
            grid=(1,),
            in_specs=[pl.BlockSpec((part, width), lambda n, idx: (0, 0)) for _ in pieces]
            + [pl.BlockSpec((1, full), lambda n, idx: (0, 0))],
            out_specs=pl.BlockSpec((part, full), lambda n, idx: (0, 0)),
        ),
        out_shape=jax.ShapeDtypeStruct((part, full), BF16),
        name="finish",
    )(index, *pieces, gain.reshape(1, full))


def from_right(x):
    return lax.ppermute(x, "y", ring(NY, -1))


def from_left(x):
    return lax.ppermute(x, "y", ring(NY, 1))


def on_device(
    queries,
    key_vectors,
    value_vectors,
    decay_logit,
    head_gain,
    routed_rows,
    pre_gain,
    expert_pick,
    route_weight,
    gate_weight,
    up_weight,
    down_weight,
    post_gain,
):
    y = lax.axis_index("y")
    core = lax.axis_index("c")
    experts = lax.axis_size(EP)
    part = routed_rows.shape[0] // (NY * 2)
    width = routed_rows.shape[1]
    index = (y * 2 + core).astype(jnp.int32).reshape(1)
    swap = [(0, 1), (1, 0)]

    outgoing, slots = dispatch(index, routed_rows, pre_gain, expert_pick, part, experts)
    arrived = exchange(outgoing.reshape(experts, 2 * CAP, width // 2))

    gate, up, down = gate_weight[0], up_weight[0], down_weight[0]
    weights = (gate, up, lax.ppermute(gate, "c", swap), lax.ppermute(up, "c", swap))
    cut = width // NY
    slices = [
        lax.dynamic_slice_in_dim(down, lax.rem(y + i, NY) * cut, cut, axis=1) for i in range(NY)
    ]
    middle = down.shape[0] // 2
    mine = [
        slices[0],
        from_right(slices[3]),
        from_left(slices[1]),
        from_left(slices[2][:middle]),
        from_right(slices[2][middle:]),
    ]
    local_out, query_carry, local_state = attn_local(
        queries, key_vectors, value_vectors, decay_logit
    )
    mine, _ = lax.optimization_barrier((mine, local_state))
    mine[3], mine[4] = from_left(mine[3]), from_right(mine[4])
    arrived, local_state = lax.optimization_barrier((arrived, local_state))
    d0, d1, d3, d2a, d2b = [(piece, lax.ppermute(piece, "c", swap)) for piece in mine]

    half = experts // 2
    top = arrived[:half].reshape(-1, width // 2)
    bottom = arrived[half:].reshape(-1, width // 2)
    right_top, right_bottom = from_right(top), from_right(bottom)
    left_top, left_bottom = from_left(top), from_left(bottom)
    far_top, far_bottom = from_left(left_top), from_right(right_bottom)

    chunk_states = exchange(local_state)
    before = prefix(chunk_states)
    sides, before = lax.optimization_barrier(
        ((right_top, right_bottom, left_top, left_bottom), before)
    )
    near = hidden_units([top, bottom, *sides], weights).reshape(3, -1, 2 * gate.shape[1])
    far = hidden_units([far_top, far_bottom], weights)
    near_left, near_right = from_left(near), from_right(near)
    far_left, far_right = from_left(far), from_right(far)
    near_passed, far = lax.optimization_barrier((near_left, far))
    near_far, far_far = from_left(near_passed), from_right(far_right)
    partial = expert_down(
        down_sides_kernel,
        (near, far, near_right, far_right, near_left, far_left),
        (*d0, *d1, *d3),
        (),
        cut,
        F32,
    )
    back = expert_down(
        down_far_kernel,
        (near_far, far_far),
        (d2a[0], d2b[0], d2a[1], d2b[1]),
        (partial, before.reshape(-1, DK)),
        cut + DK,
        BF16,
    )
    returned = exchange(back.reshape(experts, NY * CAP, cut + DK)).reshape(-1, cut + DK)

    pieces = combine(index, returned, slots, route_weight, part, cut)
    gathered = [pieces[0]] + [
        lax.ppermute(pieces[-m % NY], "y", ring(NY, -m)) for m in range(1, NY)
    ]
    routed_out = finish(index, gathered, post_gain)
    mixed_heads = attn_out(local_out, query_carry, returned, head_gain, cut // DK)
    return (mixed_heads, routed_out)


def solution(mesh):
    ep, tp = mesh.shape["ep"], mesh.shape["tp"]
    torus = Mesh(mesh.devices.reshape(ep // 4, 4, NY, tp // NY), ("z", "x", "y", "c"))
    tpa = ("y", "c")
    placed = (
        P(EP, tpa),
        P(EP, tpa),
        P(EP, tpa),
        P(EP, tpa),
        P(),
        P(EP, None),
        P(),
        P(EP, None),
        P(EP, None),
        P(EP, None, tpa),
        P(EP, None, tpa),
        P(EP, tpa, None),
        P(),
    )
    return jax.shard_map(
        on_device,
        mesh=torus,
        in_specs=placed,
        out_specs=(P(EP, tpa), P(("z", "x", "y", "c"), None)),
        check_vma=False,
    )
```

profile of v0, /device:TPU:2, one launch (start us, length us, event | category | flops | bytes accessed | tf_op | source)
XLA Modules:
  0.0 209.0 jit_solution(4321125885896368799)
XLA Ops:
  0.6 0.0 copy-start
  0.6 3.1 %dispatch.1 = (bf16[256,2048]{1,0:T(8,128)(2,1)}, s32[2,256]{1,0:T(2,128)}) custom-call(s32[1]{0:T(128)} %bitcast.idx_ref, bf16[256,4096]{1,0:T(8,128)(2,1)} %rows_ref.1, f32[1,4096]{1,0:T(1,128)} %bitcast.44, s32[2,256]{1,0:T(2,128)} %bitcast.46), custom_call_target="tpu_custom_call" | custom-call | tf_op jit(solution)/shard_map/dispatch/pallas_call | solution.py:224
  3.7 11.6 %all-to-all-start = ((bf16[32,8,2048]{2,1,0:T(8,128)(2,1)}), bf16[32,8,2048]{2,1,0:T(8,128)(2,1)S(1)}, u32[]{:S(2)}, u32[]{:S(2)}) async-start(bf16[32,8,2048]{2,1,0:T(8,128)(2,1)} %bitcast.42), calls=%async_computation | async-start | bytes 2097152 | tf_op jit(solution)/shard_map/all_to_all | solution.py:163
  15.4 0.1 collective-permute-start.4
  15.5 0.5 collective-permute-start.5
  16.0 9.5 %attn_local.1 = (f32[1024,512]{1,0:T(8,128)}, bf16[1024,256]{1,0:T(8,128)(2,1)}, bf16[32,24,128]{2,1,0:T(8,128)(2,1)}) custom-call(bf16[1024,256]{1,0:T(8,128)(2,1)} %q_ref.1, bf16[1024,256]{1,0:T(8,128)(2,1)} %k_ref.1, bf16[1024,512]{1,0:T(8,128)(2,1)} %v_ref.1, f32[1024,256]{1,0:T(8,128)} %g_ref.1), custom_call_target="tpu_custom_call" | custom-call | flops 8000000000 | bytes 6000000 | tf_op jit(solution)/shard_map/attn_local/pallas_call | solution.py:91
  25.5 17.9 %all-to-all-done = bf16[32,8,2048]{2,1,0:T(8,128)(2,1)S(1)} async-done(((bf16[32,8,2048]{2,1,0:T(8,128)(2,1)}), bf16[32,8,2048]{2,1,0:T(8,128)(2,1)S(1)}, u32[]{:S(2)}, u32[]{:S(2)}) %all-to-all-start) | async-done | bytes 1048608 | tf_op jit(solution)/shard_map/all_to_all | solution.py:163
  43.4 1.1 slice_bitcast_fusion
  44.5 3.0 %collective-permute-start.1 = (bf16[128,2048]{1,0:T(8,128)(2,1)}, bf16[128,2048]{1,0:T(8,128)(2,1)S(1)}, u32[]{:S(2)}, u32[]{:S(2)}) collective-permute-start(bf16[128,2048]{1,0:T(8,128)(2,1)} %get-tuple-element.53.refs_1_), channel_id=1, source_target_pairs={{0,6},{2,0},{4,2},{6,4},{1,7},{3,1},{5,3},{7,5},{8,14},{10,8},{12,... | collective-permute-start | bytes 1572872 | tf_op jit(solution)/shard_map/ppermute | solution.py:442
  47.5 0.0 collective-permute-start.2
  47.5 3.2 %collective-permute-start = (bf16[128,2048]{1,0:T(8,128)(2,1)}, bf16[128,2048]{1,0:T(8,128)(2,1)}, u32[]{:S(2)}, u32[]{:S(2)}) collective-permute-start(bf16[128,2048]{1,0:T(8,128)(2,1)} %get-tuple-element.54.refs_0_), channel_id=1, source_target_pairs={{0,6},{2,0},{4,2},{6,4},{1,7},{3,1},{5,3},{7,5},{8,14},{10,8},{12,... | collective-permute-start | bytes 1572872 | tf_op jit(solution)/shard_map/ppermute | solution.py:442
  50.8 9.4 %collective-permute-done.1.refs_3_ = bf16[128,2048]{1,0:T(8,128)(2,1)S(1)} collective-permute-done((bf16[128,2048]{1,0:T(8,128)(2,1)}, bf16[128,2048]{1,0:T(8,128)(2,1)S(1)}, u32[]{:S(2)}, u32[]{:S(2)}) %collective-permute-start.1) | collective-permute-done | bytes 524320 | tf_op jit(solution)/shard_map/ppermute | solution.py:442
  60.2 0.9 collective-permute-start.3
  61.1 5.6 %all-to-all-start.1 = ((bf16[32,24,128]{2,1,0:T(8,128)(2,1)}), bf16[32,24,128]{2,1,0:T(8,128)(2,1)S(1)}, u32[]{:S(2)}, u32[]{:S(2)}) async-start(bf16[32,24,128]{2,1,0:T(8,128)(2,1)} %get-tuple-element.30), calls=%async_computation.1 | async-start | bytes 393216 | tf_op jit(solution)/shard_map/all_to_all | solution.py:163
  66.7 2.5 %dynamic-slice_bitcast_fusion = (bf16[256,1024]{1,0:T(8,128)(2,1)}, bf16[256,1024]{1,0:T(8,128)(2,1)}, bf16[256,1024]{1,0:T(8,128)(2,1)S(1)}) fusion(bf16[1,256,4096]{2,1,0:T(8,128)(2,1)} %param.24, s32[]{:T(128)S(6)} %select_n.14, s32[]{:T(128)S(6)} %select_n.13, s32[]{:T(128)S(6)} %select_n.12), kind=kLoop, calls=%fused_computation | loop fusion | bytes 3145740 | tf_op jit(solution)/shard_map/dynamic_slice | solution.py:479
  69.2 2.7 %collective-permute-start.12 = (bf16[256,1024]{1,0:T(8,128)(2,1)}, bf16[256,1024]{1,0:T(8,128)(2,1)}, u32[]{:S(2)}, u32[]{:S(2)}) collective-permute-start(bf16[256,1024]{1,0:T(8,128)(2,1)} %get-tuple-element.51), channel_id=1, source_target_pairs={{0,6},{2,0},{4,2},{6,4},{1,7},{3,1},{5,3},{7,5},{8,14},{10,8},{12,... | collective-permute-start | bytes 1572872 | tf_op jit(solution)/shard_map/ppermute | solution.py:442
  71.8 0.0 collective-permute-done.refs_2_
  71.8 1.9 dynamic-slice_bitcast_fusion.3
  73.7 2.1 %all-to-all-done.1.in_ref = bf16[32,24,128]{2,1,0:T(8,128)(2,1)S(1)} async-done(((bf16[32,24,128]{2,1,0:T(8,128)(2,1)}), bf16[32,24,128]{2,1,0:T(8,128)(2,1)S(1)}, u32[]{:S(2)}, u32[]{:S(2)}) %all-to-all-start.1) | async-done | bytes 196640 | tf_op jit(solution)/shard_map/all_to_all | solution.py:163
  75.8 0.7 copy-done.3
  76.5 1.6 prefix.1
  78.1 1.6 collective-permute-start.14
  79.7 1.7 collective-permute-start.15
  81.4 8.9 %hidden_units.2 = bf16[384,512]{1,0:T(8,128)(2,1)} custom-call(bf16[128,2048]{1,0:T(8,128)(2,1)} %get-tuple-element.54.refs_0_, bf16[128,2048]{1,0:T(8,128)(2,1)} %get-tuple-element.53.refs_1_, bf16[128,2048]{1,0:T(8,128)(2,1)} %collective-permute-done.refs_2_, bf16[128,2048]{1,0:T(8,128)(2,1)} %copy-done.4, ...), custom_call_target="tpu_custom_call" | custom-call | flops 3221225472 | bytes 11534336 | tf_op jit(solution)/shard_map/hidden_units/pallas_call | solution.py:294
  90.3 1.1 collective-permute-start.6
  91.4 2.0 collective-permute-start.7
  93.4 1.4 collective-permute-start.8
  94.8 0.7 collective-permute-start.16
  95.5 18.5 %collective-permute-done.16.rest_0_ = bf16[128,1024]{1,0:T(8,128)(2,1)} collective-permute-done((bf16[128,1024]{1,0:T(8,128)(2,1)S(1)}, bf16[128,1024]{1,0:T(8,128)(2,1)}, u32[]{:S(2)}, u32[]{:S(2)}) %collective-permute-start.16) | collective-permute-done | bytes 262176 | tf_op jit(solution)/shard_map/ppermute | solution.py:446
  114.0 0.5 collective-permute-start.24
  114.5 1.4 collective-permute-start.20
  115.9 0.7 collective-permute-start.17
  116.6 0.0 copy-done.7
  116.7 6.2 %hidden_units.3.f0 = bf16[128,512]{1,0:T(8,128)(2,1)} custom-call(bf16[128,2048]{1,0:T(8,128)(2,1)} %copy-done.6, bf16[128,2048]{1,0:T(8,128)(2,1)} %copy-done.7, bf16[4096,256]{1,0:T(8,128)(2,1)} %bitcast.28, bf16[4096,256]{1,0:T(8,128)(2,1)} %bitcast.29, bf16[4096,256]{1,0:T(8,128)(2,1)} %bitcast.34, bf16[4096,256]{1,0:T(8,128)(2,1)} %bitcast.35, ...), custom_call_target="tpu_custom_call" | custom-call | flops 1073741824 | bytes 9437184 | tf_op jit(solution)/shard_map/hidden_units/pallas_call | solution.py:294
  122.9 8.6 %collective-permute-done.17.rest_1_ = bf16[128,1024]{1,0:T(8,128)(2,1)} collective-permute-done((bf16[128,1024]{1,0:T(8,128)(2,1)}, bf16[128,1024]{1,0:T(8,128)(2,1)}, u32[]{:S(2)}, u32[]{:S(2)}) %collective-permute-start.17) | collective-permute-done | bytes 262176 | tf_op jit(solution)/shard_map/ppermute | solution.py:442
  131.6 0.0 copy-start.8
  131.6 3.2 %collective-permute-start.10 = (bf16[128,512]{1,0:T(8,128)(2,1)}, bf16[128,512]{1,0:T(8,128)(2,1)S(1)}, u32[]{:S(2)}, u32[]{:S(2)}) collective-permute-start(bf16[128,512]{1,0:T(8,128)(2,1)} %hidden_units.3.f0), channel_id=1, source_target_pairs={{0,6},{2,0},{4,2},{6,4},{1,7},{3,1},{5,3},{7,5},{8,14},{10,8},{12,... | collective-permute-start | bytes 393224 | tf_op jit(solution)/shard_map/ppermute | solution.py:442
  134.8 0.1 collective-permute-start.18
  134.9 0.5 collective-permute-start.19
  135.4 2.2 %collective-permute-done.10.f1 = bf16[128,512]{1,0:T(8,128)(2,1)S(1)} collective-permute-done((bf16[128,512]{1,0:T(8,128)(2,1)}, bf16[128,512]{1,0:T(8,128)(2,1)S(1)}, u32[]{:S(2)}, u32[]{:S(2)}) %collective-permute-start.10) | collective-permute-done | bytes 131104 | tf_op jit(solution)/shard_map/ppermute | solution.py:442
  137.6 3.6 %collective-permute-start.11 = (bf16[128,512]{1,0:T(8,128)(2,1)S(1)}, bf16[128,512]{1,0:T(8,128)(2,1)S(1)}, u32[]{:S(2)}, u32[]{:S(2)}) collective-permute-start(bf16[128,512]{1,0:T(8,128)(2,1)S(1)} %collective-permute-done.10.f1), channel_id=1, source_target_pairs={{0,6},{2,0},{4,2},{6,4},{1,7},{3,1},{5,3},{7,5},{8,14},{10,8},{12,... | collective-permute-start | bytes 393224 | tf_op jit(solution)/shard_map/ppermute | solution.py:442
  141.2 4.6 %collective-permute-done.21.f3 = bf16[128,512]{1,0:T(8,128)(2,1)S(1)} collective-permute-done((bf16[128,512]{1,0:T(8,128)(2,1)}, bf16[128,512]{1,0:T(8,128)(2,1)S(1)}, u32[]{:S(2)}, u32[]{:S(2)}) %collective-permute-start.21) | collective-permute-done | bytes 131104 | tf_op jit(solution)/shard_map/ppermute | solution.py:446
  145.8 0.6 copy-done.16
  146.5 5.2 %shard_map.140.rest_4_ = f32[512,1024]{1,0:T(8,128)} custom-call(bf16[3,128,512]{2,1,0:T(8,128)(2,1)} %bitcast.41, bf16[128,512]{1,0:T(8,128)(2,1)} %hidden_units.3.f0, bf16[3,128,512]{2,1,0:T(8,128)(2,1)} %collective-permute-done.20.n1, bf16[128,512]{1,0:T(8,128)(2,1)} %copy-done.15, bf16[3,128,512]{2,1,0:T(8,128)(2,1)} %copy-done.11, ...), custom_call_target="tpu_custom_call" | custom-call | flops 1610612736 | bytes 8000000 | tf_op jit(solution)/shard_map/pallas_call | solution.py:356
  151.7 0.0 copy-start.12
  151.7 0.0 copy-start.10
  151.7 0.6 copy-done.12
  152.4 0.1 copy-done.13
  152.4 0.0 copy-done.14
  152.5 0.1 copy-done.10
  152.6 4.3 %shard_map.141 = bf16[512,1152]{1,0:T(8,128)(2,1)} custom-call(bf16[3,128,512]{2,1,0:T(8,128)(2,1)} %copy-done.10, bf16[128,512]{1,0:T(8,128)(2,1)} %copy-done.14, bf16[128,1024]{1,0:T(8,128)(2,1)} %collective-permute-done.16.rest_0_, bf16[128,1024]{1,0:T(8,128)(2,1)} %collective-permute-done.17.rest_1_, bf16[128,1024]{1,0:T(8,128)(2,1)} %copy-done.12, ...), custom_call_target="tpu_custom_call" | custom-call | flops 603979776 | bytes 8000000 | tf_op jit(solution)/shard_map/pallas_call | solution.py:356
  156.9 9.4 %all-to-all-start.2 = ((bf16[32,16,1152]{2,1,0:T(8,128)(2,1)}), bf16[32,16,1152]{2,1,0:T(8,128)(2,1)S(1)}, u32[]{:S(2)}, u32[]{:S(2)}) async-start(bf16[32,16,1152]{2,1,0:T(8,128)(2,1)} %bitcast.36), calls=%async_computation.2 | async-start | bytes 2359296 | tf_op jit(solution)/shard_map/all_to_all | solution.py:163
  166.3 0.8 copy.15.weight_ref
  167.1 28.6 %all-to-all-done.2 = bf16[32,16,1152]{2,1,0:T(8,128)(2,1)S(1)} async-done(((bf16[32,16,1152]{2,1,0:T(8,128)(2,1)}), bf16[32,16,1152]{2,1,0:T(8,128)(2,1)S(1)}, u32[]{:S(2)}, u32[]{:S(2)}) %all-to-all-start.2) | async-done | bytes 1179680 | tf_op jit(solution)/shard_map/all_to_all | solution.py:163
  195.8 1.0 copy-done.1
  196.8 2.5 %combine.1 = (bf16[32,1024]{1,0:T(8,128)(2,1)}, bf16[32,1024]{1,0:T(8,128)(2,1)}, bf16[32,1024]{1,0:T(8,128)(2,1)}, bf16[32,1024]{1,0:T(8,128)(2,1)}) custom-call(s32[1]{0:T(128)} %bitcast.idx_ref, bf16[512,1152]{1,0:T(8,128)(2,1)} %bitcast.37, s32[2,256]{1,0:T(2,128)} %get-tuple-element.43.slot_ref, f32[256,2]{1,0:T(8,128)} %copy.15.weight_ref), custom_call_target="tpu_custom_call" | custom-call | tf_op jit(solution)/shard_map/combine/pallas_call | solution.py:396
  199.3 0.5 collective-permute-start.25
  199.8 0.9 collective-permute-start.26
  200.7 0.6 collective-permute-start.27
  201.3 4.3 %attn_out.1 = bf16[1024,512]{1,0:T(8,128)(2,1)} custom-call(f32[1024,512]{1,0:T(8,128)} %get-tuple-element.25.o_ref, bf16[1024,256]{1,0:T(8,128)(2,1)} %get-tuple-element.26.qc_ref, bf16[512,1152]{1,0:T(8,128)(2,1)} %bitcast.38, f32[1,256]{1,0:T(1,128)} %bitcast.47), custom_call_target="tpu_custom_call" | custom-call | flops 3000000000 | bytes 4000000 | tf_op jit(solution)/shard_map/attn_out/pallas_call | solution.py:135
  205.6 0.2 collective-permute-done.26.p2
  205.8 0.7 collective-permute-done.27.p3
  206.5 0.6 copy-done.19
  207.2 1.8 finish.1
  (56 shorter events, 0.1 us)
Async XLA Ops:
  0.6 14.7 %copy-start = (bf16[1,4096,256]{2,1,0:T(8,128)(2,1)S(1)}, bf16[1,4096,256]{2,1,0:T(8,128)(2,1)}, u32[]{:S(2)}) copy-start(bf16[1,4096,256]{2,1,0:T(8,128)(2,1)} %param.22) | copy-start | bytes 6291460
  3.7 39.7 %all-to-all-start = ((bf16[32,8,2048]{2,1,0:T(8,128)(2,1)}), bf16[32,8,2048]{2,1,0:T(8,128)(2,1)S(1)}, u32[]{:S(2)}, u32[]{:S(2)}) async-start(bf16[32,8,2048]{2,1,0:T(8,128)(2,1)} %bitcast.42), calls=%async_computation | async-start | bytes 2097152 | tf_op jit(solution)/shard_map/all_to_all | solution.py:163
  15.4 64.3 %collective-permute-start.4 = (bf16[4096,256]{1,0:T(8,128)(2,1)S(1)}, bf16[4096,256]{1,0:T(8,128)(2,1)}, u32[]{:S(2)}, u32[]{:S(2)}) collective-permute-start(bf16[4096,256]{1,0:T(8,128)(2,1)S(1)} %bitcast.30), channel_id=1, source_target_pairs={{0,1},{1,0},{2,3},{3,2},{4,5},{5,4},{6,7},{7,6},{8,9},{9,8},{10,11... | collective-permute-start | bytes 6291464 | tf_op jit(solution)/shard_map/ppermute | solution.py:476
  15.5 65.9 %collective-permute-start.5 = (bf16[4096,256]{1,0:T(8,128)(2,1)}, bf16[4096,256]{1,0:T(8,128)(2,1)}, u32[]{:S(2)}, u32[]{:S(2)}) collective-permute-start(bf16[4096,256]{1,0:T(8,128)(2,1)} %bitcast.31), channel_id=1, source_target_pairs={{0,1},{1,0},{2,3},{3,2},{4,5},{5,4},{6,7},{7,6},{8,9},{9,8},{10,11... | collective-permute-start | bytes 6291464 | tf_op jit(solution)/shard_map/ppermute | solution.py:476
  44.5 15.6 %collective-permute-start.1 = (bf16[128,2048]{1,0:T(8,128)(2,1)}, bf16[128,2048]{1,0:T(8,128)(2,1)S(1)}, u32[]{:S(2)}, u32[]{:S(2)}) collective-permute-start(bf16[128,2048]{1,0:T(8,128)(2,1)} %get-tuple-element.53.refs_1_), channel_id=1, source_target_pairs={{0,6},{2,0},{4,2},{6,4},{1,7},{3,1},{5,3},{7,5},{8,14},{10,8},{12,... | collective-permute-start | bytes 1572872 | tf_op jit(solution)/shard_map/ppermute | solution.py:442
  47.5 21.6 %collective-permute-start.2 = (bf16[128,2048]{1,0:T(8,128)(2,1)}, bf16[128,2048]{1,0:T(8,128)(2,1)}, u32[]{:S(2)}, u32[]{:S(2)}) collective-permute-start(bf16[128,2048]{1,0:T(8,128)(2,1)} %get-tuple-element.54.refs_0_), channel_id=1, source_target_pairs={{0,2},{2,4},{4,6},{6,0},{1,3},{3,5},{5,7},{7,1},{8,10},{10,12},{12... | collective-permute-start | bytes 1572872 | tf_op jit(solution)/shard_map/ppermute | solution.py:446
  47.5 24.3 %collective-permute-start = (bf16[128,2048]{1,0:T(8,128)(2,1)}, bf16[128,2048]{1,0:T(8,128)(2,1)}, u32[]{:S(2)}, u32[]{:S(2)}) collective-permute-start(bf16[128,2048]{1,0:T(8,128)(2,1)} %get-tuple-element.54.refs_0_), channel_id=1, source_target_pairs={{0,6},{2,0},{4,2},{6,4},{1,7},{3,1},{5,3},{7,5},{8,14},{10,8},{12,... | collective-permute-start | bytes 1572872 | tf_op jit(solution)/shard_map/ppermute | solution.py:442
  60.2 13.5 %copy-start.4 = (bf16[128,2048]{1,0:T(8,128)(2,1)}, bf16[128,2048]{1,0:T(8,128)(2,1)S(1)}, u32[]{:S(2)}) copy-start(bf16[128,2048]{1,0:T(8,128)(2,1)S(1)} %collective-permute-done.1.refs_3_) | copy-start | bytes 1572868
  60.2 18.0 %collective-permute-start.3 = (bf16[128,2048]{1,0:T(8,128)(2,1)}, bf16[128,2048]{1,0:T(8,128)(2,1)}, u32[]{:S(2)}, u32[]{:S(2)}) collective-permute-start(bf16[128,2048]{1,0:T(8,128)(2,1)} %get-tuple-element.53.refs_1_), channel_id=1, source_target_pairs={{0,2},{2,4},{4,6},{6,0},{1,3},{3,5},{5,7},{7,1},{8,10},{10,12},{12... | collective-permute-start | bytes 1572872 | tf_op jit(solution)/shard_map/ppermute | solution.py:446
  61.1 14.7 %all-to-all-start.1 = ((bf16[32,24,128]{2,1,0:T(8,128)(2,1)}), bf16[32,24,128]{2,1,0:T(8,128)(2,1)S(1)}, u32[]{:S(2)}, u32[]{:S(2)}) async-start(bf16[32,24,128]{2,1,0:T(8,128)(2,1)} %get-tuple-element.30), calls=%async_computation.1 | async-start | bytes 393216 | tf_op jit(solution)/shard_map/all_to_all | solution.py:163
  69.1 26.4 %copy-start.2 = (bf16[256,1024]{1,0:T(8,128)(2,1)}, bf16[256,1024]{1,0:T(8,128)(2,1)S(1)}, u32[]{:S(2)}) copy-start(bf16[256,1024]{1,0:T(8,128)(2,1)S(1)} %get-tuple-element.39.rest_0_) | copy-start | bytes 1572868
  69.2 25.6 %collective-permute-start.12 = (bf16[256,1024]{1,0:T(8,128)(2,1)}, bf16[256,1024]{1,0:T(8,128)(2,1)}, u32[]{:S(2)}, u32[]{:S(2)}) collective-permute-start(bf16[256,1024]{1,0:T(8,128)(2,1)} %get-tuple-element.51), channel_id=1, source_target_pairs={{0,6},{2,0},{4,2},{6,4},{1,7},{3,1},{5,3},{7,5},{8,14},{10,8},{12,... | collective-permute-start | bytes 1572872 | tf_op jit(solution)/shard_map/ppermute | solution.py:442
  71.8 22.9 %collective-permute-start.13 = (bf16[256,1024]{1,0:T(8,128)(2,1)}, bf16[256,1024]{1,0:T(8,128)(2,1)}, u32[]{:S(2)}, u32[]{:S(2)}) collective-permute-start(bf16[256,1024]{1,0:T(8,128)(2,1)} %get-tuple-element.50), channel_id=1, source_target_pairs={{0,2},{2,4},{4,6},{6,0},{1,3},{3,5},{5,7},{7,1},{8,10},{10,12},{12... | collective-permute-start | bytes 1572872 | tf_op jit(solution)/shard_map/ppermute | solution.py:446
  75.8 0.7 copy-start.3
  78.1 13.3 %collective-permute-start.14 = (bf16[128,1024]{1,0:T(8,128)(2,1)}, bf16[128,1024]{1,0:T(8,128)(2,1)S(1)}, u32[]{:S(2)}, u32[]{:S(2)}) collective-permute-start(bf16[128,1024]{1,0:T(8,128)(2,1)} %get-tuple-element.49), channel_id=1, source_target_pairs={{0,2},{2,4},{4,6},{6,0},{1,3},{3,5},{5,7},{7,1},{8,10},{10,12},{12... | collective-permute-start | bytes 786440 | tf_op jit(solution)/shard_map/ppermute | solution.py:446
  79.7 13.7 %copy-start.5 = (bf16[128,2048]{1,0:T(8,128)(2,1)S(1)}, bf16[128,2048]{1,0:T(8,128)(2,1)}, u32[]{:S(2)}) copy-start(bf16[128,2048]{1,0:T(8,128)(2,1)} %copy-done.4) | copy-start | bytes 1572868
  79.7 13.7 %collective-permute-start.15 = (bf16[128,1024]{1,0:T(8,128)(2,1)}, bf16[128,1024]{1,0:T(8,128)(2,1)S(1)}, u32[]{:S(2)}, u32[]{:S(2)}) collective-permute-start(bf16[128,1024]{1,0:T(8,128)(2,1)} %get-tuple-element.48), channel_id=1, source_target_pairs={{0,6},{2,0},{4,2},{6,4},{1,7},{3,1},{5,3},{7,5},{8,14},{10,8},{12,... | collective-permute-start | bytes 786440 | tf_op jit(solution)/shard_map/ppermute | solution.py:442
  90.3 23.7 %collective-permute-start.6 = (bf16[3,128,512]{2,1,0:T(8,128)(2,1)}, bf16[3,128,512]{2,1,0:T(8,128)(2,1)S(1)}, u32[]{:S(2)}, u32[]{:S(2)}) collective-permute-start(bf16[3,128,512]{2,1,0:T(8,128)(2,1)} %bitcast.39), channel_id=1, source_target_pairs={{0,2},{2,4},{4,6},{6,0},{1,3},{3,5},{5,7},{7,1},{8,10},{10,12},{12... | collective-permute-start | bytes 1179656 | tf_op jit(solution)/shard_map/ppermute | solution.py:446
  91.4 23.1 %collective-permute-start.7 = (bf16[128,2048]{1,0:T(8,128)(2,1)}, bf16[128,2048]{1,0:T(8,128)(2,1)S(1)}, u32[]{:S(2)}, u32[]{:S(2)}) collective-permute-start(bf16[128,2048]{1,0:T(8,128)(2,1)} %collective-permute-done.2.refs_4_), channel_id=1, source_target_pairs={{0,2},{2,4},{4,6},{6,0},{1,3},{3,5},{5,7},{7,1},{8,10},{10,12},{12... | collective-permute-start | bytes 1572872 | tf_op jit(solution)/shard_map/ppermute | solution.py:446
  93.4 2.1 %copy-start.21 = (bf16[128,1024]{1,0:T(8,128)(2,1)}, bf16[128,1024]{1,0:T(8,128)(2,1)S(1)}, u32[]{:S(2)}) copy-start(bf16[128,1024]{1,0:T(8,128)(2,1)S(1)} %collective-permute-done.15) | copy-start | bytes 786436
  93.4 22.5 %collective-permute-start.8 = (bf16[128,2048]{1,0:T(8,128)(2,1)S(1)}, bf16[128,2048]{1,0:T(8,128)(2,1)S(1)}, u32[]{:S(2)}, u32[]{:S(2)}) collective-permute-start(bf16[128,2048]{1,0:T(8,128)(2,1)S(1)} %copy-done.5), channel_id=1, source_target_pairs={{0,6},{2,0},{4,2},{6,4},{1,7},{3,1},{5,3},{7,5},{8,14},{10,8},{12,... | collective-permute-start | bytes 1572872 | tf_op jit(solution)/shard_map/ppermute | solution.py:442
  94.8 19.2 %collective-permute-start.16 = (bf16[128,1024]{1,0:T(8,128)(2,1)S(1)}, bf16[128,1024]{1,0:T(8,128)(2,1)}, u32[]{:S(2)}, u32[]{:S(2)}) collective-permute-start(bf16[128,1024]{1,0:T(8,128)(2,1)S(1)} %collective-permute-done.14), channel_id=1, source_target_pairs={{0,2},{2,4},{4,6},{6,0},{1,3},{3,5},{5,7},{7,1},{8,10},{10,12},{12... | collective-permute-start | bytes 786440 | tf_op jit(solution)/shard_map/ppermute | solution.py:446
  95.5 36.0 %collective-permute-start.22 = (bf16[256,1024]{1,0:T(8,128)(2,1)S(1)}, bf16[256,1024]{1,0:T(8,128)(2,1)S(1)}, u32[]{:S(2)}, u32[]{:S(2)}) collective-permute-start(bf16[256,1024]{1,0:T(8,128)(2,1)S(1)} %get-tuple-element.39.rest_0_), channel_id=1, source_target_pairs={{0,1},{1,0},{2,3},{3,2},{4,5},{5,4},{6,7},{7,6},{8,9},{9,8},{10,11... | collective-permute-start | bytes 1572872 | tf_op jit(solution)/shard_map/ppermute | solution.py:495
  114.0 20.8 %collective-permute-start.23 = (bf16[256,1024]{1,0:T(8,128)(2,1)}, bf16[256,1024]{1,0:T(8,128)(2,1)S(1)}, u32[]{:S(2)}, u32[]{:S(2)}) collective-permute-start(bf16[256,1024]{1,0:T(8,128)(2,1)} %collective-permute-done.12.rest_2_), channel_id=1, source_target_pairs={{0,1},{1,0},{2,3},{3,2},{4,5},{5,4},{6,7},{7,6},{8,9},{9,8},{10,11... | collective-permute-start | bytes 1572872 | tf_op jit(solution)/shard_map/ppermute | solution.py:495
  114.0 17.6 %copy-start.11 = (bf16[3,128,512]{2,1,0:T(8,128)(2,1)}, bf16[3,128,512]{2,1,0:T(8,128)(2,1)S(1)}, u32[]{:S(2)}) copy-start(bf16[3,128,512]{2,1,0:T(8,128)(2,1)S(1)} %collective-permute-done.6.n3) | copy-start | bytes 1179652
  114.0 20.8 %collective-permute-start.24 = (bf16[256,1024]{1,0:T(8,128)(2,1)}, bf16[256,1024]{1,0:T(8,128)(2,1)}, u32[]{:S(2)}, u32[]{:S(2)}) collective-permute-start(bf16[256,1024]{1,0:T(8,128)(2,1)} %collective-permute-done.13.rest_4_), channel_id=1, source_target_pairs={{0,1},{1,0},{2,3},{3,2},{4,5},{5,4},{6,7},{7,6},{8,9},{9,8},{10,11... | collective-permute-start | bytes 1572872 | tf_op jit(solution)/shard_map/ppermute | solution.py:495
  114.5 2.2 %copy-start.6 = (bf16[128,2048]{1,0:T(8,128)(2,1)}, bf16[128,2048]{1,0:T(8,128)(2,1)S(1)}, u32[]{:S(2)}) copy-start(bf16[128,2048]{1,0:T(8,128)(2,1)S(1)} %collective-permute-done.7.refs_0_) | copy-start | bytes 1572868
  114.5 20.4 %collective-permute-start.20 = (bf16[3,128,512]{2,1,0:T(8,128)(2,1)}, bf16[3,128,512]{2,1,0:T(8,128)(2,1)}, u32[]{:S(2)}, u32[]{:S(2)}) collective-permute-start(bf16[3,128,512]{2,1,0:T(8,128)(2,1)} %bitcast.40), channel_id=1, source_target_pairs={{0,6},{2,0},{4,2},{6,4},{1,7},{3,1},{5,3},{7,5},{8,14},{10,8},{12,... | collective-permute-start | bytes 1179656 | tf_op jit(solution)/shard_map/ppermute | solution.py:442
  115.9 0.8 copy-start.7
  115.9 15.6 %collective-permute-start.17 = (bf16[128,1024]{1,0:T(8,128)(2,1)}, bf16[128,1024]{1,0:T(8,128)(2,1)}, u32[]{:S(2)}, u32[]{:S(2)}) collective-permute-start(bf16[128,1024]{1,0:T(8,128)(2,1)} %copy-done.21), channel_id=1, source_target_pairs={{0,6},{2,0},{4,2},{6,4},{1,7},{3,1},{5,3},{7,5},{8,14},{10,8},{12,... | collective-permute-start | bytes 786440 | tf_op jit(solution)/shard_map/ppermute | solution.py:442
  131.5 20.2 %collective-permute-start.9 = (bf16[3,128,512]{2,1,0:T(8,128)(2,1)S(1)}, bf16[3,128,512]{2,1,0:T(8,128)(2,1)S(1)}, u32[]{:S(2)}, u32[]{:S(2)}) collective-permute-start(bf16[3,128,512]{2,1,0:T(8,128)(2,1)S(1)} %collective-permute-done.6.n3), channel_id=1, source_target_pairs={{0,2},{2,4},{4,6},{6,0},{1,3},{3,5},{5,7},{7,1},{8,10},{10,12},{12... | collective-permute-start | bytes 1179656 | tf_op jit(solution)/shard_map/ppermute | solution.py:446
  131.6 14.3 %copy-start.8 = (bf16[256,1024]{1,0:T(8,128)(2,1)}, bf16[256,1024]{1,0:T(8,128)(2,1)S(1)}, u32[]{:S(2)}) copy-start(bf16[256,1024]{1,0:T(8,128)(2,1)S(1)} %collective-permute-done.22.rest_1_) | copy-start | bytes 1572868
  131.6 6.1 %collective-permute-start.10 = (bf16[128,512]{1,0:T(8,128)(2,1)}, bf16[128,512]{1,0:T(8,128)(2,1)S(1)}, u32[]{:S(2)}, u32[]{:S(2)}) collective-permute-start(bf16[128,512]{1,0:T(8,128)(2,1)} %hidden_units.3.f0), channel_id=1, source_target_pairs={{0,6},{2,0},{4,2},{6,4},{1,7},{3,1},{5,3},{7,5},{8,14},{10,8},{12,... | collective-permute-start | bytes 393224 | tf_op jit(solution)/shard_map/ppermute | solution.py:442
  134.8 11.0 %copy-start.9 = (bf16[256,1024]{1,0:T(8,128)(2,1)}, bf16[256,1024]{1,0:T(8,128)(2,1)S(1)}, u32[]{:S(2)}) copy-start(bf16[256,1024]{1,0:T(8,128)(2,1)S(1)} %collective-permute-done.23.rest_3_) | copy-start | bytes 1572868
  134.8 11.0 %collective-permute-start.21 = (bf16[128,512]{1,0:T(8,128)(2,1)}, bf16[128,512]{1,0:T(8,128)(2,1)S(1)}, u32[]{:S(2)}, u32[]{:S(2)}) collective-permute-start(bf16[128,512]{1,0:T(8,128)(2,1)} %hidden_units.3.f0), channel_id=1, source_target_pairs={{0,2},{2,4},{4,6},{6,0},{1,3},{3,5},{5,7},{7,1},{8,10},{10,12},{12... | collective-permute-start | bytes 393224 | tf_op jit(solution)/shard_map/ppermute | solution.py:446
  134.8 16.8 %collective-permute-start.18 = (bf16[128,1024]{1,0:T(8,128)(2,1)}, bf16[128,1024]{1,0:T(8,128)(2,1)S(1)}, u32[]{:S(2)}, u32[]{:S(2)}) collective-permute-start(bf16[128,1024]{1,0:T(8,128)(2,1)} %collective-permute-done.16.rest_0_), channel_id=1, source_target_pairs={{0,1},{1,0},{2,3},{3,2},{4,5},{5,4},{6,7},{7,6},{8,9},{9,8},{10,11... | collective-permute-start | bytes 786440 | tf_op jit(solution)/shard_map/ppermute | solution.py:495
  134.9 16.8 %collective-permute-start.19 = (bf16[128,1024]{1,0:T(8,128)(2,1)}, bf16[128,1024]{1,0:T(8,128)(2,1)S(1)}, u32[]{:S(2)}, u32[]{:S(2)}) collective-permute-start(bf16[128,1024]{1,0:T(8,128)(2,1)} %collective-permute-done.17.rest_1_), channel_id=1, source_target_pairs={{0,1},{1,0},{2,3},{3,2},{4,5},{5,4},{6,7},{7,6},{8,9},{9,8},{10,11... | collective-permute-start | bytes 786440 | tf_op jit(solution)/shard_map/ppermute | solution.py:495
  137.6 8.2 %copy-start.15 = (bf16[128,512]{1,0:T(8,128)(2,1)}, bf16[128,512]{1,0:T(8,128)(2,1)S(1)}, u32[]{:S(2)}) copy-start(bf16[128,512]{1,0:T(8,128)(2,1)S(1)} %collective-permute-done.10.f1) | copy-start | bytes 393220
  137.6 14.1 %collective-permute-start.11 = (bf16[128,512]{1,0:T(8,128)(2,1)S(1)}, bf16[128,512]{1,0:T(8,128)(2,1)S(1)}, u32[]{:S(2)}, u32[]{:S(2)}) collective-permute-start(bf16[128,512]{1,0:T(8,128)(2,1)S(1)} %collective-permute-done.10.f1), channel_id=1, source_target_pairs={{0,6},{2,0},{4,2},{6,4},{1,7},{3,1},{5,3},{7,5},{8,14},{10,8},{12,... | collective-permute-start | bytes 393224 | tf_op jit(solution)/shard_map/ppermute | solution.py:442
  145.8 0.6 copy-start.16
  151.7 0.7 copy-start.12
  151.7 0.8 copy-start.13
  151.7 0.8 copy-start.14
  151.7 0.9 copy-start.10
  156.9 9.4 %copy-start.20 = (f32[256,2]{0,1:T(2,128)S(1)}, f32[256,2]{0,1:T(2,128)}, u32[]{:S(2)}) copy-start(f32[256,2]{0,1:T(2,128)} %param.21) | copy-start | bytes 6148
  156.9 38.8 %all-to-all-start.2 = ((bf16[32,16,1152]{2,1,0:T(8,128)(2,1)}), bf16[32,16,1152]{2,1,0:T(8,128)(2,1)S(1)}, u32[]{:S(2)}, u32[]{:S(2)}) async-start(bf16[32,16,1152]{2,1,0:T(8,128)(2,1)} %bitcast.36), calls=%async_computation.2 | async-start | bytes 2359296 | tf_op jit(solution)/shard_map/all_to_all | solution.py:163
  195.8 1.0 copy-start.1
  199.3 6.3 %collective-permute-start.25 = (bf16[32,1024]{1,0:T(8,128)(2,1)}, bf16[32,1024]{1,0:T(8,128)(2,1)S(1)}, u32[]{:S(2)}, u32[]{:S(2)}) collective-permute-start(bf16[32,1024]{1,0:T(8,128)(2,1)} %get-tuple-element.45), channel_id=1, source_target_pairs={{0,6},{2,0},{4,2},{6,4},{1,7},{3,1},{5,3},{7,5},{8,14},{10,8},{12,... | collective-permute-start | bytes 196616 | tf_op jit(solution)/shard_map/ppermute | solution.py:535
  199.8 6.0 %collective-permute-start.26 = (bf16[32,1024]{1,0:T(8,128)(2,1)}, bf16[32,1024]{1,0:T(8,128)(2,1)S(1)}, u32[]{:S(2)}, u32[]{:S(2)}) collective-permute-start(bf16[32,1024]{1,0:T(8,128)(2,1)} %get-tuple-element.46), channel_id=1, source_target_pairs={{0,4},{2,6},{4,0},{6,2},{1,5},{3,7},{5,1},{7,3},{8,12},{10,14},{12... | collective-permute-start | bytes 196616 | tf_op jit(solution)/shard_map/ppermute | solution.py:535
  200.7 5.8 %collective-permute-start.27 = (bf16[32,1024]{1,0:T(8,128)(2,1)}, bf16[32,1024]{1,0:T(8,128)(2,1)S(1)}, u32[]{:S(2)}, u32[]{:S(2)}) collective-permute-start(bf16[32,1024]{1,0:T(8,128)(2,1)} %get-tuple-element.47), channel_id=1, source_target_pairs={{0,2},{2,4},{4,6},{6,0},{1,3},{3,5},{5,7},{7,1},{8,10},{10,12},{12... | collective-permute-start | bytes 196616 | tf_op jit(solution)/shard_map/ppermute | solution.py:535
  205.6 0.9 copy-start.17
  205.8 0.7 copy-start.18
  206.5 0.6 copy-start.19
where the time goes:
time: 210 us; the launch traced here: 209 us
  waiting for transfers between devices  93 us (44%)
  starting transfers between devices  57.5 us (27%)
  Pallas kernels  47.5 us (23%)
  local copies, waits for them, and re-layouts  10.1 us (5%)
    all_to_all x3, waiting for transfers between devices, exchange(): return lax.all_to_all(x, EP, split_axis=0, concat_axis=0, tiled=True)  48.6 us
    all_to_all x3, starting transfers between devices, exchange(): return lax.all_to_all(x, EP, split_axis=0, concat_axis=0, tiled=True)  26.6 us
    ppermute x9, waiting for transfers between devices, from_left(): return lax.ppermute(x, 'y', ring(NY, 1))  23.1 us
    ppermute x9, starting transfers between devices, from_right(): return lax.ppermute(x, 'y', ring(NY, -1))  20.8 us
    ppermute x9, waiting for transfers between devices, from_right(): return lax.ppermute(x, 'y', ring(NY, -1))  20.3 us
    pallas_call x2, Pallas kernels, hidden_units(): pl.pallas_call(functools.partial(hidden_kernel, parts=len(xs)), grid=(ste...  15.1 us
    pallas_call x1, Pallas kernels, attn_local(): pl.pallas_call(attn_local_kernel, grid=(rows // tile,), in_specs=[pl.Bloc...  9.53 us
    pallas_call x2, Pallas kernels, expert_down(): pl.pallas_call(body, grid=(tiles,), in_specs=[spec(h) for h in hs] + [pl....  9.49 us
  transfers between devices with their start and end apart: 31, of which 10 were waited for; matrix products, arithmetic and copies ran while one was open for 3% of the time, Pallas kernels for 17%

commit v1 on v0

--- a/solution.py
+++ b/solution.py
@@ -129,7 +129,7 @@
         out_ref[:, vs] = (total * lax.rsqrt(mean + 1e-06) * gain).astype(BF16)
 
 
-def attn_out(o, qc, returned, gain, column):
+def attn_out(o, qc, incoming, gain):
     rows, values = o.shape
     tile = 256
     return pl.pallas_call(
@@ -138,7 +138,7 @@
         in_specs=[
             pl.BlockSpec((tile, values), lambda n: (n, 0)),
             pl.BlockSpec((tile, qc.shape[1]), lambda n: (n, 0)),
-            pl.BlockSpec((returned.shape[0], DK), lambda n: (0, column)),
+            pl.BlockSpec(incoming.shape, lambda n: (0, 0)),
             pl.BlockSpec((1, DV), lambda n: (0, 0)),
         ],
         out_specs=pl.BlockSpec((tile, values), lambda n: (n, 0)),
@@ -148,7 +148,7 @@
             flops=3 * 10**9, transcendentals=2048, bytes_accessed=4 * 10**6
         ),
         name="attn_out",
-    )(o, qc, returned, gain.reshape(1, DV))
+    )(o, qc, incoming, gain.reshape(1, DV))
 
 
 def prefix_kernel(in_ref, out_ref):
@@ -313,40 +313,35 @@
     return jnp.concatenate([ordered[(i - shift) % NY] for i in range(NY)], axis=0)
 
 
-def down_sides_kernel(n0, f0, n1, f1, n3, f3, *rest):
-    weights = rest[:6]
-    out_ref = rest[6]
-    width = weights[0].shape[0]
+def down_kernel(n0, f0, n1, f1, n2, f2, n3, f3, *rest):
+    weights = rest[:10]
+    out_ref = rest[10]
+    rows, _ = out_ref.shape
+    group = rows // NY
     total = None
-    for m, act in enumerate((in_blocks(n0, f0, 0), in_blocks(n1, f1, 1), in_blocks(n3, f3, 3))):
-        for c in range(2):
-            term = contract(act[:, c * width : (c + 1) * width], weights[2 * m + c][...], 1, 0)
+    used = 0
+    for m, pair in enumerate(((n0, f0), (n1, f1), (n2, f2), (n3, f3))):
+        act = in_blocks(*pair, m)
+        start = 0
+        while start < act.shape[1]:
+            weight = weights[used]
+            stop = start + weight.shape[0]
+            term = contract(act[:, start:stop], weight[...], 1, 0)
             total = term if total is None else total + term
-    out_ref[...] = total
-
-
-def down_far_kernel(n2, f2, *rest):
-    weights = rest[:4]
-    partial_ref, state_ref, out_ref = rest[4:7]
-    width, depth = weights[0].shape
-    group = f2.shape[0]
-    rows = NY * group
-    total = partial_ref[...]
-    act = in_blocks(n2, f2, 2)
-    for c in range(4):
-        total += contract(act[:, c * width : (c + 1) * width], weights[c][...], 1, 0)
+            start = stop
+            used += 1
     new = lax.broadcasted_iota(jnp.int32, (rows, rows), 0)
     old = lax.broadcasted_iota(jnp.int32, (rows, rows), 1)
     want = (new // CAP % NY) * group + (new // (CAP * NY)) * CAP + new % CAP
     order = jnp.where(old == want, 1.0, 0.0).astype(BF16)
-    out_ref[:, 0:depth] = contract(order, total.astype(BF16), 1, 0).astype(BF16)
-    out_ref[:, depth:] = state_ref[...]
-
-
-def expert_down(body, hs, weights, extra, columns, dtype, tiles=2):
+    out_ref[...] = contract(order, total.astype(BF16), 1, 0).astype(BF16)
+
+
+def expert_down(hs, weights, tiles=2):
     rows, units = hs[1].shape
     group = rows // tiles
     out_rows = NY * rows
+    columns = weights[0].shape[1]
 
     def spec(h):
         if h.ndim == 2:
@@ -354,20 +349,20 @@
         return pl.BlockSpec((h.shape[0], group, units), lambda n: (0, n, 0))
 
     return pl.pallas_call(
-        body,
+        down_kernel,
         grid=(tiles,),
         in_specs=[spec(h) for h in hs]
-        + [pl.BlockSpec(w.shape, lambda n: (0, 0)) for w in weights]
-        + [pl.BlockSpec((out_rows // tiles, x.shape[1]), lambda n: (n, 0)) for x in extra],
+        + [pl.BlockSpec(w.shape, lambda n: (0, 0)) for w in weights],
         out_specs=pl.BlockSpec((out_rows // tiles, columns), lambda n: (n, 0)),
-        out_shape=jax.ShapeDtypeStruct((out_rows, columns), dtype),
+        out_shape=jax.ShapeDtypeStruct((out_rows, columns), BF16),
         compiler_params=pltpu.CompilerParams(dimension_semantics=("arbitrary",)),
         cost_estimate=pl.CostEstimate(
             flops=2 * out_rows * columns * sum(w.shape[0] for w in weights),
             transcendentals=0,
             bytes_accessed=8 * 10**6,
         ),
-    )(*hs, *weights, *extra)
+        name="expert_down",
+    )(*hs, *weights)
 
 
 def combine_kernel(idx_ref, back_ref, slot_ref, weight_ref, o0, o1, o2, o3, *, part):
@@ -391,19 +386,21 @@
         out[...] = mixed[i * part : (i + 1) * part].astype(out.dtype)
 
 
-def combine(index, back, slots, weight, part, width):
+def combine(index, back, slots, weight, part, tiles=4):
     total = weight.shape[0]
+    width = back.shape[1]
+    tile = width // tiles
     return pl.pallas_call(
         functools.partial(combine_kernel, part=part),
         grid_spec=pltpu.PrefetchScalarGridSpec(
             num_scalar_prefetch=1,
-            grid=(1,),
+            grid=(tiles,),
             in_specs=[
-                pl.BlockSpec((back.shape[0], width), lambda n, idx: (0, 0)),
+                pl.BlockSpec((back.shape[0], tile), lambda n, idx: (0, n)),
                 pl.BlockSpec((2, total), lambda n, idx: (0, 0)),
                 pl.BlockSpec((total, 2), lambda n, idx: (0, 0)),
             ],
-            out_specs=[pl.BlockSpec((part, width), lambda n, idx: (0, 0)) for _ in range(NY)],
+            out_specs=[pl.BlockSpec((part, tile), lambda n, idx: (0, n)) for _ in range(NY)],
         ),
         out_shape=[jax.ShapeDtypeStruct((part, width), BF16) for _ in range(NY)],
         name="combine",
@@ -491,7 +488,7 @@
     )
     mine, _ = lax.optimization_barrier((mine, local_state))
     mine[3], mine[4] = from_left(mine[3]), from_right(mine[4])
-    arrived, local_state = lax.optimization_barrier((arrived, local_state))
+    arrived, local_state, mine = lax.optimization_barrier((arrived, local_state, mine))
     d0, d1, d3, d2a, d2b = [(piece, lax.ppermute(piece, "c", swap)) for piece in mine]
 
     half = experts // 2
@@ -511,31 +508,22 @@
     near_left, near_right = from_left(near), from_right(near)
     far_left, far_right = from_left(far), from_right(far)
     near_passed, far = lax.optimization_barrier((near_left, far))
-    near_far, far_far = from_left(near_passed), from_right(far_right)
-    partial = expert_down(
-        down_sides_kernel,
-        (near, far, near_right, far_right, near_left, far_left),
-        (*d0, *d1, *d3),
-        (),
-        cut,
-        F32,
-    )
+    near_far = from_left(near_passed)
+    far_far = from_right(far_right)
+    incoming = exchange(before)
     back = expert_down(
-        down_far_kernel,
-        (near_far, far_far),
-        (d2a[0], d2b[0], d2a[1], d2b[1]),
-        (partial, before.reshape(-1, DK)),
-        cut + DK,
-        BF16,
-    )
-    returned = exchange(back.reshape(experts, NY * CAP, cut + DK)).reshape(-1, cut + DK)
-
-    pieces = combine(index, returned, slots, route_weight, part, cut)
+        (near, far, near_right, far_right, near_far, far_far, near_left, far_left),
+        (*d0, *d1, d2a[0], d2b[0], d2a[1], d2b[1], *d3),
+    )
+    returned = exchange(back.reshape(experts, NY * CAP, cut)).reshape(-1, cut)
+    mixed_heads = attn_out(local_out, query_carry, incoming.reshape(-1, DK), head_gain)
+    returned, mixed_heads = lax.optimization_barrier((returned, mixed_heads))
+
+    pieces = combine(index, returned, slots, route_weight, part)
     gathered = [pieces[0]] + [
         lax.ppermute(pieces[-m % NY], "y", ring(NY, -m)) for m in range(1, NY)
     ]
     routed_out = finish(index, gathered, post_gain)
-    mixed_heads = attn_out(local_out, query_carry, returned, head_gain, cut // DK)
     return (mixed_heads, routed_out)
 
 

time: 210 us -> 199 us (0.948)
  waiting for transfers between devices: 93 us -> 61.7 us
  blocking collectives: 0 us -> 18.8 us
  starting transfers between devices: 57.5 us -> 59.6 us
    all_to_all x3, waiting for transfers between devices: 48.6 us -> 21.9 us  [exchange(): return lax.all_to_all(x, EP, split_axis=0, concat_axis=0, tiled=True)]
    all_to_all x0 -> x1, blocking collectives: none -> 18.8 us  [exchange(): return lax.all_to_all(x, EP, split_axis=0, concat_axis=0, tiled=True)]
    ppermute x9, waiting for transfers between devices: 23.1 us -> 10.5 us  [from_left(): return lax.ppermute(x, 'y', ring(NY, 1))]
    ppermute x3, waiting for transfers between devices: 0.91 us -> 5.12 us  [on_device(): lax.ppermute(pieces[-m % NY], 'y', ring(NY, -m))]
    ppermute x9, waiting for transfers between devices: 20.3 us -> 24.2 us  [from_right(): return lax.ppermute(x, 'y', ring(NY, -1))]
    ppermute x9, starting transfers between devices: 6.38 us -> 9.25 us  [from_left(): return lax.ppermute(x, 'y', ring(NY, 1))]
    pallas_call x2 -> x1, Pallas kernels: 9.49 us -> 6.94 us  [expert_down(): pl.pallas_call(down_kernel, grid=(tiles,), in_specs=[spec(h) for h in hs]...]
    unnamed x45 -> x49, local copies, waits for them, and re-layouts: 4.75 us -> 5.5 us
  transfers between devices with their start and end apart: 31 -> 31, of which waited for: 10 -> 12; matrix products, arithmetic and copies ran while one was open for 3% -> 3% of each run, Pallas kernels for 17% -> 19%
where the time goes in v1:
time: 199 us; the launch traced here: 198 us
  waiting for transfers between devices  61.7 us (31%)
  starting transfers between devices  59.6 us (30%)
  Pallas kernels  46.3 us (23%)
  blocking collectives  18.8 us (9%)
  local copies, waits for them, and re-layouts  11 us (6%)
    all_to_all x3, starting transfers between devices, exchange(): return lax.all_to_all(x, EP, split_axis=0, concat_axis=0, tiled=True)  27 us
    ppermute x9, waiting for transfers between devices, from_right(): return lax.ppermute(x, 'y', ring(NY, -1))  24.2 us
    all_to_all x3, waiting for transfers between devices, exchange(): return lax.all_to_all(x, EP, split_axis=0, concat_axis=0, tiled=True)  21.9 us
    ppermute x9, starting transfers between devices, from_right(): return lax.ppermute(x, 'y', ring(NY, -1))  20.2 us
    all_to_all x1, blocking collectives, exchange(): return lax.all_to_all(x, EP, split_axis=0, concat_axis=0, tiled=True)  18.8 us
    pallas_call x2, Pallas kernels, hidden_units(): pl.pallas_call(functools.partial(hidden_kernel, parts=len(xs)), grid=(ste...  15.1 us
    ppermute x9, waiting for transfers between devices, from_left(): return lax.ppermute(x, 'y', ring(NY, 1))  10.5 us
    pallas_call x1, Pallas kernels, attn_local(): pl.pallas_call(attn_local_kernel, grid=(rows // tile,), in_specs=[pl.Bloc...  9.5 us
  transfers between devices with their start and end apart: 31, of which 12 were waited for; matrix products, arithmetic and copies ran while one was open for 3% of the time, Pallas kernels for 19%

profile of v1, /device:TPU:2, one launch (start us, length us, event | category | flops | bytes accessed | tf_op | source)
XLA Modules:
  0.0 198.3 jit_solution(10071641608110753425)
XLA Ops:
  0.6 3.0 %dispatch.1 = (bf16[256,2048]{1,0:T(8,128)(2,1)}, s32[2,256]{1,0:T(2,128)}) custom-call(s32[1]{0:T(128)} %bitcast.idx_ref, bf16[256,4096]{1,0:T(8,128)(2,1)} %rows_ref.1, f32[1,4096]{1,0:T(1,128)} %bitcast.38, s32[2,256]{1,0:T(2,128)} %bitcast.40), custom_call_target="tpu_custom_call" | custom-call | tf_op jit(solution)/shard_map/dispatch/pallas_call | solution.py:224
  3.6 11.6 %all-to-all-start = ((bf16[32,8,2048]{2,1,0:T(8,128)(2,1)}), bf16[32,8,2048]{2,1,0:T(8,128)(2,1)S(1)}, u32[]{:S(2)}, u32[]{:S(2)}) async-start(bf16[32,8,2048]{2,1,0:T(8,128)(2,1)} %bitcast.32), calls=%async_computation | async-start | bytes 2097152 | tf_op jit(solution)/shard_map/all_to_all | solution.py:163
  15.2 0.0 copy-start
  15.2 1.9 dynamic-slice_bitcast_fusion.3
  17.2 1.6 collective-permute-start.2
  18.7 2.5 %dynamic-slice_bitcast_fusion = (bf16[256,1024]{1,0:T(8,128)(2,1)}, bf16[256,1024]{1,0:T(8,128)(2,1)}, bf16[256,1024]{1,0:T(8,128)(2,1)}) fusion(bf16[1,256,4096]{2,1,0:T(8,128)(2,1)} %param.24, s32[]{:T(128)S(6)} %select_n.14, s32[]{:T(128)S(6)} %select_n.13, s32[]{:T(128)S(6)} %select_n.12), kind=kLoop, calls=%fused_computation.2 | loop fusion | bytes 3145740 | tf_op jit(solution)/shard_map/dynamic_slice | solution.py:476
  21.3 1.7 collective-permute-start
  22.9 0.4 collective-permute-start.1
  23.3 2.9 %collective-permute-start.3 = (bf16[128,1024]{1,0:T(8,128)(2,1)S(1)}, bf16[128,1024]{1,0:T(8,128)(2,1)}, u32[]{:S(2)}, u32[]{:S(2)}) collective-permute-start(bf16[128,1024]{1,0:T(8,128)(2,1)S(1)} %get-tuple-element.62), channel_id=1, source_target_pairs={{0,6},{2,0},{4,2},{6,4},{1,7},{3,1},{5,3},{7,5},{8,14},{10,8},{12,... | collective-permute-start | bytes 786440 | tf_op jit(solution)/shard_map/ppermute | solution.py:439
  26.2 0.0 collective-permute-start.10
  26.2 0.4 collective-permute-done.2
  26.6 0.1 collective-permute-start.11
  26.7 9.5 %attn_local.1 = (f32[1024,512]{1,0:T(8,128)}, bf16[1024,256]{1,0:T(8,128)(2,1)}, bf16[32,24,128]{2,1,0:T(8,128)(2,1)}) custom-call(bf16[1024,256]{1,0:T(8,128)(2,1)} %q_ref.1, bf16[1024,256]{1,0:T(8,128)(2,1)} %k_ref.1, bf16[1024,512]{1,0:T(8,128)(2,1)} %v_ref.1, f32[1024,256]{1,0:T(8,128)} %g_ref.1), custom_call_target="tpu_custom_call" | custom-call | flops 8000000000 | bytes 6000000 | tf_op jit(solution)/shard_map/attn_local/pallas_call | solution.py:91
  36.2 3.8 %collective-permute-done.3 = bf16[128,1024]{1,0:T(8,128)(2,1)} collective-permute-done((bf16[128,1024]{1,0:T(8,128)(2,1)S(1)}, bf16[128,1024]{1,0:T(8,128)(2,1)}, u32[]{:S(2)}, u32[]{:S(2)}) %collective-permute-start.3) | collective-permute-done | bytes 262176 | tf_op jit(solution)/shard_map/ppermute | solution.py:439
  40.0 0.0 collective-permute-done.1.rest_8_
  40.0 1.6 collective-permute-start.4
  41.7 1.7 collective-permute-start.5
  43.4 4.6 %collective-permute-done.4.rest_4_ = bf16[128,1024]{1,0:T(8,128)(2,1)S(1)} collective-permute-done((bf16[128,1024]{1,0:T(8,128)(2,1)}, bf16[128,1024]{1,0:T(8,128)(2,1)S(1)}, u32[]{:S(2)}, u32[]{:S(2)}) %collective-permute-start.4) | collective-permute-done | bytes 262176 | tf_op jit(solution)/shard_map/ppermute | solution.py:443
  47.9 0.7 copy-done.18
  48.6 1.1 slice_bitcast_fusion
  49.7 2.6 %collective-permute-start.6 = (bf16[128,2048]{1,0:T(8,128)(2,1)}, bf16[128,2048]{1,0:T(8,128)(2,1)S(1)}, u32[]{:S(2)}, u32[]{:S(2)}) collective-permute-start(bf16[128,2048]{1,0:T(8,128)(2,1)} %get-tuple-element.68.refs_0_), channel_id=1, source_target_pairs={{0,6},{2,0},{4,2},{6,4},{1,7},{3,1},{5,3},{7,5},{8,14},{10,8},{12,... | collective-permute-start | bytes 1572872 | tf_op jit(solution)/shard_map/ppermute | solution.py:439
  52.3 0.0 collective-permute-start.8
  52.3 3.2 %collective-permute-start.7 = (bf16[128,2048]{1,0:T(8,128)(2,1)}, bf16[128,2048]{1,0:T(8,128)(2,1)S(1)}, u32[]{:S(2)}, u32[]{:S(2)}) collective-permute-start(bf16[128,2048]{1,0:T(8,128)(2,1)} %get-tuple-element.67.refs_1_), channel_id=1, source_target_pairs={{0,6},{2,0},{4,2},{6,4},{1,7},{3,1},{5,3},{7,5},{8,14},{10,8},{12,... | collective-permute-start | bytes 1572872 | tf_op jit(solution)/shard_map/ppermute | solution.py:439
  55.6 9.4 %collective-permute-done.6.refs_2_ = bf16[128,2048]{1,0:T(8,128)(2,1)S(1)} collective-permute-done((bf16[128,2048]{1,0:T(8,128)(2,1)}, bf16[128,2048]{1,0:T(8,128)(2,1)S(1)}, u32[]{:S(2)}, u32[]{:S(2)}) %collective-permute-start.6) | collective-permute-done | bytes 524320 | tf_op jit(solution)/shard_map/ppermute | solution.py:439
  65.0 0.8 collective-permute-start.9
  65.7 18.8 %all_to_all.20.in_ref = bf16[32,24,128]{2,1,0:T(8,128)(2,1)} all-to-all(bf16[32,24,128]{2,1,0:T(8,128)(2,1)S(1)} %copy-done.7), channel_id=1, replica_groups=mesh['z'=8,'x'=4,'y'=4,'c'=2] {'z','x'}, dimensions={0} | all-to-all | bytes 393216 | tf_op jit(solution)/shard_map/all_to_all | solution.py:163
  84.5 1.6 prefix.1
  86.2 1.8 collective-permute-start.13
  88.0 8.9 %hidden_units.2 = bf16[384,512]{1,0:T(8,128)(2,1)} custom-call(bf16[128,2048]{1,0:T(8,128)(2,1)} %get-tuple-element.68.refs_0_, bf16[128,2048]{1,0:T(8,128)(2,1)} %get-tuple-element.67.refs_1_, bf16[128,2048]{1,0:T(8,128)(2,1)} %copy-done.4, bf16[128,2048]{1,0:T(8,128)(2,1)} %copy-done.3, bf16[128,2048]{1,0:T(8,128)(2,1)} %collective-permute-done.8.refs_4_, ...), custom_call_target="tpu_custom_call" | custom-call | flops 3221225472 | bytes 11534336 | tf_op jit(solution)/shard_map/hidden_units/pallas_call | solution.py:294
  96.9 2.8 %collective-permute-start.12 = (bf16[3,128,512]{2,1,0:T(8,128)(2,1)}, bf16[3,128,512]{2,1,0:T(8,128)(2,1)S(1)}, u32[]{:S(2)}, u32[]{:S(2)}) collective-permute-start(bf16[3,128,512]{2,1,0:T(8,128)(2,1)} %bitcast.34), channel_id=1, source_target_pairs={{0,2},{2,4},{4,6},{6,0},{1,3},{3,5},{5,7},{7,1},{8,10},{10,12},{12... | collective-permute-start | bytes 1179656 | tf_op jit(solution)/shard_map/ppermute | solution.py:443
  99.7 0.5 collective-permute-start.14
  100.2 0.5 collective-permute-start.21
  100.7 5.4 %collective-permute-done.12.n3 = bf16[3,128,512]{2,1,0:T(8,128)(2,1)S(1)} collective-permute-done((bf16[3,128,512]{2,1,0:T(8,128)(2,1)}, bf16[3,128,512]{2,1,0:T(8,128)(2,1)S(1)}, u32[]{:S(2)}, u32[]{:S(2)}) %collective-permute-start.12) | collective-permute-done | bytes 393248 | tf_op jit(solution)/shard_map/ppermute | solution.py:443
  106.2 0.5 collective-permute-start.23
  106.7 2.4 %collective-permute-done.14.refs_1_ = bf16[128,2048]{1,0:T(8,128)(2,1)S(1)} collective-permute-done((bf16[128,2048]{1,0:T(8,128)(2,1)}, bf16[128,2048]{1,0:T(8,128)(2,1)S(1)}, u32[]{:S(2)}, u32[]{:S(2)}) %collective-permute-start.14) | collective-permute-done | bytes 524320 | tf_op jit(solution)/shard_map/ppermute | solution.py:439
  109.1 0.8 copy-done.5
  109.9 6.2 %hidden_units.3.f0 = bf16[128,512]{1,0:T(8,128)(2,1)} custom-call(bf16[128,2048]{1,0:T(8,128)(2,1)} %collective-permute-done.13.refs_0_, bf16[128,2048]{1,0:T(8,128)(2,1)} %copy-done.5, bf16[4096,256]{1,0:T(8,128)(2,1)} %bitcast.28, bf16[4096,256]{1,0:T(8,128)(2,1)} %bitcast.29, bf16[4096,256]{1,0:T(8,128)(2,1)} %bitcast.12.refs_8_.refs_9_.refs_4_.refs_5_, ...), custom_call_target="tpu_custom_call" | custom-call | flops 1073741824 | bytes 9437184 | tf_op jit(solution)/shard_map/hidden_units/pallas_call | solution.py:294
  116.1 1.8 collective-permute-start.15
  117.9 0.3 collective-permute-start.17
  118.2 2.9 %collective-permute-start.16 = (bf16[128,512]{1,0:T(8,128)(2,1)}, bf16[128,512]{1,0:T(8,128)(2,1)S(1)}, u32[]{:S(2)}, u32[]{:S(2)}) collective-permute-start(bf16[128,512]{1,0:T(8,128)(2,1)} %hidden_units.3.f0), channel_id=1, source_target_pairs={{0,6},{2,0},{4,2},{6,4},{1,7},{3,1},{5,3},{7,5},{8,14},{10,8},{12,... | collective-permute-start | bytes 393224 | tf_op jit(solution)/shard_map/ppermute | solution.py:439
  121.2 8.6 %collective-permute-done.16.f1 = bf16[128,512]{1,0:T(8,128)(2,1)S(1)} collective-permute-done((bf16[128,512]{1,0:T(8,128)(2,1)}, bf16[128,512]{1,0:T(8,128)(2,1)S(1)}, u32[]{:S(2)}, u32[]{:S(2)}) %collective-permute-start.16) | collective-permute-done | bytes 131104 | tf_op jit(solution)/shard_map/ppermute | solution.py:439
  129.8 2.9 %collective-permute-start.18 = (bf16[128,512]{1,0:T(8,128)(2,1)S(1)}, bf16[128,512]{1,0:T(8,128)(2,1)S(1)}, u32[]{:S(2)}, u32[]{:S(2)}) collective-permute-start(bf16[128,512]{1,0:T(8,128)(2,1)S(1)} %collective-permute-done.16.f1), channel_id=1, source_target_pairs={{0,6},{2,0},{4,2},{6,4},{1,7},{3,1},{5,3},{7,5},{8,14},{10,8},{12,... | collective-permute-start | bytes 393224 | tf_op jit(solution)/shard_map/ppermute | solution.py:439
  132.7 5.6 %all-to-all-start.3 = ((bf16[32,16,128]{2,1,0:T(8,128)(2,1)}), bf16[32,16,128]{2,1,0:T(8,128)(2,1)S(1)}, u32[]{:S(2)}, u32[]{:S(2)}) async-start(bf16[32,16,128]{2,1,0:T(8,128)(2,1)} %prefix.1), calls=%async_computation.3 | async-start | bytes 262144 | tf_op jit(solution)/shard_map/all_to_all | solution.py:163
  138.4 0.7 copy-done.16
  139.1 0.1 copy-done.22
  139.2 0.0 copy-done.23
  139.2 0.8 copy-done.17
  139.9 6.9 %expert_down.1 = bf16[512,1024]{1,0:T(8,128)(2,1)} custom-call(bf16[3,128,512]{2,1,0:T(8,128)(2,1)} %bitcast.35, bf16[128,512]{1,0:T(8,128)(2,1)} %hidden_units.3.f0, bf16[3,128,512]{2,1,0:T(8,128)(2,1)} %copy-done.16, bf16[128,512]{1,0:T(8,128)(2,1)} %copy-done.21, bf16[3,128,512]{2,1,0:T(8,128)(2,1)} %copy-done.17, bf16[128,512]{1,0:T(8,128)(2,1)} %copy-done.23, ...), custom_call_target="tpu_custom_call" | custom-call | flops 2147483648 | bytes 8000000 | tf_op jit(solution)/shard_map/expert_down/pallas_call | solution.py:351
  146.9 0.0 copy-start.12
  146.9 0.4 all-to-all-done.3
  147.3 9.7 %all-to-all-start.2 = ((bf16[32,16,1024]{2,1,0:T(8,128)(2,1)}), bf16[32,16,1024]{2,1,0:T(8,128)(2,1)S(1)}, u32[]{:S(2)}, u32[]{:S(2)}) async-start(bf16[32,16,1024]{2,1,0:T(8,128)(2,1)} %bitcast.33), calls=%async_computation.2 | async-start | bytes 2097152 | tf_op jit(solution)/shard_map/all_to_all | solution.py:163
  157.1 0.8 copy.15.weight_ref
  157.9 4.3 %attn_out.1 = bf16[1024,512]{1,0:T(8,128)(2,1)} custom-call(f32[1024,512]{1,0:T(8,128)} %get-tuple-element.52.o_ref, bf16[1024,256]{1,0:T(8,128)(2,1)} %get-tuple-element.53.qc_ref, bf16[512,128]{1,0:T(8,128)(2,1)} %bitcast.37, f32[1,256]{1,0:T(1,128)} %bitcast.41), custom_call_target="tpu_custom_call" | custom-call | flops 3000000000 | bytes 4000000 | tf_op jit(solution)/shard_map/attn_out/pallas_call | solution.py:135
  162.1 21.5 %all-to-all-done.2 = bf16[32,16,1024]{2,1,0:T(8,128)(2,1)S(1)} async-done(((bf16[32,16,1024]{2,1,0:T(8,128)(2,1)}), bf16[32,16,1024]{2,1,0:T(8,128)(2,1)S(1)}, u32[]{:S(2)}, u32[]{:S(2)}) %all-to-all-start.2) | async-done | bytes 1048608 | tf_op jit(solution)/shard_map/all_to_all | solution.py:163
  183.6 1.0 copy-done.1
  184.6 4.1 %combine.1 = (bf16[32,1024]{1,0:T(8,128)(2,1)}, bf16[32,1024]{1,0:T(8,128)(2,1)}, bf16[32,1024]{1,0:T(8,128)(2,1)}, bf16[32,1024]{1,0:T(8,128)(2,1)}) custom-call(s32[1]{0:T(128)} %bitcast.idx_ref, bf16[512,1024]{1,0:T(8,128)(2,1)} %bitcast.31, s32[2,256]{1,0:T(2,128)} %get-tuple-element.57.slot_ref, f32[256,2]{1,0:T(8,128)} %copy.15.weight_ref), custom_call_target="tpu_custom_call" | custom-call | tf_op jit(solution)/shard_map/combine/pallas_call | solution.py:393
  188.7 0.3 collective-permute-start.25
  189.0 0.9 collective-permute-start.26
  189.9 0.8 collective-permute-start.27
  190.8 2.4 %collective-permute-done.25.p1 = bf16[32,1024]{1,0:T(8,128)(2,1)S(1)} collective-permute-done((bf16[32,1024]{1,0:T(8,128)(2,1)}, bf16[32,1024]{1,0:T(8,128)(2,1)S(1)}, u32[]{:S(2)}, u32[]{:S(2)}) %collective-permute-start.25) | collective-permute-done | bytes 65568 | tf_op jit(solution)/shard_map/ppermute | solution.py:524
  193.2 1.8 collective-permute-done.26.p2
  195.0 0.9 collective-permute-done.27.p3
  195.9 0.6 copy-done.11
  196.5 1.8 finish.1
  (60 shorter events, 0.1 us)
Async XLA Ops:
  3.6 45.0 %all-to-all-start = ((bf16[32,8,2048]{2,1,0:T(8,128)(2,1)}), bf16[32,8,2048]{2,1,0:T(8,128)(2,1)S(1)}, u32[]{:S(2)}, u32[]{:S(2)}) async-start(bf16[32,8,2048]{2,1,0:T(8,128)(2,1)} %bitcast.32), calls=%async_computation | async-start | bytes 2097152 | tf_op jit(solution)/shard_map/all_to_all | solution.py:163
  15.2 10.9 %copy-start = (bf16[1,4096,256]{2,1,0:T(8,128)(2,1)S(1)}, bf16[1,4096,256]{2,1,0:T(8,128)(2,1)}, u32[]{:S(2)}) copy-start(bf16[1,4096,256]{2,1,0:T(8,128)(2,1)} %param.22) | copy-start | bytes 6291460
  17.2 9.5 %collective-permute-start.2 = (bf16[128,1024]{1,0:T(8,128)(2,1)}, bf16[128,1024]{1,0:T(8,128)(2,1)}, u32[]{:S(2)}, u32[]{:S(2)}) collective-permute-start(bf16[128,1024]{1,0:T(8,128)(2,1)} %get-tuple-element.63), channel_id=1, source_target_pairs={{0,2},{2,4},{4,6},{6,0},{1,3},{3,5},{5,7},{7,1},{8,10},{10,12},{12... | collective-permute-start | bytes 786440 | tf_op jit(solution)/shard_map/ppermute | solution.py:443
  21.3 18.8 %collective-permute-start = (bf16[256,1024]{1,0:T(8,128)(2,1)}, bf16[256,1024]{1,0:T(8,128)(2,1)}, u32[]{:S(2)}, u32[]{:S(2)}) collective-permute-start(bf16[256,1024]{1,0:T(8,128)(2,1)} %get-tuple-element.65), channel_id=1, source_target_pairs={{0,6},{2,0},{4,2},{6,4},{1,7},{3,1},{5,3},{7,5},{8,14},{10,8},{12,... | collective-permute-start | bytes 1572872 | tf_op jit(solution)/shard_map/ppermute | solution.py:439
  22.9 17.1 %collective-permute-start.1 = (bf16[256,1024]{1,0:T(8,128)(2,1)}, bf16[256,1024]{1,0:T(8,128)(2,1)}, u32[]{:S(2)}, u32[]{:S(2)}) collective-permute-start(bf16[256,1024]{1,0:T(8,128)(2,1)} %get-tuple-element.64), channel_id=1, source_target_pairs={{0,2},{2,4},{4,6},{6,0},{1,3},{3,5},{5,7},{7,1},{8,10},{10,12},{12... | collective-permute-start | bytes 1572872 | tf_op jit(solution)/shard_map/ppermute | solution.py:443
  23.3 16.7 %collective-permute-start.3 = (bf16[128,1024]{1,0:T(8,128)(2,1)S(1)}, bf16[128,1024]{1,0:T(8,128)(2,1)}, u32[]{:S(2)}, u32[]{:S(2)}) collective-permute-start(bf16[128,1024]{1,0:T(8,128)(2,1)S(1)} %get-tuple-element.62), channel_id=1, source_target_pairs={{0,6},{2,0},{4,2},{6,4},{1,7},{3,1},{5,3},{7,5},{8,14},{10,8},{12,... | collective-permute-start | bytes 786440 | tf_op jit(solution)/shard_map/ppermute | solution.py:439
  26.2 61.8 %collective-permute-start.10 = (bf16[4096,256]{1,0:T(8,128)(2,1)S(1)}, bf16[4096,256]{1,0:T(8,128)(2,1)}, u32[]{:S(2)}, u32[]{:S(2)}) collective-permute-start(bf16[4096,256]{1,0:T(8,128)(2,1)S(1)} %bitcast.30), channel_id=1, source_target_pairs={{0,1},{1,0},{2,3},{3,2},{4,5},{5,4},{6,7},{7,6},{8,9},{9,8},{10,11... | collective-permute-start | bytes 6291464 | tf_op jit(solution)/shard_map/ppermute | solution.py:473
  26.6 61.3 %collective-permute-start.11 = (bf16[4096,256]{1,0:T(8,128)(2,1)}, bf16[4096,256]{1,0:T(8,128)(2,1)}, u32[]{:S(2)}, u32[]{:S(2)}) collective-permute-start(bf16[4096,256]{1,0:T(8,128)(2,1)} %bitcast.12.refs_8_.refs_9_.refs_4_.refs_5_), channel_id=1, source_target_pairs={{0,1},{1,0},{2,3},{3,2},{4,5},{5,4},{6,7},{7,6},{8,9},{9,8},{10,11... | collective-permute-start | bytes 6291464 | tf_op jit(solution)/shard_map/ppermute | solution.py:473
  40.0 25.7 %copy-start.7 = (bf16[32,24,128]{2,1,0:T(8,128)(2,1)S(1)}, bf16[32,24,128]{2,1,0:T(8,128)(2,1)}, u32[]{:S(2)}) copy-start(bf16[32,24,128]{2,1,0:T(8,128)(2,1)} %get-tuple-element.40) | copy-start | bytes 589828
  40.0 7.9 %collective-permute-start.4 = (bf16[128,1024]{1,0:T(8,128)(2,1)}, bf16[128,1024]{1,0:T(8,128)(2,1)S(1)}, u32[]{:S(2)}, u32[]{:S(2)}) collective-permute-start(bf16[128,1024]{1,0:T(8,128)(2,1)} %collective-permute-done.2), channel_id=1, source_target_pairs={{0,2},{2,4},{4,6},{6,0},{1,3},{3,5},{5,7},{7,1},{8,10},{10,12},{12... | collective-permute-start | bytes 786440 | tf_op jit(solution)/shard_map/ppermute | solution.py:443
  41.7 6.9 %collective-permute-start.5 = (bf16[128,1024]{1,0:T(8,128)(2,1)}, bf16[128,1024]{1,0:T(8,128)(2,1)}, u32[]{:S(2)}, u32[]{:S(2)}) collective-permute-start(bf16[128,1024]{1,0:T(8,128)(2,1)} %collective-permute-done.3), channel_id=1, source_target_pairs={{0,6},{2,0},{4,2},{6,4},{1,7},{3,1},{5,3},{7,5},{8,14},{10,8},{12,... | collective-permute-start | bytes 786440 | tf_op jit(solution)/shard_map/ppermute | solution.py:439
  47.9 0.7 copy-start.18
  49.7 15.3 %collective-permute-start.6 = (bf16[128,2048]{1,0:T(8,128)(2,1)}, bf16[128,2048]{1,0:T(8,128)(2,1)S(1)}, u32[]{:S(2)}, u32[]{:S(2)}) collective-permute-start(bf16[128,2048]{1,0:T(8,128)(2,1)} %get-tuple-element.68.refs_0_), channel_id=1, source_target_pairs={{0,6},{2,0},{4,2},{6,4},{1,7},{3,1},{5,3},{7,5},{8,14},{10,8},{12,... | collective-permute-start | bytes 1572872 | tf_op jit(solution)/shard_map/ppermute | solution.py:439
  52.3 33.9 %collective-permute-start.8 = (bf16[128,2048]{1,0:T(8,128)(2,1)}, bf16[128,2048]{1,0:T(8,128)(2,1)}, u32[]{:S(2)}, u32[]{:S(2)}) collective-permute-start(bf16[128,2048]{1,0:T(8,128)(2,1)} %get-tuple-element.68.refs_0_), channel_id=1, source_target_pairs={{0,2},{2,4},{4,6},{6,0},{1,3},{3,5},{5,7},{7,1},{8,10},{10,12},{12... | collective-permute-start | bytes 1572872 | tf_op jit(solution)/shard_map/ppermute | solution.py:443
  52.3 33.9 %collective-permute-start.7 = (bf16[128,2048]{1,0:T(8,128)(2,1)}, bf16[128,2048]{1,0:T(8,128)(2,1)S(1)}, u32[]{:S(2)}, u32[]{:S(2)}) collective-permute-start(bf16[128,2048]{1,0:T(8,128)(2,1)} %get-tuple-element.67.refs_1_), channel_id=1, source_target_pairs={{0,6},{2,0},{4,2},{6,4},{1,7},{3,1},{5,3},{7,5},{8,14},{10,8},{12,... | collective-permute-start | bytes 1572872 | tf_op jit(solution)/shard_map/ppermute | solution.py:439
  65.0 19.6 %copy-start.4 = (bf16[128,2048]{1,0:T(8,128)(2,1)}, bf16[128,2048]{1,0:T(8,128)(2,1)S(1)}, u32[]{:S(2)}) copy-start(bf16[128,2048]{1,0:T(8,128)(2,1)S(1)} %collective-permute-done.6.refs_2_) | copy-start | bytes 1572868
  65.0 21.2 %collective-permute-start.9 = (bf16[128,2048]{1,0:T(8,128)(2,1)}, bf16[128,2048]{1,0:T(8,128)(2,1)}, u32[]{:S(2)}, u32[]{:S(2)}) collective-permute-start(bf16[128,2048]{1,0:T(8,128)(2,1)} %get-tuple-element.67.refs_1_), channel_id=1, source_target_pairs={{0,2},{2,4},{4,6},{6,0},{1,3},{3,5},{5,7},{7,1},{8,10},{10,12},{12... | collective-permute-start | bytes 1572872 | tf_op jit(solution)/shard_map/ppermute | solution.py:443
  86.2 14.0 %copy-start.2 = (bf16[256,1024]{1,0:T(8,128)(2,1)S(1)}, bf16[256,1024]{1,0:T(8,128)(2,1)}, u32[]{:S(2)}) copy-start(bf16[256,1024]{1,0:T(8,128)(2,1)} %get-tuple-element.47.rest_0_) | copy-start | bytes 1572868
  86.2 20.0 %copy-start.19 = (bf16[128,1024]{1,0:T(8,128)(2,1)S(1)}, bf16[128,1024]{1,0:T(8,128)(2,1)}, u32[]{:S(2)}) copy-start(bf16[128,1024]{1,0:T(8,128)(2,1)} %copy-done.18) | copy-start | bytes 786436
  86.2 1.8 copy-start.3
  86.2 20.0 %collective-permute-start.13 = (bf16[128,2048]{1,0:T(8,128)(2,1)}, bf16[128,2048]{1,0:T(8,128)(2,1)}, u32[]{:S(2)}, u32[]{:S(2)}) collective-permute-start(bf16[128,2048]{1,0:T(8,128)(2,1)} %collective-permute-done.8.refs_4_), channel_id=1, source_target_pairs={{0,2},{2,4},{4,6},{6,0},{1,3},{3,5},{5,7},{7,1},{8,10},{10,12},{12... | collective-permute-start | bytes 1572872 | tf_op jit(solution)/shard_map/ppermute | solution.py:443
  96.9 19.2 %copy-start.6 = (bf16[384,512]{1,0:T(8,128)(2,1)S(1)}, bf16[384,512]{1,0:T(8,128)(2,1)}, u32[]{:S(2)}) copy-start(bf16[384,512]{1,0:T(8,128)(2,1)} %hidden_units.2) | copy-start | bytes 1179652
  96.9 9.3 %collective-permute-start.12 = (bf16[3,128,512]{2,1,0:T(8,128)(2,1)}, bf16[3,128,512]{2,1,0:T(8,128)(2,1)S(1)}, u32[]{:S(2)}, u32[]{:S(2)}) collective-permute-start(bf16[3,128,512]{2,1,0:T(8,128)(2,1)} %bitcast.34), channel_id=1, source_target_pairs={{0,2},{2,4},{4,6},{6,0},{1,3},{3,5},{5,7},{7,1},{8,10},{10,12},{12... | collective-permute-start | bytes 1179656 | tf_op jit(solution)/shard_map/ppermute | solution.py:443
  99.7 9.4 %collective-permute-start.14 = (bf16[128,2048]{1,0:T(8,128)(2,1)}, bf16[128,2048]{1,0:T(8,128)(2,1)S(1)}, u32[]{:S(2)}, u32[]{:S(2)}) collective-permute-start(bf16[128,2048]{1,0:T(8,128)(2,1)} %copy-done.3), channel_id=1, source_target_pairs={{0,6},{2,0},{4,2},{6,4},{1,7},{3,1},{5,3},{7,5},{8,14},{10,8},{12,... | collective-permute-start | bytes 1572872 | tf_op jit(solution)/shard_map/ppermute | solution.py:439
  100.2 18.0 %collective-permute-start.20 = (bf16[256,1024]{1,0:T(8,128)(2,1)S(1)}, bf16[256,1024]{1,0:T(8,128)(2,1)S(1)}, u32[]{:S(2)}, u32[]{:S(2)}) collective-permute-start(bf16[256,1024]{1,0:T(8,128)(2,1)S(1)} %copy-done.2), channel_id=1, source_target_pairs={{0,1},{1,0},{2,3},{3,2},{4,5},{5,4},{6,7},{7,6},{8,9},{9,8},{10,11... | collective-permute-start | bytes 1572872 | tf_op jit(solution)/shard_map/ppermute | solution.py:492
  100.2 21.0 %collective-permute-start.21 = (bf16[256,1024]{1,0:T(8,128)(2,1)}, bf16[256,1024]{1,0:T(8,128)(2,1)S(1)}, u32[]{:S(2)}, u32[]{:S(2)}) collective-permute-start(bf16[256,1024]{1,0:T(8,128)(2,1)} %collective-permute-done.rest_2_), channel_id=1, source_target_pairs={{0,1},{1,0},{2,3},{3,2},{4,5},{5,4},{6,7},{7,6},{8,9},{9,8},{10,11... | collective-permute-start | bytes 1572872 | tf_op jit(solution)/shard_map/ppermute | solution.py:492
  106.2 11.7 %copy-start.15 = (bf16[3,128,512]{2,1,0:T(8,128)(2,1)}, bf16[3,128,512]{2,1,0:T(8,128)(2,1)S(1)}, u32[]{:S(2)}) copy-start(bf16[3,128,512]{2,1,0:T(8,128)(2,1)S(1)} %collective-permute-done.12.n3) | copy-start | bytes 1179652
  106.2 9.9 %collective-permute-start.22 = (bf16[128,1024]{1,0:T(8,128)(2,1)S(1)}, bf16[128,1024]{1,0:T(8,128)(2,1)S(1)}, u32[]{:S(2)}, u32[]{:S(2)}) collective-permute-start(bf16[128,1024]{1,0:T(8,128)(2,1)S(1)} %copy-done.19), channel_id=1, source_target_pairs={{0,1},{1,0},{2,3},{3,2},{4,5},{5,4},{6,7},{7,6},{8,9},{9,8},{10,11... | collective-permute-start | bytes 786440 | tf_op jit(solution)/shard_map/ppermute | solution.py:492
  106.2 11.7 %collective-permute-start.23 = (bf16[128,1024]{1,0:T(8,128)(2,1)}, bf16[128,1024]{1,0:T(8,128)(2,1)}, u32[]{:S(2)}, u32[]{:S(2)}) collective-permute-start(bf16[128,1024]{1,0:T(8,128)(2,1)} %collective-permute-done.5.rest_5_), channel_id=1, source_target_pairs={{0,1},{1,0},{2,3},{3,2},{4,5},{5,4},{6,7},{7,6},{8,9},{9,8},{10,11... | collective-permute-start | bytes 786440 | tf_op jit(solution)/shard_map/ppermute | solution.py:492
  109.1 0.8 copy-start.5
  109.1 29.2 %collective-permute-start.24 = (bf16[256,1024]{1,0:T(8,128)(2,1)}, bf16[256,1024]{1,0:T(8,128)(2,1)}, u32[]{:S(2)}, u32[]{:S(2)}) collective-permute-start(bf16[256,1024]{1,0:T(8,128)(2,1)} %collective-permute-done.1.rest_8_), channel_id=1, source_target_pairs={{0,1},{1,0},{2,3},{3,2},{4,5},{5,4},{6,7},{7,6},{8,9},{9,8},{10,11... | collective-permute-start | bytes 1572872 | tf_op jit(solution)/shard_map/ppermute | solution.py:492
  116.1 16.6 %copy-start.20 = (bf16[128,1024]{1,0:T(8,128)(2,1)}, bf16[128,1024]{1,0:T(8,128)(2,1)S(1)}, u32[]{:S(2)}) copy-start(bf16[128,1024]{1,0:T(8,128)(2,1)S(1)} %collective-permute-done.22.rest_6_) | copy-start | bytes 786436
  116.1 22.2 %collective-permute-start.15 = (bf16[3,128,512]{2,1,0:T(8,128)(2,1)S(1)}, bf16[3,128,512]{2,1,0:T(8,128)(2,1)S(1)}, u32[]{:S(2)}, u32[]{:S(2)}) collective-permute-start(bf16[3,128,512]{2,1,0:T(8,128)(2,1)S(1)} %bitcast.36), channel_id=1, source_target_pairs={{0,6},{2,0},{4,2},{6,4},{1,7},{3,1},{5,3},{7,5},{8,14},{10,8},{12,... | collective-permute-start | bytes 1179656 | tf_op jit(solution)/shard_map/ppermute | solution.py:439
  117.9 20.5 %collective-permute-start.17 = (bf16[3,128,512]{2,1,0:T(8,128)(2,1)S(1)}, bf16[3,128,512]{2,1,0:T(8,128)(2,1)S(1)}, u32[]{:S(2)}, u32[]{:S(2)}) collective-permute-start(bf16[3,128,512]{2,1,0:T(8,128)(2,1)S(1)} %collective-permute-done.12.n3), channel_id=1, source_target_pairs={{0,2},{2,4},{4,6},{6,0},{1,3},{3,5},{5,7},{7,1},{8,10},{10,12},{12... | collective-permute-start | bytes 1179656 | tf_op jit(solution)/shard_map/ppermute | solution.py:443
  118.2 20.2 %copy-start.13 = (bf16[256,1024]{1,0:T(8,128)(2,1)}, bf16[256,1024]{1,0:T(8,128)(2,1)S(1)}, u32[]{:S(2)}) copy-start(bf16[256,1024]{1,0:T(8,128)(2,1)S(1)} %collective-permute-done.20.rest_1_) | copy-start | bytes 1572868
  118.2 11.5 %collective-permute-start.16 = (bf16[128,512]{1,0:T(8,128)(2,1)}, bf16[128,512]{1,0:T(8,128)(2,1)S(1)}, u32[]{:S(2)}, u32[]{:S(2)}) collective-permute-start(bf16[128,512]{1,0:T(8,128)(2,1)} %hidden_units.3.f0), channel_id=1, source_target_pairs={{0,6},{2,0},{4,2},{6,4},{1,7},{3,1},{5,3},{7,5},{8,14},{10,8},{12,... | collective-permute-start | bytes 393224 | tf_op jit(solution)/shard_map/ppermute | solution.py:439
  121.2 17.3 %copy-start.14 = (bf16[256,1024]{1,0:T(8,128)(2,1)}, bf16[256,1024]{1,0:T(8,128)(2,1)S(1)}, u32[]{:S(2)}) copy-start(bf16[256,1024]{1,0:T(8,128)(2,1)S(1)} %collective-permute-done.21.rest_3_) | copy-start | bytes 1572868
  121.2 17.2 %collective-permute-start.19 = (bf16[128,512]{1,0:T(8,128)(2,1)}, bf16[128,512]{1,0:T(8,128)(2,1)S(1)}, u32[]{:S(2)}, u32[]{:S(2)}) collective-permute-start(bf16[128,512]{1,0:T(8,128)(2,1)} %hidden_units.3.f0), channel_id=1, source_target_pairs={{0,2},{2,4},{4,6},{6,0},{1,3},{3,5},{5,7},{7,1},{8,10},{10,12},{12... | collective-permute-start | bytes 393224 | tf_op jit(solution)/shard_map/ppermute | solution.py:443
  129.8 8.7 %copy-start.21 = (bf16[128,512]{1,0:T(8,128)(2,1)}, bf16[128,512]{1,0:T(8,128)(2,1)S(1)}, u32[]{:S(2)}) copy-start(bf16[128,512]{1,0:T(8,128)(2,1)S(1)} %collective-permute-done.16.f1) | copy-start | bytes 393220
  129.8 8.6 %collective-permute-start.18 = (bf16[128,512]{1,0:T(8,128)(2,1)S(1)}, bf16[128,512]{1,0:T(8,128)(2,1)S(1)}, u32[]{:S(2)}, u32[]{:S(2)}) collective-permute-start(bf16[128,512]{1,0:T(8,128)(2,1)S(1)} %collective-permute-done.16.f1), channel_id=1, source_target_pairs={{0,6},{2,0},{4,2},{6,4},{1,7},{3,1},{5,3},{7,5},{8,14},{10,8},{12,... | collective-permute-start | bytes 393224 | tf_op jit(solution)/shard_map/ppermute | solution.py:439
  132.7 14.6 %all-to-all-start.3 = ((bf16[32,16,128]{2,1,0:T(8,128)(2,1)}), bf16[32,16,128]{2,1,0:T(8,128)(2,1)S(1)}, u32[]{:S(2)}, u32[]{:S(2)}) async-start(bf16[32,16,128]{2,1,0:T(8,128)(2,1)} %prefix.1), calls=%async_computation.3 | async-start | bytes 262144 | tf_op jit(solution)/shard_map/all_to_all | solution.py:163
  138.4 0.8 copy-start.16
  138.4 0.8 copy-start.22
  138.4 0.8 copy-start.23
  139.2 0.8 copy-start.17
  146.9 10.2 %copy-start.12 = (f32[256,2]{0,1:T(2,128)S(1)}, f32[256,2]{0,1:T(2,128)}, u32[]{:S(2)}) copy-start(f32[256,2]{0,1:T(2,128)} %param.21) | copy-start | bytes 6148
  147.3 10.5 %copy-start.8 = (bf16[32,16,128]{2,1,0:T(8,128)(2,1)}, bf16[32,16,128]{2,1,0:T(8,128)(2,1)S(1)}, u32[]{:S(2)}) copy-start(bf16[32,16,128]{2,1,0:T(8,128)(2,1)S(1)} %all-to-all-done.3) | copy-start | bytes 393220
  147.3 36.3 %all-to-all-start.2 = ((bf16[32,16,1024]{2,1,0:T(8,128)(2,1)}), bf16[32,16,1024]{2,1,0:T(8,128)(2,1)S(1)}, u32[]{:S(2)}, u32[]{:S(2)}) async-start(bf16[32,16,1024]{2,1,0:T(8,128)(2,1)} %bitcast.33), calls=%async_computation.2 | async-start | bytes 2097152 | tf_op jit(solution)/shard_map/all_to_all | solution.py:163
  183.6 1.0 copy-start.1
  188.7 4.5 %collective-permute-start.25 = (bf16[32,1024]{1,0:T(8,128)(2,1)}, bf16[32,1024]{1,0:T(8,128)(2,1)S(1)}, u32[]{:S(2)}, u32[]{:S(2)}) collective-permute-start(bf16[32,1024]{1,0:T(8,128)(2,1)} %get-tuple-element.59), channel_id=1, source_target_pairs={{0,6},{2,0},{4,2},{6,4},{1,7},{3,1},{5,3},{7,5},{8,14},{10,8},{12,... | collective-permute-start | bytes 196616 | tf_op jit(solution)/shard_map/ppermute | solution.py:524
  189.0 6.0 %collective-permute-start.26 = (bf16[32,1024]{1,0:T(8,128)(2,1)}, bf16[32,1024]{1,0:T(8,128)(2,1)S(1)}, u32[]{:S(2)}, u32[]{:S(2)}) collective-permute-start(bf16[32,1024]{1,0:T(8,128)(2,1)} %get-tuple-element.60), channel_id=1, source_target_pairs={{0,4},{2,6},{4,0},{6,2},{1,5},{3,7},{5,1},{7,3},{8,12},{10,14},{12... | collective-permute-start | bytes 196616 | tf_op jit(solution)/shard_map/ppermute | solution.py:524
  189.9 6.0 %collective-permute-start.27 = (bf16[32,1024]{1,0:T(8,128)(2,1)}, bf16[32,1024]{1,0:T(8,128)(2,1)S(1)}, u32[]{:S(2)}, u32[]{:S(2)}) collective-permute-start(bf16[32,1024]{1,0:T(8,128)(2,1)} %get-tuple-element.61), channel_id=1, source_target_pairs={{0,2},{2,4},{4,6},{6,0},{1,3},{3,5},{5,7},{7,1},{8,10},{10,12},{12... | collective-permute-start | bytes 196616 | tf_op jit(solution)/shard_map/ppermute | solution.py:524
  193.2 2.7 %copy-start.9 = (bf16[32,1024]{1,0:T(8,128)(2,1)}, bf16[32,1024]{1,0:T(8,128)(2,1)S(1)}, u32[]{:S(2)}) copy-start(bf16[32,1024]{1,0:T(8,128)(2,1)S(1)} %collective-permute-done.25.p1) | copy-start | bytes 196612
  195.0 0.9 copy-start.10
  195.9 0.6 copy-start.11

commit v2 on v0

--- a/solution.py
+++ b/solution.py
@@ -184,7 +184,18 @@
     return contract(wide, pick, 1, 0)[0:2].astype(jnp.int32)
 
 
-def dispatch_kernel(idx_ref, rows_ref, gain_ref, pick_ref, out_ref, slot_ref, *, part, experts):
+def dispatch_kernel(
+    idx_ref, rows_ref, gain_ref, pick_ref, down_ref, out_ref, slot_ref, *rest, part, experts
+):
+    cuts, sems = rest[:NY], rest[NY]
+    cut = cuts[0].shape[1]
+    copies = []
+    for i, dst in enumerate(cuts):
+        column = pl.multiple_of(((idx_ref[0] // 2 + i) % NY) * cut, cut)
+        copies.append(
+            pltpu.make_async_copy(down_ref.at[:, pl.ds(column, cut)], dst, sems.at[i])
+        )
+        copies[-1].start()
     total = pick_ref.shape[1]
     pick = pick_ref[...]
     first = pick[0:1]
@@ -217,9 +228,11 @@
         )
         total_out = piece if total_out is None else total_out + piece
     out_ref[...] = total_out.astype(BF16)
-
-
-def dispatch(index, rows, gain, pick, part, experts):
+    for copy in copies:
+        copy.wait()
+
+
+def dispatch(index, rows, gain, pick, down, part, experts):
     total, width = rows.shape
     return pl.pallas_call(
         functools.partial(dispatch_kernel, part=part, experts=experts),
@@ -230,18 +243,22 @@
                 pl.BlockSpec((part, width), lambda n, idx: (idx[0], 0)),
                 pl.BlockSpec((1, width), lambda n, idx: (0, 0)),
                 pl.BlockSpec((2, total), lambda n, idx: (0, 0)),
+                pl.BlockSpec(memory_space=pl.ANY),
             ],
             out_specs=[
                 pl.BlockSpec((experts * CAP * 2, width // 2), lambda n, idx: (0, 0)),
                 pl.BlockSpec((2, total), lambda n, idx: (0, 0)),
-            ],
+            ]
+            + [pl.BlockSpec(memory_space=pl.ANY)] * NY,
+            scratch_shapes=[pltpu.SemaphoreType.DMA((NY,))],
         ),
         out_shape=[
             jax.ShapeDtypeStruct((experts * CAP * 2, width // 2), BF16),
             jax.ShapeDtypeStruct((2, total), jnp.int32),
-        ],
+        ]
+        + [jax.ShapeDtypeStruct((down.shape[0], down.shape[1] // NY), BF16)] * NY,
         name="dispatch",
-    )(index, rows, gain.reshape(1, width), pick.T)
+    )(index, rows, gain.reshape(1, width), pick.T, down)
 
 
 def hidden_kernel(*refs, parts):
@@ -313,28 +330,19 @@
     return jnp.concatenate([ordered[(i - shift) % NY] for i in range(NY)], axis=0)
 
 
-def down_sides_kernel(n0, f0, n1, f1, n3, f3, *rest):
-    weights = rest[:6]
-    out_ref = rest[6]
-    width = weights[0].shape[0]
+def down_kernel(n0, f0, n1, f1, n2a, n2b, f2, n3, f3, *rest):
+    weights = rest[:8]
+    state_ref, out_ref = rest[8:10]
+    width, depth = weights[0].shape
+    rows = out_ref.shape[0]
+    group = rows // NY
+    pairs = ((n0, f0), (n1, f1), ((n2a[0], n2a[1], n2b[0]), f2), (n3, f3))
     total = None
-    for m, act in enumerate((in_blocks(n0, f0, 0), in_blocks(n1, f1, 1), in_blocks(n3, f3, 3))):
+    for m, pair in enumerate(pairs):
+        act = in_blocks(*pair, m)
         for c in range(2):
             term = contract(act[:, c * width : (c + 1) * width], weights[2 * m + c][...], 1, 0)
             total = term if total is None else total + term
-    out_ref[...] = total
-
-
-def down_far_kernel(n2, f2, *rest):
-    weights = rest[:4]
-    partial_ref, state_ref, out_ref = rest[4:7]
-    width, depth = weights[0].shape
-    group = f2.shape[0]
-    rows = NY * group
-    total = partial_ref[...]
-    act = in_blocks(n2, f2, 2)
-    for c in range(4):
-        total += contract(act[:, c * width : (c + 1) * width], weights[c][...], 1, 0)
     new = lax.broadcasted_iota(jnp.int32, (rows, rows), 0)
     old = lax.broadcasted_iota(jnp.int32, (rows, rows), 1)
     want = (new // CAP % NY) * group + (new // (CAP * NY)) * CAP + new % CAP
@@ -343,10 +351,11 @@
     out_ref[:, depth:] = state_ref[...]
 
 
-def expert_down(body, hs, weights, extra, columns, dtype, tiles=2):
+def expert_down(hs, weights, states, tiles=2):
     rows, units = hs[1].shape
     group = rows // tiles
     out_rows = NY * rows
+    columns = weights[0].shape[1] + states.shape[1]
 
     def spec(h):
         if h.ndim == 2:
@@ -354,20 +363,21 @@
         return pl.BlockSpec((h.shape[0], group, units), lambda n: (0, n, 0))
 
     return pl.pallas_call(
-        body,
+        down_kernel,
         grid=(tiles,),
         in_specs=[spec(h) for h in hs]
         + [pl.BlockSpec(w.shape, lambda n: (0, 0)) for w in weights]
-        + [pl.BlockSpec((out_rows // tiles, x.shape[1]), lambda n: (n, 0)) for x in extra],
+        + [pl.BlockSpec((out_rows // tiles, states.shape[1]), lambda n: (n, 0))],
         out_specs=pl.BlockSpec((out_rows // tiles, columns), lambda n: (n, 0)),
-        out_shape=jax.ShapeDtypeStruct((out_rows, columns), dtype),
+        out_shape=jax.ShapeDtypeStruct((out_rows, columns), BF16),
         compiler_params=pltpu.CompilerParams(dimension_semantics=("arbitrary",)),
         cost_estimate=pl.CostEstimate(
             flops=2 * out_rows * columns * sum(w.shape[0] for w in weights),
             transcendentals=0,
             bytes_accessed=8 * 10**6,
         ),
-    )(*hs, *weights, *extra)
+        name="expert_down",
+    )(*hs, *weights, states)
 
 
 def combine_kernel(idx_ref, back_ref, slot_ref, weight_ref, o0, o1, o2, o3, *, part):
@@ -469,30 +479,23 @@
     index = (y * 2 + core).astype(jnp.int32).reshape(1)
     swap = [(0, 1), (1, 0)]
 
-    outgoing, slots = dispatch(index, routed_rows, pre_gain, expert_pick, part, experts)
+    gate, up, down = gate_weight[0], up_weight[0], down_weight[0]
+    outgoing, slots, *slices = dispatch(
+        index, routed_rows, pre_gain, expert_pick, down, part, experts
+    )
     arrived = exchange(outgoing.reshape(experts, 2 * CAP, width // 2))
 
-    gate, up, down = gate_weight[0], up_weight[0], down_weight[0]
     weights = (gate, up, lax.ppermute(gate, "c", swap), lax.ppermute(up, "c", swap))
     cut = width // NY
-    slices = [
-        lax.dynamic_slice_in_dim(down, lax.rem(y + i, NY) * cut, cut, axis=1) for i in range(NY)
-    ]
-    middle = down.shape[0] // 2
-    mine = [
-        slices[0],
-        from_right(slices[3]),
-        from_left(slices[1]),
-        from_left(slices[2][:middle]),
-        from_right(slices[2][middle:]),
-    ]
+    mine = [slices[0]] + [lax.ppermute(slices[-m % NY], "y", ring(NY, -m)) for m in range(1, NY)]
     local_out, query_carry, local_state = attn_local(
         queries, key_vectors, value_vectors, decay_logit
     )
     mine, _ = lax.optimization_barrier((mine, local_state))
-    mine[3], mine[4] = from_left(mine[3]), from_right(mine[4])
     arrived, local_state = lax.optimization_barrier((arrived, local_state))
-    d0, d1, d3, d2a, d2b = [(piece, lax.ppermute(piece, "c", swap)) for piece in mine]
+    downs = []
+    for piece in mine:
+        downs += [piece, lax.ppermute(piece, "c", swap)]
 
     half = experts // 2
     top = arrived[:half].reshape(-1, width // 2)
@@ -510,23 +513,13 @@
     far = hidden_units([far_top, far_bottom], weights)
     near_left, near_right = from_left(near), from_right(near)
     far_left, far_right = from_left(far), from_right(far)
-    near_passed, far = lax.optimization_barrier((near_left, far))
-    near_far, far_far = from_left(near_passed), from_right(far_right)
-    partial = expert_down(
-        down_sides_kernel,
-        (near, far, near_right, far_right, near_left, far_left),
-        (*d0, *d1, *d3),
-        (),
-        cut,
-        F32,
-    )
+    far_far = lax.ppermute(far, "y", ring(NY, 2))
+    near_left, near_right, far = lax.optimization_barrier((near_left, near_right, far))
+    near_far = (from_left(near_left[:2]), from_right(near_right[2:]))
     back = expert_down(
-        down_far_kernel,
-        (near_far, far_far),
-        (d2a[0], d2b[0], d2a[1], d2b[1]),
-        (partial, before.reshape(-1, DK)),
-        cut + DK,
-        BF16,
+        (near, far, near_right, far_right, *near_far, far_far, near_left, far_left),
+        downs,
+        before.reshape(-1, DK),
     )
     returned = exchange(back.reshape(experts, NY * CAP, cut + DK)).reshape(-1, cut + DK)
 

time: 210 us -> 268 us (1.28)
  Pallas kernels: 47.5 us -> 108 us
  waiting for transfers between devices: 93 us -> 102 us
  starting transfers between devices: 57.5 us -> 51 us
  local copies, waits for them, and re-layouts: 10.1 us -> 5.56 us
    pallas_call x1, Pallas kernels: 3.1 us -> 66.6 us  [dispatch(): pl.pallas_call(functools.partial(dispatch_kernel, part=part, experts=expe...]
    ppermute x5 -> x8, waiting for transfers between devices: 0.01 us -> 12.2 us  [the longest x3 11.4 us: on_device(): lax.ppermute(slices[-m % NY], 'y', ring(NY, -m))]
    ppermute x9 -> x6, starting transfers between devices: 20.8 us -> 12 us  [from_right(): return lax.ppermute(x, 'y', ring(NY, -1))]
    ppermute x9 -> x6, waiting for transfers between devices: 23.1 us -> 14.8 us  [from_left(): return lax.ppermute(x, 'y', ring(NY, 1))]
    ppermute x5 -> x8, starting transfers between devices: 1.09 us -> 8.94 us  [the longest x3 7.7 us: on_device(): lax.ppermute(slices[-m % NY], 'y', ring(NY, -m))]
    all_to_all x3, starting transfers between devices: 26.6 us -> 23.1 us  [exchange(): return lax.all_to_all(x, EP, split_axis=0, concat_axis=0, tiled=True)]
    all_to_all x3, waiting for transfers between devices: 48.6 us -> 51.8 us  [exchange(): return lax.all_to_all(x, EP, split_axis=0, concat_axis=0, tiled=True)]
    pallas_call x2 -> x1, Pallas kernels: 9.49 us -> 6.43 us  [expert_down(): pl.pallas_call(down_kernel, grid=(tiles,), in_specs=[spec(h) for h in hs]...]
  transfers between devices with their start and end apart: 31 -> 28, of which waited for: 10 -> 14; matrix products, arithmetic and copies ran while one was open for 3% -> 1% of each run, Pallas kernels for 17% -> 11%
where the time goes in v2:
time: 268 us; the launch traced here: 267 us
  Pallas kernels  108 us (40%)
  waiting for transfers between devices  102 us (38%)
  starting transfers between devices  51 us (19%)
  local copies, waits for them, and re-layouts  5.56 us (2%)
    pallas_call x1, Pallas kernels, dispatch(): pl.pallas_call(functools.partial(dispatch_kernel, part=part, experts=expe...  66.6 us
    all_to_all x3, waiting for transfers between devices, exchange(): return lax.all_to_all(x, EP, split_axis=0, concat_axis=0, tiled=True)  51.8 us
    all_to_all x3, starting transfers between devices, exchange(): return lax.all_to_all(x, EP, split_axis=0, concat_axis=0, tiled=True)  23.1 us
    ppermute x6, waiting for transfers between devices, from_right(): return lax.ppermute(x, 'y', ring(NY, -1))  22.1 us
    pallas_call x2, Pallas kernels, hidden_units(): pl.pallas_call(functools.partial(hidden_kernel, parts=len(xs)), grid=(ste...  15.1 us
    ppermute x6, waiting for transfers between devices, from_left(): return lax.ppermute(x, 'y', ring(NY, 1))  14.8 us
    ppermute x6, starting transfers between devices, from_right(): return lax.ppermute(x, 'y', ring(NY, -1))  12 us
    ppermute x3, waiting for transfers between devices, on_device(): lax.ppermute(slices[-m % NY], 'y', ring(NY, -m))  11.4 us
  transfers between devices with their start and end apart: 28, of which 14 were waited for; matrix products, arithmetic and copies ran while one was open for 1% of the time, Pallas kernels for 11%

profile of v2, /device:TPU:2, one launch (start us, length us, event | category | flops | bytes accessed | tf_op | source)
XLA Modules:
  0.0 267.2 jit_solution(9693722543233498925)
XLA Ops:
  0.6 66.6 %dispatch.1 = (bf16[256,2048]{1,0:T(8,128)(2,1)}, s32[2,256]{1,0:T(2,128)}, bf16[256,1024]{1,0:T(8,128)(2,1)}, bf16[256,1024]{1,0:T(8,128)(2,1)}, bf16[256,1024]{1,0:T(8,128)(2,1)}, /*index=5*/bf16[256,1024]{1,0:T(8,128)(2,1)}) custom-call(s32[1]{0:T(128)} %bitcast.idx_ref, bf16[256,4096]{1,0:T(8,128)(2,1)} %rows_ref.1, f32[1,4096]{1,0:T(1,128)} %bitcast.36, ...), custom_call_target="tpu_custom_call" | custom-call | tf_op jit(solution)/shard_map/dispatch/pallas_call | solution.py:237
  67.3 0.0 copy-start
  67.3 11.8 %all-to-all-start = ((bf16[32,8,2048]{2,1,0:T(8,128)(2,1)}), bf16[32,8,2048]{2,1,0:T(8,128)(2,1)S(1)}, u32[]{:S(2)}, u32[]{:S(2)}) async-start(bf16[32,8,2048]{2,1,0:T(8,128)(2,1)} %bitcast.31), calls=%async_computation | async-start | bytes 2097152 | tf_op jit(solution)/shard_map/all_to_all | solution.py:163
  79.1 0.1 collective-permute-start.4
  79.2 0.5 collective-permute-start.5
  79.7 9.5 %attn_local.1 = (f32[1024,512]{1,0:T(8,128)}, bf16[1024,256]{1,0:T(8,128)(2,1)}, bf16[32,24,128]{2,1,0:T(8,128)(2,1)}) custom-call(bf16[1024,256]{1,0:T(8,128)(2,1)} %q_ref.1, bf16[1024,256]{1,0:T(8,128)(2,1)} %k_ref.1, bf16[1024,512]{1,0:T(8,128)(2,1)} %v_ref.1, f32[1024,256]{1,0:T(8,128)} %g_ref.1), custom_call_target="tpu_custom_call" | custom-call | flops 8000000000 | bytes 6000000 | tf_op jit(solution)/shard_map/attn_local/pallas_call | solution.py:91
  89.1 18.0 %all-to-all-done = bf16[32,8,2048]{2,1,0:T(8,128)(2,1)S(1)} async-done(((bf16[32,8,2048]{2,1,0:T(8,128)(2,1)}), bf16[32,8,2048]{2,1,0:T(8,128)(2,1)S(1)}, u32[]{:S(2)}, u32[]{:S(2)}) %all-to-all-start) | async-done | bytes 1048608 | tf_op jit(solution)/shard_map/all_to_all | solution.py:163
  107.1 1.0 slice_bitcast_fusion
  108.1 3.0 %collective-permute-start = (bf16[128,2048]{1,0:T(8,128)(2,1)}, bf16[128,2048]{1,0:T(8,128)(2,1)}, u32[]{:S(2)}, u32[]{:S(2)}) collective-permute-start(bf16[128,2048]{1,0:T(8,128)(2,1)} %get-tuple-element.57.refs_0_), channel_id=1, source_target_pairs={{0,6},{2,0},{4,2},{6,4},{1,7},{3,1},{5,3},{7,5},{8,14},{10,8},{12,... | collective-permute-start | bytes 1572872 | tf_op jit(solution)/shard_map/ppermute | solution.py:452
  111.2 0.7 collective-permute-start.1
  111.9 1.3 collective-permute-start.2
  113.2 10.6 %collective-permute-done.refs_2_ = bf16[128,2048]{1,0:T(8,128)(2,1)} collective-permute-done((bf16[128,2048]{1,0:T(8,128)(2,1)}, bf16[128,2048]{1,0:T(8,128)(2,1)}, u32[]{:S(2)}, u32[]{:S(2)}) %collective-permute-start) | collective-permute-done | bytes 524320 | tf_op jit(solution)/shard_map/ppermute | solution.py:452
  123.8 1.0 collective-permute-start.3
  124.8 5.6 %all-to-all-start.1 = ((bf16[32,24,128]{2,1,0:T(8,128)(2,1)}), bf16[32,24,128]{2,1,0:T(8,128)(2,1)S(1)}, u32[]{:S(2)}, u32[]{:S(2)}) async-start(bf16[32,24,128]{2,1,0:T(8,128)(2,1)} %get-tuple-element.34), calls=%async_computation.1 | async-start | bytes 393216 | tf_op jit(solution)/shard_map/all_to_all | solution.py:163
  130.4 1.7 collective-permute-done.1.refs_3_
  132.1 3.6 %collective-permute-start.15 = (bf16[256,1024]{1,0:T(8,128)(2,1)}, bf16[256,1024]{1,0:T(8,128)(2,1)}, u32[]{:S(2)}, u32[]{:S(2)}) collective-permute-start(bf16[256,1024]{1,0:T(8,128)(2,1)} %get-tuple-element.43), channel_id=1, source_target_pairs={{0,6},{2,0},{4,2},{6,4},{1,7},{3,1},{5,3},{7,5},{8,14},{10,8},{12,... | collective-permute-start | bytes 1572872 | tf_op jit(solution)/shard_map/ppermute | solution.py:490
  135.6 3.9 %all-to-all-done.1.in_ref = bf16[32,24,128]{2,1,0:T(8,128)(2,1)S(1)} async-done(((bf16[32,24,128]{2,1,0:T(8,128)(2,1)}), bf16[32,24,128]{2,1,0:T(8,128)(2,1)S(1)}, u32[]{:S(2)}, u32[]{:S(2)}) %all-to-all-start.1) | async-done | bytes 196640 | tf_op jit(solution)/shard_map/all_to_all | solution.py:163
  139.5 0.7 copy-done.2
  140.2 1.6 prefix.1
  141.8 0.0 collective-permute-done.2.refs_4_
  141.8 4.1 %collective-permute-start.16 = (bf16[256,1024]{1,0:T(8,128)(2,1)}, bf16[256,1024]{1,0:T(8,128)(2,1)}, u32[]{:S(2)}, u32[]{:S(2)}) collective-permute-start(bf16[256,1024]{1,0:T(8,128)(2,1)} %get-tuple-element.44), channel_id=1, source_target_pairs={{0,4},{2,6},{4,0},{6,2},{1,5},{3,7},{5,1},{7,3},{8,12},{10,14},{12... | collective-permute-start | bytes 1572872 | tf_op jit(solution)/shard_map/ppermute | solution.py:490
  146.0 0.1 collective-permute-start.8
  146.1 3.4 %collective-permute-start.9 = (bf16[128,2048]{1,0:T(8,128)(2,1)S(1)}, bf16[128,2048]{1,0:T(8,128)(2,1)S(1)}, u32[]{:S(2)}, u32[]{:S(2)}) collective-permute-start(bf16[128,2048]{1,0:T(8,128)(2,1)S(1)} %collective-permute-done.1.refs_3_), channel_id=1, source_target_pairs={{0,6},{2,0},{4,2},{6,4},{1,7},{3,1},{5,3},{7,5},{8,14},{10,8},{12,... | collective-permute-start | bytes 1572872 | tf_op jit(solution)/shard_map/ppermute | solution.py:452
  149.5 8.9 %hidden_units.2 = bf16[384,512]{1,0:T(8,128)(2,1)} custom-call(bf16[128,2048]{1,0:T(8,128)(2,1)} %get-tuple-element.57.refs_0_, bf16[128,2048]{1,0:T(8,128)(2,1)} %get-tuple-element.56.refs_1_, bf16[128,2048]{1,0:T(8,128)(2,1)} %collective-permute-done.refs_2_, bf16[128,2048]{1,0:T(8,128)(2,1)} %copy-done.3, bf16[128,2048]{1,0:T(8,128)(2,1)} %copy-done.4, ...), custom_call_target="tpu_custom_call" | custom-call | flops 3221225472 | bytes 11534336 | tf_op jit(solution)/shard_map/hidden_units/pallas_call | solution.py:311
  158.4 0.1 collective-permute-start.6
  158.5 0.6 collective-permute-done.16.rest_4_
  159.0 10.8 %collective-permute-done.17.rest_6_ = bf16[256,1024]{1,0:T(8,128)(2,1)} collective-permute-done((bf16[256,1024]{1,0:T(8,128)(2,1)}, bf16[256,1024]{1,0:T(8,128)(2,1)}, u32[]{:S(2)}, u32[]{:S(2)}) %collective-permute-start.17) | collective-permute-done | bytes 524320 | tf_op jit(solution)/shard_map/ppermute | solution.py:490
  169.8 0.0 collective-permute-start.18
  169.8 0.5 collective-permute-start.19
  170.3 13.3 %collective-permute-done.6.n3 = bf16[3,128,512]{2,1,0:T(8,128)(2,1)S(1)} collective-permute-done((bf16[3,128,512]{2,1,0:T(8,128)(2,1)}, bf16[3,128,512]{2,1,0:T(8,128)(2,1)S(1)}, u32[]{:S(2)}, u32[]{:S(2)}) %collective-permute-start.6) | collective-permute-done | bytes 393248 | tf_op jit(solution)/shard_map/ppermute | solution.py:456
  183.7 0.0 copy-start.5
  183.7 0.7 collective-permute-start.7
  184.4 0.0 collective-permute-done.9.refs_1_
  184.4 0.1 collective-permute-start.21
  184.5 0.6 copy-done.6
  185.1 6.2 %hidden_units.3.f0 = bf16[128,512]{1,0:T(8,128)(2,1)} custom-call(bf16[128,2048]{1,0:T(8,128)(2,1)} %copy-done.5, bf16[128,2048]{1,0:T(8,128)(2,1)} %copy-done.6, bf16[4096,256]{1,0:T(8,128)(2,1)} %bitcast.19, bf16[4096,256]{1,0:T(8,128)(2,1)} %bitcast.20, bf16[4096,256]{1,0:T(8,128)(2,1)} %bitcast.25, bf16[4096,256]{1,0:T(8,128)(2,1)} %bitcast.26, ...), custom_call_target="tpu_custom_call" | custom-call | flops 1073741824 | bytes 9437184 | tf_op jit(solution)/shard_map/hidden_units/pallas_call | solution.py:311
  191.4 4.1 %collective-permute-done.7.n1 = bf16[3,128,512]{2,1,0:T(8,128)(2,1)S(1)} collective-permute-done((bf16[3,128,512]{2,1,0:T(8,128)(2,1)}, bf16[3,128,512]{2,1,0:T(8,128)(2,1)S(1)}, u32[]{:S(2)}, u32[]{:S(2)}) %collective-permute-start.7) | collective-permute-done | bytes 393248 | tf_op jit(solution)/shard_map/ppermute | solution.py:452
  195.5 1.8 collective-permute-start.11
  197.3 1.6 collective-permute-start.10
  198.9 0.6 collective-permute-start.13
  199.5 0.0 collective-permute-done.20.rest_5_
  199.5 2.6 collective-permute-start.12
  202.1 0.0 collective-permute-start.14
  202.1 2.2 collective-permute-done.10.f1
  204.3 3.6 %collective-permute-done.12.n2b = bf16[1,128,512]{2,1,0:T(8,128)(2,1)S(1)} collective-permute-done((bf16[1,128,512]{2,1,0:T(8,128)(2,1)S(1)}, bf16[1,128,512]{2,1,0:T(8,128)(2,1)S(1)}, u32[]{:S(2)}, u32[]{:S(2)}) %collective-permute-start.12) | collective-permute-done | bytes 131104 | tf_op jit(solution)/shard_map/ppermute | solution.py:452
  207.9 0.8 collective-permute-done.13.f2
  208.7 1.4 collective-permute-done.14.f3
  210.2 0.6 copy-done.18
  210.8 0.1 copy-done.14
  210.9 6.4 %expert_down.1 = bf16[512,1152]{1,0:T(8,128)(2,1)} custom-call(bf16[3,128,512]{2,1,0:T(8,128)(2,1)} %bitcast.34, bf16[128,512]{1,0:T(8,128)(2,1)} %hidden_units.3.f0, bf16[3,128,512]{2,1,0:T(8,128)(2,1)} %copy-done.11, bf16[128,512]{1,0:T(8,128)(2,1)} %copy-done.15, bf16[2,128,512]{2,1,0:T(8,128)(2,1)} %copy-done.14, bf16[1,128,512]{2,1,0:T(8,128)(2,1)} %copy-done.17, ...), custom_call_target="tpu_custom_call" | custom-call | flops 2415919104 | bytes 8000000 | tf_op jit(solution)/shard_map/expert_down/pallas_call | solution.py:365
  217.4 0.0 copy-start.12
  217.4 5.7 %all-to-all-start.2 = ((bf16[32,16,1152]{2,1,0:T(8,128)(2,1)}), bf16[32,16,1152]{2,1,0:T(8,128)(2,1)S(1)}, u32[]{:S(2)}, u32[]{:S(2)}) async-start(bf16[32,16,1152]{2,1,0:T(8,128)(2,1)} %bitcast.30), calls=%async_computation.2 | async-start | bytes 2359296 | tf_op jit(solution)/shard_map/all_to_all | solution.py:163
  223.2 0.8 copy.15.weight_ref
  224.0 30.0 %all-to-all-done.2 = bf16[32,16,1152]{2,1,0:T(8,128)(2,1)S(1)} async-done(((bf16[32,16,1152]{2,1,0:T(8,128)(2,1)}), bf16[32,16,1152]{2,1,0:T(8,128)(2,1)S(1)}, u32[]{:S(2)}, u32[]{:S(2)}) %all-to-all-start.2) | async-done | bytes 1179680 | tf_op jit(solution)/shard_map/all_to_all | solution.py:163
  253.9 1.0 copy-done.1
  254.9 2.5 combine.1
  257.5 0.2 collective-permute-start.22
  257.7 1.4 collective-permute-start.23
  259.1 0.4 collective-permute-start.24
  259.5 4.3 %attn_out.1 = bf16[1024,512]{1,0:T(8,128)(2,1)} custom-call(f32[1024,512]{1,0:T(8,128)} %get-tuple-element.29.o_ref, bf16[1024,256]{1,0:T(8,128)(2,1)} %get-tuple-element.30.qc_ref, bf16[512,1152]{1,0:T(8,128)(2,1)} %bitcast.28, f32[1,256]{1,0:T(1,128)} %bitcast.39), custom_call_target="tpu_custom_call" | custom-call | flops 3000000000 | bytes 4000000 | tf_op jit(solution)/shard_map/attn_out/pallas_call | solution.py:135
  263.8 0.0 collective-permute-done.22.p1
  263.8 0.9 collective-permute-done.24.p3
  264.8 0.6 copy-done.10
  265.4 1.8 finish.1
  (43 shorter events, 0.1 us)
Async XLA Ops:
  67.3 11.8 %copy-start = (bf16[1,4096,256]{2,1,0:T(8,128)(2,1)S(1)}, bf16[1,4096,256]{2,1,0:T(8,128)(2,1)}, u32[]{:S(2)}) copy-start(bf16[1,4096,256]{2,1,0:T(8,128)(2,1)} %param.22) | copy-start | bytes 6291460
  67.3 39.8 %all-to-all-start = ((bf16[32,8,2048]{2,1,0:T(8,128)(2,1)}), bf16[32,8,2048]{2,1,0:T(8,128)(2,1)S(1)}, u32[]{:S(2)}, u32[]{:S(2)}) async-start(bf16[32,8,2048]{2,1,0:T(8,128)(2,1)} %bitcast.31), calls=%async_computation | async-start | bytes 2097152 | tf_op jit(solution)/shard_map/all_to_all | solution.py:163
  79.1 66.9 %collective-permute-start.4 = (bf16[4096,256]{1,0:T(8,128)(2,1)S(1)}, bf16[4096,256]{1,0:T(8,128)(2,1)}, u32[]{:S(2)}, u32[]{:S(2)}) collective-permute-start(bf16[4096,256]{1,0:T(8,128)(2,1)S(1)} %bitcast.21), channel_id=1, source_target_pairs={{0,1},{1,0},{2,3},{3,2},{4,5},{5,4},{6,7},{7,6},{8,9},{9,8},{10,11... | collective-permute-start | bytes 6291464 | tf_op jit(solution)/shard_map/ppermute | solution.py:488
  79.2 66.9 %collective-permute-start.5 = (bf16[4096,256]{1,0:T(8,128)(2,1)}, bf16[4096,256]{1,0:T(8,128)(2,1)}, u32[]{:S(2)}, u32[]{:S(2)}) collective-permute-start(bf16[4096,256]{1,0:T(8,128)(2,1)} %bitcast.22), channel_id=1, source_target_pairs={{0,1},{1,0},{2,3},{3,2},{4,5},{5,4},{6,7},{7,6},{8,9},{9,8},{10,11... | collective-permute-start | bytes 6291464 | tf_op jit(solution)/shard_map/ppermute | solution.py:488
  108.1 15.6 %collective-permute-start = (bf16[128,2048]{1,0:T(8,128)(2,1)}, bf16[128,2048]{1,0:T(8,128)(2,1)}, u32[]{:S(2)}, u32[]{:S(2)}) collective-permute-start(bf16[128,2048]{1,0:T(8,128)(2,1)} %get-tuple-element.57.refs_0_), channel_id=1, source_target_pairs={{0,6},{2,0},{4,2},{6,4},{1,7},{3,1},{5,3},{7,5},{8,14},{10,8},{12,... | collective-permute-start | bytes 1572872 | tf_op jit(solution)/shard_map/ppermute | solution.py:452
  111.2 20.9 %collective-permute-start.1 = (bf16[128,2048]{1,0:T(8,128)(2,1)}, bf16[128,2048]{1,0:T(8,128)(2,1)S(1)}, u32[]{:S(2)}, u32[]{:S(2)}) collective-permute-start(bf16[128,2048]{1,0:T(8,128)(2,1)} %get-tuple-element.56.refs_1_), channel_id=1, source_target_pairs={{0,6},{2,0},{4,2},{6,4},{1,7},{3,1},{5,3},{7,5},{8,14},{10,8},{12,... | collective-permute-start | bytes 1572872 | tf_op jit(solution)/shard_map/ppermute | solution.py:452
  111.9 29.9 %collective-permute-start.2 = (bf16[128,2048]{1,0:T(8,128)(2,1)}, bf16[128,2048]{1,0:T(8,128)(2,1)S(1)}, u32[]{:S(2)}, u32[]{:S(2)}) collective-permute-start(bf16[128,2048]{1,0:T(8,128)(2,1)} %get-tuple-element.57.refs_0_), channel_id=1, source_target_pairs={{0,2},{2,4},{4,6},{6,0},{1,3},{3,5},{5,7},{7,1},{8,10},{10,12},{12... | collective-permute-start | bytes 1572872 | tf_op jit(solution)/shard_map/ppermute | solution.py:456
  123.8 22.2 %collective-permute-start.3 = (bf16[128,2048]{1,0:T(8,128)(2,1)}, bf16[128,2048]{1,0:T(8,128)(2,1)}, u32[]{:S(2)}, u32[]{:S(2)}) collective-permute-start(bf16[128,2048]{1,0:T(8,128)(2,1)} %get-tuple-element.56.refs_1_), channel_id=1, source_target_pairs={{0,2},{2,4},{4,6},{6,0},{1,3},{3,5},{5,7},{7,1},{8,10},{10,12},{12... | collective-permute-start | bytes 1572872 | tf_op jit(solution)/shard_map/ppermute | solution.py:456
  124.8 14.7 %all-to-all-start.1 = ((bf16[32,24,128]{2,1,0:T(8,128)(2,1)}), bf16[32,24,128]{2,1,0:T(8,128)(2,1)S(1)}, u32[]{:S(2)}, u32[]{:S(2)}) async-start(bf16[32,24,128]{2,1,0:T(8,128)(2,1)} %get-tuple-element.34), calls=%async_computation.1 | async-start | bytes 393216 | tf_op jit(solution)/shard_map/all_to_all | solution.py:163
  132.1 17.4 %copy-start.3 = (bf16[128,2048]{1,0:T(8,128)(2,1)}, bf16[128,2048]{1,0:T(8,128)(2,1)S(1)}, u32[]{:S(2)}) copy-start(bf16[128,2048]{1,0:T(8,128)(2,1)S(1)} %collective-permute-done.1.refs_3_) | copy-start | bytes 1572868
  132.1 26.3 %collective-permute-start.15 = (bf16[256,1024]{1,0:T(8,128)(2,1)}, bf16[256,1024]{1,0:T(8,128)(2,1)}, u32[]{:S(2)}, u32[]{:S(2)}) collective-permute-start(bf16[256,1024]{1,0:T(8,128)(2,1)} %get-tuple-element.43), channel_id=1, source_target_pairs={{0,6},{2,0},{4,2},{6,4},{1,7},{3,1},{5,3},{7,5},{8,14},{10,8},{12,... | collective-permute-start | bytes 1572872 | tf_op jit(solution)/shard_map/ppermute | solution.py:490
  139.5 0.7 copy-start.2
  141.8 7.6 %copy-start.4 = (bf16[128,2048]{1,0:T(8,128)(2,1)}, bf16[128,2048]{1,0:T(8,128)(2,1)S(1)}, u32[]{:S(2)}) copy-start(bf16[128,2048]{1,0:T(8,128)(2,1)S(1)} %collective-permute-done.2.refs_4_) | copy-start | bytes 1572868
  141.8 17.2 %collective-permute-start.16 = (bf16[256,1024]{1,0:T(8,128)(2,1)}, bf16[256,1024]{1,0:T(8,128)(2,1)}, u32[]{:S(2)}, u32[]{:S(2)}) collective-permute-start(bf16[256,1024]{1,0:T(8,128)(2,1)} %get-tuple-element.44), channel_id=1, source_target_pairs={{0,4},{2,6},{4,0},{6,2},{1,5},{3,7},{5,1},{7,3},{8,12},{10,14},{12... | collective-permute-start | bytes 1572872 | tf_op jit(solution)/shard_map/ppermute | solution.py:490
  146.0 23.9 %collective-permute-start.17 = (bf16[256,1024]{1,0:T(8,128)(2,1)}, bf16[256,1024]{1,0:T(8,128)(2,1)}, u32[]{:S(2)}, u32[]{:S(2)}) collective-permute-start(bf16[256,1024]{1,0:T(8,128)(2,1)} %get-tuple-element.45), channel_id=1, source_target_pairs={{0,2},{2,4},{4,6},{6,0},{1,3},{3,5},{5,7},{7,1},{8,10},{10,12},{12... | collective-permute-start | bytes 1572872 | tf_op jit(solution)/shard_map/ppermute | solution.py:490
  146.0 37.7 %collective-permute-start.8 = (bf16[128,2048]{1,0:T(8,128)(2,1)S(1)}, bf16[128,2048]{1,0:T(8,128)(2,1)S(1)}, u32[]{:S(2)}, u32[]{:S(2)}) collective-permute-start(bf16[128,2048]{1,0:T(8,128)(2,1)S(1)} %collective-permute-done.2.refs_4_), channel_id=1, source_target_pairs={{0,2},{2,4},{4,6},{6,0},{1,3},{3,5},{5,7},{7,1},{8,10},{10,12},{12... | collective-permute-start | bytes 1572872 | tf_op jit(solution)/shard_map/ppermute | solution.py:456
  146.1 38.3 %collective-permute-start.9 = (bf16[128,2048]{1,0:T(8,128)(2,1)S(1)}, bf16[128,2048]{1,0:T(8,128)(2,1)S(1)}, u32[]{:S(2)}, u32[]{:S(2)}) collective-permute-start(bf16[128,2048]{1,0:T(8,128)(2,1)S(1)} %collective-permute-done.1.refs_3_), channel_id=1, source_target_pairs={{0,6},{2,0},{4,2},{6,4},{1,7},{3,1},{5,3},{7,5},{8,14},{10,8},{12,... | collective-permute-start | bytes 1572872 | tf_op jit(solution)/shard_map/ppermute | solution.py:452
  158.4 25.3 %collective-permute-start.6 = (bf16[3,128,512]{2,1,0:T(8,128)(2,1)}, bf16[3,128,512]{2,1,0:T(8,128)(2,1)S(1)}, u32[]{:S(2)}, u32[]{:S(2)}) collective-permute-start(bf16[3,128,512]{2,1,0:T(8,128)(2,1)} %bitcast.32), channel_id=1, source_target_pairs={{0,2},{2,4},{4,6},{6,0},{1,3},{3,5},{5,7},{7,1},{8,10},{10,12},{12... | collective-permute-start | bytes 1179656 | tf_op jit(solution)/shard_map/ppermute | solution.py:456
  169.8 27.5 %collective-permute-start.18 = (bf16[256,1024]{1,0:T(8,128)(2,1)}, bf16[256,1024]{1,0:T(8,128)(2,1)}, u32[]{:S(2)}, u32[]{:S(2)}) collective-permute-start(bf16[256,1024]{1,0:T(8,128)(2,1)} %get-tuple-element.46.rest_0_), channel_id=1, source_target_pairs={{0,1},{1,0},{2,3},{3,2},{4,5},{5,4},{6,7},{7,6},{8,9},{9,8},{10,11... | collective-permute-start | bytes 1572872 | tf_op jit(solution)/shard_map/ppermute | solution.py:498
  169.8 29.1 %collective-permute-start.19 = (bf16[256,1024]{1,0:T(8,128)(2,1)}, bf16[256,1024]{1,0:T(8,128)(2,1)}, u32[]{:S(2)}, u32[]{:S(2)}) collective-permute-start(bf16[256,1024]{1,0:T(8,128)(2,1)} %collective-permute-done.15.rest_2_), channel_id=1, source_target_pairs={{0,1},{1,0},{2,3},{3,2},{4,5},{5,4},{6,7},{7,6},{8,9},{9,8},{10,11... | collective-permute-start | bytes 1572872 | tf_op jit(solution)/shard_map/ppermute | solution.py:498
  183.6 11.8 %copy-start.7 = (bf16[3,128,512]{2,1,0:T(8,128)(2,1)}, bf16[3,128,512]{2,1,0:T(8,128)(2,1)S(1)}, u32[]{:S(2)}) copy-start(bf16[3,128,512]{2,1,0:T(8,128)(2,1)S(1)} %collective-permute-done.6.n3) | copy-start | bytes 1179652
  183.6 15.8 %collective-permute-start.20 = (bf16[256,1024]{1,0:T(8,128)(2,1)}, bf16[256,1024]{1,0:T(8,128)(2,1)}, u32[]{:S(2)}, u32[]{:S(2)}) collective-permute-start(bf16[256,1024]{1,0:T(8,128)(2,1)} %collective-permute-done.16.rest_4_), channel_id=1, source_target_pairs={{0,1},{1,0},{2,3},{3,2},{4,5},{5,4},{6,7},{7,6},{8,9},{9,8},{10,11... | collective-permute-start | bytes 1572872 | tf_op jit(solution)/shard_map/ppermute | solution.py:498
  183.7 0.8 copy-start.5
  183.7 11.8 %collective-permute-start.7 = (bf16[3,128,512]{2,1,0:T(8,128)(2,1)}, bf16[3,128,512]{2,1,0:T(8,128)(2,1)S(1)}, u32[]{:S(2)}, u32[]{:S(2)}) collective-permute-start(bf16[3,128,512]{2,1,0:T(8,128)(2,1)} %bitcast.33), channel_id=1, source_target_pairs={{0,6},{2,0},{4,2},{6,4},{1,7},{3,1},{5,3},{7,5},{8,14},{10,8},{12,... | collective-permute-start | bytes 1179656 | tf_op jit(solution)/shard_map/ppermute | solution.py:452
  184.4 0.8 copy-start.6
  184.4 17.7 %collective-permute-start.21 = (bf16[256,1024]{1,0:T(8,128)(2,1)}, bf16[256,1024]{1,0:T(8,128)(2,1)S(1)}, u32[]{:S(2)}, u32[]{:S(2)}) collective-permute-start(bf16[256,1024]{1,0:T(8,128)(2,1)} %collective-permute-done.17.rest_6_), channel_id=1, source_target_pairs={{0,1},{1,0},{2,3},{3,2},{4,5},{5,4},{6,7},{7,6},{8,9},{9,8},{10,11... | collective-permute-start | bytes 1572872 | tf_op jit(solution)/shard_map/ppermute | solution.py:498
  195.4 14.8 %copy-start.11 = (bf16[3,128,512]{2,1,0:T(8,128)(2,1)}, bf16[3,128,512]{2,1,0:T(8,128)(2,1)S(1)}, u32[]{:S(2)}) copy-start(bf16[3,128,512]{2,1,0:T(8,128)(2,1)S(1)} %collective-permute-done.7.n1) | copy-start | bytes 1179652
  195.5 14.7 %collective-permute-start.11 = (bf16[2,128,512]{2,1,0:T(8,128)(2,1)S(1)}, bf16[2,128,512]{2,1,0:T(8,128)(2,1)S(1)}, u32[]{:S(2)}, u32[]{:S(2)}) collective-permute-start(bf16[2,128,512]{2,1,0:T(8,128)(2,1)S(1)} %slice.14), channel_id=1, source_target_pairs={{0,2},{2,4},{4,6},{6,0},{1,3},{3,5},{5,7},{7,1},{8,10},{10,12},{12... | collective-permute-start | bytes 786440 | tf_op jit(solution)/shard_map/ppermute | solution.py:456
  197.3 7.0 %collective-permute-start.10 = (bf16[128,512]{1,0:T(8,128)(2,1)}, bf16[128,512]{1,0:T(8,128)(2,1)S(1)}, u32[]{:S(2)}, u32[]{:S(2)}) collective-permute-start(bf16[128,512]{1,0:T(8,128)(2,1)} %hidden_units.3.f0), channel_id=1, source_target_pairs={{0,6},{2,0},{4,2},{6,4},{1,7},{3,1},{5,3},{7,5},{8,14},{10,8},{12,... | collective-permute-start | bytes 393224 | tf_op jit(solution)/shard_map/ppermute | solution.py:452
  198.9 9.9 %collective-permute-start.13 = (bf16[128,512]{1,0:T(8,128)(2,1)}, bf16[128,512]{1,0:T(8,128)(2,1)S(1)}, u32[]{:S(2)}, u32[]{:S(2)}) collective-permute-start(bf16[128,512]{1,0:T(8,128)(2,1)} %hidden_units.3.f0), channel_id=1, source_target_pairs={{0,4},{2,6},{4,0},{6,2},{1,5},{3,7},{5,1},{7,3},{8,12},{10,14},{12... | collective-permute-start | bytes 393224 | tf_op jit(solution)/shard_map/ppermute | solution.py:516
  199.5 8.4 %collective-permute-start.12 = (bf16[1,128,512]{2,1,0:T(8,128)(2,1)S(1)}, bf16[1,128,512]{2,1,0:T(8,128)(2,1)S(1)}, u32[]{:S(2)}, u32[]{:S(2)}) collective-permute-start(bf16[1,128,512]{2,1,0:T(8,128)(2,1)S(1)} %slice.15), channel_id=1, source_target_pairs={{0,6},{2,0},{4,2},{6,4},{1,7},{3,1},{5,3},{7,5},{8,14},{10,8},{12,... | collective-permute-start | bytes 393224 | tf_op jit(solution)/shard_map/ppermute | solution.py:452
  202.1 8.1 %copy-start.13 = (bf16[256,1024]{1,0:T(8,128)(2,1)}, bf16[256,1024]{1,0:T(8,128)(2,1)S(1)}, u32[]{:S(2)}) copy-start(bf16[256,1024]{1,0:T(8,128)(2,1)S(1)} %collective-permute-done.21.rest_7_) | copy-start | bytes 1572868
  202.1 8.1 %collective-permute-start.14 = (bf16[128,512]{1,0:T(8,128)(2,1)}, bf16[128,512]{1,0:T(8,128)(2,1)S(1)}, u32[]{:S(2)}, u32[]{:S(2)}) collective-permute-start(bf16[128,512]{1,0:T(8,128)(2,1)} %hidden_units.3.f0), channel_id=1, source_target_pairs={{0,2},{2,4},{4,6},{6,0},{1,3},{3,5},{5,7},{7,1},{8,10},{10,12},{12... | collective-permute-start | bytes 393224 | tf_op jit(solution)/shard_map/ppermute | solution.py:456
  204.3 5.9 %copy-start.15 = (bf16[128,512]{1,0:T(8,128)(2,1)}, bf16[128,512]{1,0:T(8,128)(2,1)S(1)}, u32[]{:S(2)}) copy-start(bf16[128,512]{1,0:T(8,128)(2,1)S(1)} %collective-permute-done.10.f1) | copy-start | bytes 393220
  207.9 2.3 copy-start.17
  208.7 1.5 copy-start.16
  210.2 0.6 copy-start.18
  210.2 0.7 copy-start.14
  217.4 5.8 %copy-start.12 = (f32[256,2]{0,1:T(2,128)S(1)}, f32[256,2]{0,1:T(2,128)}, u32[]{:S(2)}) copy-start(f32[256,2]{0,1:T(2,128)} %param.21) | copy-start | bytes 6148
  217.4 36.5 %all-to-all-start.2 = ((bf16[32,16,1152]{2,1,0:T(8,128)(2,1)}), bf16[32,16,1152]{2,1,0:T(8,128)(2,1)S(1)}, u32[]{:S(2)}, u32[]{:S(2)}) async-start(bf16[32,16,1152]{2,1,0:T(8,128)(2,1)} %bitcast.30), calls=%async_computation.2 | async-start | bytes 2359296 | tf_op jit(solution)/shard_map/all_to_all | solution.py:163
  253.9 1.0 copy-start.1
  257.5 6.3 %collective-permute-start.22 = (bf16[32,1024]{1,0:T(8,128)(2,1)}, bf16[32,1024]{1,0:T(8,128)(2,1)S(1)}, u32[]{:S(2)}, u32[]{:S(2)}) collective-permute-start(bf16[32,1024]{1,0:T(8,128)(2,1)} %get-tuple-element.53), channel_id=1, source_target_pairs={{0,6},{2,0},{4,2},{6,4},{1,7},{3,1},{5,3},{7,5},{8,14},{10,8},{12,... | collective-permute-start | bytes 196616 | tf_op jit(solution)/shard_map/ppermute | solution.py:528
  257.7 6.1 %collective-permute-start.23 = (bf16[32,1024]{1,0:T(8,128)(2,1)}, bf16[32,1024]{1,0:T(8,128)(2,1)S(1)}, u32[]{:S(2)}, u32[]{:S(2)}) collective-permute-start(bf16[32,1024]{1,0:T(8,128)(2,1)} %get-tuple-element.54), channel_id=1, source_target_pairs={{0,4},{2,6},{4,0},{6,2},{1,5},{3,7},{5,1},{7,3},{8,12},{10,14},{12... | collective-permute-start | bytes 196616 | tf_op jit(solution)/shard_map/ppermute | solution.py:528
  259.1 5.7 %collective-permute-start.24 = (bf16[32,1024]{1,0:T(8,128)(2,1)}, bf16[32,1024]{1,0:T(8,128)(2,1)S(1)}, u32[]{:S(2)}, u32[]{:S(2)}) collective-permute-start(bf16[32,1024]{1,0:T(8,128)(2,1)} %get-tuple-element.55), channel_id=1, source_target_pairs={{0,2},{2,4},{4,6},{6,0},{1,3},{3,5},{5,7},{7,1},{8,10},{10,12},{12... | collective-permute-start | bytes 196616 | tf_op jit(solution)/shard_map/ppermute | solution.py:528
  263.8 1.0 copy-start.8
  263.8 1.0 copy-start.9
  264.8 0.6 copy-start.10

commit v3 on v2

--- a/solution.py
+++ b/solution.py
@@ -184,18 +184,7 @@
     return contract(wide, pick, 1, 0)[0:2].astype(jnp.int32)
 
 
-def dispatch_kernel(
-    idx_ref, rows_ref, gain_ref, pick_ref, down_ref, out_ref, slot_ref, *rest, part, experts
-):
-    cuts, sems = rest[:NY], rest[NY]
-    cut = cuts[0].shape[1]
-    copies = []
-    for i, dst in enumerate(cuts):
-        column = pl.multiple_of(((idx_ref[0] // 2 + i) % NY) * cut, cut)
-        copies.append(
-            pltpu.make_async_copy(down_ref.at[:, pl.ds(column, cut)], dst, sems.at[i])
-        )
-        copies[-1].start()
+def dispatch_kernel(idx_ref, rows_ref, gain_ref, pick_ref, out_ref, slot_ref, *, part, experts):
     total = pick_ref.shape[1]
     pick = pick_ref[...]
     first = pick[0:1]
@@ -228,11 +217,9 @@
         )
         total_out = piece if total_out is None else total_out + piece
     out_ref[...] = total_out.astype(BF16)
-    for copy in copies:
-        copy.wait()
-
-
-def dispatch(index, rows, gain, pick, down, part, experts):
+
+
+def dispatch(index, rows, gain, pick, part, experts):
     total, width = rows.shape
     return pl.pallas_call(
         functools.partial(dispatch_kernel, part=part, experts=experts),
@@ -243,22 +230,18 @@
                 pl.BlockSpec((part, width), lambda n, idx: (idx[0], 0)),
                 pl.BlockSpec((1, width), lambda n, idx: (0, 0)),
                 pl.BlockSpec((2, total), lambda n, idx: (0, 0)),
-                pl.BlockSpec(memory_space=pl.ANY),
             ],
             out_specs=[
                 pl.BlockSpec((experts * CAP * 2, width // 2), lambda n, idx: (0, 0)),
                 pl.BlockSpec((2, total), lambda n, idx: (0, 0)),
-            ]
-            + [pl.BlockSpec(memory_space=pl.ANY)] * NY,
-            scratch_shapes=[pltpu.SemaphoreType.DMA((NY,))],
+            ],
         ),
         out_shape=[
             jax.ShapeDtypeStruct((experts * CAP * 2, width // 2), BF16),
             jax.ShapeDtypeStruct((2, total), jnp.int32),
-        ]
-        + [jax.ShapeDtypeStruct((down.shape[0], down.shape[1] // NY), BF16)] * NY,
+        ],
         name="dispatch",
-    )(index, rows, gain.reshape(1, width), pick.T, down)
+    )(index, rows, gain.reshape(1, width), pick.T)
 
 
 def hidden_kernel(*refs, parts):
@@ -480,13 +463,14 @@
     swap = [(0, 1), (1, 0)]
 
     gate, up, down = gate_weight[0], up_weight[0], down_weight[0]
-    outgoing, slots, *slices = dispatch(
-        index, routed_rows, pre_gain, expert_pick, down, part, experts
-    )
+    outgoing, slots = dispatch(index, routed_rows, pre_gain, expert_pick, part, experts)
     arrived = exchange(outgoing.reshape(experts, 2 * CAP, width // 2))
 
     weights = (gate, up, lax.ppermute(gate, "c", swap), lax.ppermute(up, "c", swap))
     cut = width // NY
+    slices = [
+        lax.dynamic_slice_in_dim(down, lax.rem(y + i, NY) * cut, cut, axis=1) for i in range(NY)
+    ]
     mine = [slices[0]] + [lax.ppermute(slices[-m % NY], "y", ring(NY, -m)) for m in range(1, NY)]
     local_out, query_carry, local_state = attn_local(
         queries, key_vectors, value_vectors, decay_logit

time: 268 us -> 204 us (0.76)
  Pallas kernels: 108 us -> 44.4 us
  local copies, waits for them, and re-layouts: 5.56 us -> 8.46 us
    pallas_call x1, Pallas kernels: 66.6 us -> 3.1 us  [dispatch(): pl.pallas_call(functools.partial(dispatch_kernel, part=part, experts=expe...]
    dynamic_slice x0 -> x1, local copies, waits for them, and re-layouts: none -> 2.87 us  [on_device(): lax.dynamic_slice_in_dim(down, lax.rem(y + i, NY) * cut, cut, axis=1)]
  transfers between devices with their start and end apart: 28 -> 28, of which waited for: 14 -> 13; matrix products, arithmetic and copies ran while one was open for 1% -> 2% of each run, Pallas kernels for 11% -> 15%
where the time goes in v3:
time: 204 us
  waiting for transfers between devices  99.4 us (49%)
  starting transfers between devices  50.4 us (25%)
  Pallas kernels  44.4 us (22%)
  local copies, waits for them, and re-layouts  8.46 us (4%)
    all_to_all x3, waiting for transfers between devices, exchange(): return lax.all_to_all(x, EP, split_axis=0, concat_axis=0, tiled=True)  51 us
    all_to_all x3, starting transfers between devices, exchange(): return lax.all_to_all(x, EP, split_axis=0, concat_axis=0, tiled=True)  23.4 us
    ppermute x6, waiting for transfers between devices, from_right(): return lax.ppermute(x, 'y', ring(NY, -1))  20.5 us
    pallas_call x2, Pallas kernels, hidden_units(): pl.pallas_call(functools.partial(hidden_kernel, parts=len(xs)), grid=(ste...  15.1 us
    ppermute x6, waiting for transfers between devices, from_left(): return lax.ppermute(x, 'y', ring(NY, 1))  14.8 us
    ppermute x6, starting transfers between devices, from_right(): return lax.ppermute(x, 'y', ring(NY, -1))  12 us
    ppermute x3, waiting for transfers between devices, on_device(): lax.ppermute(slices[-m % NY], 'y', ring(NY, -m))  11.4 us
    pallas_call x1, Pallas kernels, attn_local(): pl.pallas_call(attn_local_kernel, grid=(rows // tile,), in_specs=[pl.Bloc...  9.47 us
  transfers between devices with their start and end apart: 28, of which 13 were waited for; matrix products, arithmetic and copies ran while one was open for 2% of the time, Pallas kernels for 15%

profile of v3, /device:TPU:2, one launch (start us, length us, event | category | flops | bytes accessed | tf_op | source)
XLA Modules:
  0.0 203.6 jit_solution(1823468534799165577)
XLA Ops:
  0.6 0.0 copy-start
  0.6 3.1 %dispatch.1 = (bf16[256,2048]{1,0:T(8,128)(2,1)}, s32[2,256]{1,0:T(2,128)}) custom-call(s32[1]{0:T(128)} %bitcast.idx_ref, bf16[256,4096]{1,0:T(8,128)(2,1)} %rows_ref.1, f32[1,4096]{1,0:T(1,128)} %bitcast.42, s32[2,256]{1,0:T(2,128)} %bitcast.44), custom_call_target="tpu_custom_call" | custom-call | tf_op jit(solution)/shard_map/dispatch/pallas_call | solution.py:224
  3.7 11.6 %all-to-all-start = ((bf16[32,8,2048]{2,1,0:T(8,128)(2,1)}), bf16[32,8,2048]{2,1,0:T(8,128)(2,1)S(1)}, u32[]{:S(2)}, u32[]{:S(2)}) async-start(bf16[32,8,2048]{2,1,0:T(8,128)(2,1)} %bitcast.37), calls=%async_computation | async-start | bytes 2097152 | tf_op jit(solution)/shard_map/all_to_all | solution.py:163
  15.4 0.1 collective-permute-start.4
  15.5 0.5 collective-permute-start.5
  16.0 9.5 %attn_local.1 = (f32[1024,512]{1,0:T(8,128)}, bf16[1024,256]{1,0:T(8,128)(2,1)}, bf16[32,24,128]{2,1,0:T(8,128)(2,1)}) custom-call(bf16[1024,256]{1,0:T(8,128)(2,1)} %q_ref.1, bf16[1024,256]{1,0:T(8,128)(2,1)} %k_ref.1, bf16[1024,512]{1,0:T(8,128)(2,1)} %v_ref.1, f32[1024,256]{1,0:T(8,128)} %g_ref.1), custom_call_target="tpu_custom_call" | custom-call | flops 8000000000 | bytes 6000000 | tf_op jit(solution)/shard_map/attn_local/pallas_call | solution.py:91
  25.5 18.0 %all-to-all-done = bf16[32,8,2048]{2,1,0:T(8,128)(2,1)S(1)} async-done(((bf16[32,8,2048]{2,1,0:T(8,128)(2,1)}), bf16[32,8,2048]{2,1,0:T(8,128)(2,1)S(1)}, u32[]{:S(2)}, u32[]{:S(2)}) %all-to-all-start) | async-done | bytes 1048608 | tf_op jit(solution)/shard_map/all_to_all | solution.py:163
  43.4 1.0 slice_bitcast_fusion
  44.5 3.0 %collective-permute-start = (bf16[128,2048]{1,0:T(8,128)(2,1)}, bf16[128,2048]{1,0:T(8,128)(2,1)}, u32[]{:S(2)}, u32[]{:S(2)}) collective-permute-start(bf16[128,2048]{1,0:T(8,128)(2,1)} %get-tuple-element.53.refs_0_), channel_id=1, source_target_pairs={{0,6},{2,0},{4,2},{6,4},{1,7},{3,1},{5,3},{7,5},{8,14},{10,8},{12,... | collective-permute-start | bytes 1572872 | tf_op jit(solution)/shard_map/ppermute | solution.py:435
  47.5 0.7 collective-permute-start.1
  48.2 1.3 collective-permute-start.2
  49.5 10.6 %collective-permute-done.refs_2_ = bf16[128,2048]{1,0:T(8,128)(2,1)} collective-permute-done((bf16[128,2048]{1,0:T(8,128)(2,1)}, bf16[128,2048]{1,0:T(8,128)(2,1)}, u32[]{:S(2)}, u32[]{:S(2)}) %collective-permute-start) | collective-permute-done | bytes 524320 | tf_op jit(solution)/shard_map/ppermute | solution.py:435
  60.1 1.0 collective-permute-start.3
  61.2 5.6 %all-to-all-start.1 = ((bf16[32,24,128]{2,1,0:T(8,128)(2,1)}), bf16[32,24,128]{2,1,0:T(8,128)(2,1)S(1)}, u32[]{:S(2)}, u32[]{:S(2)}) async-start(bf16[32,24,128]{2,1,0:T(8,128)(2,1)} %get-tuple-element.30), calls=%async_computation.1 | async-start | bytes 393216 | tf_op jit(solution)/shard_map/all_to_all | solution.py:163
  66.7 2.9 %dynamic-slice_bitcast_fusion = (bf16[256,1024]{1,0:T(8,128)(2,1)}, bf16[256,1024]{1,0:T(8,128)(2,1)}, bf16[256,1024]{1,0:T(8,128)(2,1)}, bf16[256,1024]{1,0:T(8,128)(2,1)}) fusion(bf16[1,256,4096]{2,1,0:T(8,128)(2,1)} %param.24, s32[]{:T(128)S(6)} %select_n.15, s32[]{:T(128)S(6)} %select_n.13, s32[]{:T(128)S(6)} %select_n.12, s32[]{:T(128)S(6)} %select_n.14), kind=kLoop, calls=%fused_computation | loop fusion | bytes 4194320 | tf_op jit(solution)/shard_map/dynamic_slice | solution.py:472
  69.6 0.0 collective-permute-done.1.refs_3_
  69.6 2.7 %collective-permute-start.15 = (bf16[256,1024]{1,0:T(8,128)(2,1)}, bf16[256,1024]{1,0:T(8,128)(2,1)}, u32[]{:S(2)}, u32[]{:S(2)}) collective-permute-start(bf16[256,1024]{1,0:T(8,128)(2,1)} %get-tuple-element.49), channel_id=1, source_target_pairs={{0,6},{2,0},{4,2},{6,4},{1,7},{3,1},{5,3},{7,5},{8,14},{10,8},{12,... | collective-permute-start | bytes 1572872 | tf_op jit(solution)/shard_map/ppermute | solution.py:474
  72.3 3.5 %all-to-all-done.1.in_ref = bf16[32,24,128]{2,1,0:T(8,128)(2,1)S(1)} async-done(((bf16[32,24,128]{2,1,0:T(8,128)(2,1)}), bf16[32,24,128]{2,1,0:T(8,128)(2,1)S(1)}, u32[]{:S(2)}, u32[]{:S(2)}) %all-to-all-start.1) | async-done | bytes 196640 | tf_op jit(solution)/shard_map/all_to_all | solution.py:163
  75.9 0.7 copy-done.2
  76.5 1.6 prefix.1
  78.2 0.0 collective-permute-done.2.refs_4_
  78.2 4.1 %collective-permute-start.16 = (bf16[256,1024]{1,0:T(8,128)(2,1)}, bf16[256,1024]{1,0:T(8,128)(2,1)}, u32[]{:S(2)}, u32[]{:S(2)}) collective-permute-start(bf16[256,1024]{1,0:T(8,128)(2,1)} %get-tuple-element.51), channel_id=1, source_target_pairs={{0,4},{2,6},{4,0},{6,2},{1,5},{3,7},{5,1},{7,3},{8,12},{10,14},{12... | collective-permute-start | bytes 1572872 | tf_op jit(solution)/shard_map/ppermute | solution.py:474
  82.3 0.0 collective-permute-done.3.refs_5_
  82.3 0.0 collective-permute-start.17
  82.3 0.0 collective-permute-done.4.refs_10_.refs_11_.refs_6_.refs_7_
  82.3 0.1 collective-permute-start.8
  82.4 0.0 collective-permute-done.5.refs_12_.refs_13_.refs_8_.refs_9_
  82.4 3.4 %collective-permute-start.9 = (bf16[128,2048]{1,0:T(8,128)(2,1)S(1)}, bf16[128,2048]{1,0:T(8,128)(2,1)S(1)}, u32[]{:S(2)}, u32[]{:S(2)}) collective-permute-start(bf16[128,2048]{1,0:T(8,128)(2,1)S(1)} %collective-permute-done.1.refs_3_), channel_id=1, source_target_pairs={{0,6},{2,0},{4,2},{6,4},{1,7},{3,1},{5,3},{7,5},{8,14},{10,8},{12,... | collective-permute-start | bytes 1572872 | tf_op jit(solution)/shard_map/ppermute | solution.py:435
  85.8 8.9 %hidden_units.2 = bf16[384,512]{1,0:T(8,128)(2,1)} custom-call(bf16[128,2048]{1,0:T(8,128)(2,1)} %get-tuple-element.53.refs_0_, bf16[128,2048]{1,0:T(8,128)(2,1)} %get-tuple-element.52.refs_1_, bf16[128,2048]{1,0:T(8,128)(2,1)} %collective-permute-done.refs_2_, bf16[128,2048]{1,0:T(8,128)(2,1)} %copy-done.3, bf16[128,2048]{1,0:T(8,128)(2,1)} %copy-done.4, ...), custom_call_target="tpu_custom_call" | custom-call | flops 3221225472 | bytes 11534336 | tf_op jit(solution)/shard_map/hidden_units/pallas_call | solution.py:294
  94.7 0.1 collective-permute-start.6
  94.8 0.6 collective-permute-done.16.rest_4_
  95.4 10.8 %collective-permute-done.17.rest_6_ = bf16[256,1024]{1,0:T(8,128)(2,1)} collective-permute-done((bf16[256,1024]{1,0:T(8,128)(2,1)}, bf16[256,1024]{1,0:T(8,128)(2,1)}, u32[]{:S(2)}, u32[]{:S(2)}) %collective-permute-start.17) | collective-permute-done | bytes 524320 | tf_op jit(solution)/shard_map/ppermute | solution.py:474
  106.2 0.5 collective-permute-start.19
  106.7 13.3 %collective-permute-done.6.n3 = bf16[3,128,512]{2,1,0:T(8,128)(2,1)S(1)} collective-permute-done((bf16[3,128,512]{2,1,0:T(8,128)(2,1)}, bf16[3,128,512]{2,1,0:T(8,128)(2,1)S(1)}, u32[]{:S(2)}, u32[]{:S(2)}) %collective-permute-start.6) | collective-permute-done | bytes 393248 | tf_op jit(solution)/shard_map/ppermute | solution.py:439
  120.0 0.0 copy-start.5
  120.0 0.7 collective-permute-start.7
  120.7 0.1 collective-permute-start.21
  120.9 0.7 copy-done.6
  121.5 6.2 %hidden_units.3.f0 = bf16[128,512]{1,0:T(8,128)(2,1)} custom-call(bf16[128,2048]{1,0:T(8,128)(2,1)} %copy-done.5, bf16[128,2048]{1,0:T(8,128)(2,1)} %copy-done.6, bf16[4096,256]{1,0:T(8,128)(2,1)} %bitcast.26, bf16[4096,256]{1,0:T(8,128)(2,1)} %bitcast.27, bf16[4096,256]{1,0:T(8,128)(2,1)} %bitcast.32, bf16[4096,256]{1,0:T(8,128)(2,1)} %bitcast.33, ...), custom_call_target="tpu_custom_call" | custom-call | flops 1073741824 | bytes 9437184 | tf_op jit(solution)/shard_map/hidden_units/pallas_call | solution.py:294
  127.7 4.1 %collective-permute-done.7.n1 = bf16[3,128,512]{2,1,0:T(8,128)(2,1)S(1)} collective-permute-done((bf16[3,128,512]{2,1,0:T(8,128)(2,1)}, bf16[3,128,512]{2,1,0:T(8,128)(2,1)S(1)}, u32[]{:S(2)}, u32[]{:S(2)}) %collective-permute-start.7) | collective-permute-done | bytes 393248 | tf_op jit(solution)/shard_map/ppermute | solution.py:435
  131.8 1.8 collective-permute-start.11
  133.7 1.6 collective-permute-start.10
  135.2 0.6 collective-permute-start.13
  135.8 2.6 %collective-permute-start.12 = (bf16[1,128,512]{2,1,0:T(8,128)(2,1)S(1)}, bf16[1,128,512]{2,1,0:T(8,128)(2,1)S(1)}, u32[]{:S(2)}, u32[]{:S(2)}) collective-permute-start(bf16[1,128,512]{2,1,0:T(8,128)(2,1)S(1)} %slice.15), channel_id=1, source_target_pairs={{0,6},{2,0},{4,2},{6,4},{1,7},{3,1},{5,3},{7,5},{8,14},{10,8},{12,... | collective-permute-start | bytes 393224 | tf_op jit(solution)/shard_map/ppermute | solution.py:435
  138.5 2.2 %collective-permute-done.10.f1 = bf16[128,512]{1,0:T(8,128)(2,1)S(1)} collective-permute-done((bf16[128,512]{1,0:T(8,128)(2,1)}, bf16[128,512]{1,0:T(8,128)(2,1)S(1)}, u32[]{:S(2)}, u32[]{:S(2)}) %collective-permute-start.10) | collective-permute-done | bytes 131104 | tf_op jit(solution)/shard_map/ppermute | solution.py:435
  140.7 3.6 %collective-permute-done.12.n2b = bf16[1,128,512]{2,1,0:T(8,128)(2,1)S(1)} collective-permute-done((bf16[1,128,512]{2,1,0:T(8,128)(2,1)S(1)}, bf16[1,128,512]{2,1,0:T(8,128)(2,1)S(1)}, u32[]{:S(2)}, u32[]{:S(2)}) %collective-permute-start.12) | collective-permute-done | bytes 131104 | tf_op jit(solution)/shard_map/ppermute | solution.py:435
  144.3 0.8 collective-permute-done.13.f2
  145.1 1.4 collective-permute-done.14.f3
  146.6 0.6 copy-done.18
  147.2 0.1 copy-done.14
  147.3 6.4 %expert_down.1 = bf16[512,1152]{1,0:T(8,128)(2,1)} custom-call(bf16[3,128,512]{2,1,0:T(8,128)(2,1)} %bitcast.40, bf16[128,512]{1,0:T(8,128)(2,1)} %hidden_units.3.f0, bf16[3,128,512]{2,1,0:T(8,128)(2,1)} %copy-done.11, bf16[128,512]{1,0:T(8,128)(2,1)} %copy-done.15, bf16[2,128,512]{2,1,0:T(8,128)(2,1)} %copy-done.14, bf16[1,128,512]{2,1,0:T(8,128)(2,1)} %copy-done.17, ...), custom_call_target="tpu_custom_call" | custom-call | flops 2415919104 | bytes 8000000 | tf_op jit(solution)/shard_map/expert_down/pallas_call | solution.py:348
  153.7 0.0 copy-start.12
  153.8 6.2 %all-to-all-start.2 = ((bf16[32,16,1152]{2,1,0:T(8,128)(2,1)}), bf16[32,16,1152]{2,1,0:T(8,128)(2,1)S(1)}, u32[]{:S(2)}, u32[]{:S(2)}) async-start(bf16[32,16,1152]{2,1,0:T(8,128)(2,1)} %bitcast.36), calls=%async_computation.2 | async-start | bytes 2359296 | tf_op jit(solution)/shard_map/all_to_all | solution.py:163
  160.0 0.8 copy.15.weight_ref
  160.8 29.5 %all-to-all-done.2 = bf16[32,16,1152]{2,1,0:T(8,128)(2,1)S(1)} async-done(((bf16[32,16,1152]{2,1,0:T(8,128)(2,1)}), bf16[32,16,1152]{2,1,0:T(8,128)(2,1)S(1)}, u32[]{:S(2)}, u32[]{:S(2)}) %all-to-all-start.2) | async-done | bytes 1179680 | tf_op jit(solution)/shard_map/all_to_all | solution.py:163
  190.3 1.0 copy-done.1
  191.3 2.5 %combine.1 = (bf16[32,1024]{1,0:T(8,128)(2,1)}, bf16[32,1024]{1,0:T(8,128)(2,1)}, bf16[32,1024]{1,0:T(8,128)(2,1)}, bf16[32,1024]{1,0:T(8,128)(2,1)}) custom-call(s32[1]{0:T(128)} %bitcast.idx_ref, bf16[512,1152]{1,0:T(8,128)(2,1)} %bitcast.34, s32[2,256]{1,0:T(2,128)} %get-tuple-element.43.slot_ref, f32[256,2]{1,0:T(8,128)} %copy.15.weight_ref), custom_call_target="tpu_custom_call" | custom-call | tf_op jit(solution)/shard_map/combine/pallas_call | solution.py:389
  193.8 0.3 collective-permute-start.22
  194.1 1.3 collective-permute-start.23
  195.4 0.4 collective-permute-start.24
  195.9 4.3 %attn_out.1 = bf16[1024,512]{1,0:T(8,128)(2,1)} custom-call(f32[1024,512]{1,0:T(8,128)} %get-tuple-element.25.o_ref, bf16[1024,256]{1,0:T(8,128)(2,1)} %get-tuple-element.26.qc_ref, bf16[512,1152]{1,0:T(8,128)(2,1)} %bitcast.35, f32[1,256]{1,0:T(1,128)} %bitcast.45), custom_call_target="tpu_custom_call" | custom-call | flops 3000000000 | bytes 4000000 | tf_op jit(solution)/shard_map/attn_out/pallas_call | solution.py:135
  200.2 0.9 collective-permute-done.24.p3
  201.1 0.6 copy-done.10
  201.7 1.8 finish.1
  (44 shorter events, 0.1 us)
Async XLA Ops:
  0.6 14.7 %copy-start = (bf16[1,4096,256]{2,1,0:T(8,128)(2,1)S(1)}, bf16[1,4096,256]{2,1,0:T(8,128)(2,1)}, u32[]{:S(2)}) copy-start(bf16[1,4096,256]{2,1,0:T(8,128)(2,1)} %param.22) | copy-start | bytes 6291460
  3.7 39.7 %all-to-all-start = ((bf16[32,8,2048]{2,1,0:T(8,128)(2,1)}), bf16[32,8,2048]{2,1,0:T(8,128)(2,1)S(1)}, u32[]{:S(2)}, u32[]{:S(2)}) async-start(bf16[32,8,2048]{2,1,0:T(8,128)(2,1)} %bitcast.37), calls=%async_computation | async-start | bytes 2097152 | tf_op jit(solution)/shard_map/all_to_all | solution.py:163
  15.4 66.9 %collective-permute-start.4 = (bf16[4096,256]{1,0:T(8,128)(2,1)S(1)}, bf16[4096,256]{1,0:T(8,128)(2,1)}, u32[]{:S(2)}, u32[]{:S(2)}) collective-permute-start(bf16[4096,256]{1,0:T(8,128)(2,1)S(1)} %bitcast.28), channel_id=1, source_target_pairs={{0,1},{1,0},{2,3},{3,2},{4,5},{5,4},{6,7},{7,6},{8,9},{9,8},{10,11... | collective-permute-start | bytes 6291464 | tf_op jit(solution)/shard_map/ppermute | solution.py:469
  15.5 66.9 %collective-permute-start.5 = (bf16[4096,256]{1,0:T(8,128)(2,1)}, bf16[4096,256]{1,0:T(8,128)(2,1)}, u32[]{:S(2)}, u32[]{:S(2)}) collective-permute-start(bf16[4096,256]{1,0:T(8,128)(2,1)} %bitcast.29), channel_id=1, source_target_pairs={{0,1},{1,0},{2,3},{3,2},{4,5},{5,4},{6,7},{7,6},{8,9},{9,8},{10,11... | collective-permute-start | bytes 6291464 | tf_op jit(solution)/shard_map/ppermute | solution.py:469
  44.5 15.6 %collective-permute-start = (bf16[128,2048]{1,0:T(8,128)(2,1)}, bf16[128,2048]{1,0:T(8,128)(2,1)}, u32[]{:S(2)}, u32[]{:S(2)}) collective-permute-start(bf16[128,2048]{1,0:T(8,128)(2,1)} %get-tuple-element.53.refs_0_), channel_id=1, source_target_pairs={{0,6},{2,0},{4,2},{6,4},{1,7},{3,1},{5,3},{7,5},{8,14},{10,8},{12,... | collective-permute-start | bytes 1572872 | tf_op jit(solution)/shard_map/ppermute | solution.py:435
  47.5 22.1 %collective-permute-start.1 = (bf16[128,2048]{1,0:T(8,128)(2,1)}, bf16[128,2048]{1,0:T(8,128)(2,1)S(1)}, u32[]{:S(2)}, u32[]{:S(2)}) collective-permute-start(bf16[128,2048]{1,0:T(8,128)(2,1)} %get-tuple-element.52.refs_1_), channel_id=1, source_target_pairs={{0,6},{2,0},{4,2},{6,4},{1,7},{3,1},{5,3},{7,5},{8,14},{10,8},{12,... | collective-permute-start | bytes 1572872 | tf_op jit(solution)/shard_map/ppermute | solution.py:435
  48.2 29.9 %collective-permute-start.2 = (bf16[128,2048]{1,0:T(8,128)(2,1)}, bf16[128,2048]{1,0:T(8,128)(2,1)S(1)}, u32[]{:S(2)}, u32[]{:S(2)}) collective-permute-start(bf16[128,2048]{1,0:T(8,128)(2,1)} %get-tuple-element.53.refs_0_), channel_id=1, source_target_pairs={{0,2},{2,4},{4,6},{6,0},{1,3},{3,5},{5,7},{7,1},{8,10},{10,12},{12... | collective-permute-start | bytes 1572872 | tf_op jit(solution)/shard_map/ppermute | solution.py:439
  60.1 22.2 %collective-permute-start.3 = (bf16[128,2048]{1,0:T(8,128)(2,1)}, bf16[128,2048]{1,0:T(8,128)(2,1)}, u32[]{:S(2)}, u32[]{:S(2)}) collective-permute-start(bf16[128,2048]{1,0:T(8,128)(2,1)} %get-tuple-element.52.refs_1_), channel_id=1, source_target_pairs={{0,2},{2,4},{4,6},{6,0},{1,3},{3,5},{5,7},{7,1},{8,10},{10,12},{12... | collective-permute-start | bytes 1572872 | tf_op jit(solution)/shard_map/ppermute | solution.py:439
  61.2 14.7 %all-to-all-start.1 = ((bf16[32,24,128]{2,1,0:T(8,128)(2,1)}), bf16[32,24,128]{2,1,0:T(8,128)(2,1)S(1)}, u32[]{:S(2)}, u32[]{:S(2)}) async-start(bf16[32,24,128]{2,1,0:T(8,128)(2,1)} %get-tuple-element.30), calls=%async_computation.1 | async-start | bytes 393216 | tf_op jit(solution)/shard_map/all_to_all | solution.py:163
  69.6 16.2 %copy-start.3 = (bf16[128,2048]{1,0:T(8,128)(2,1)}, bf16[128,2048]{1,0:T(8,128)(2,1)S(1)}, u32[]{:S(2)}) copy-start(bf16[128,2048]{1,0:T(8,128)(2,1)S(1)} %collective-permute-done.1.refs_3_) | copy-start | bytes 1572868
  69.6 25.1 %collective-permute-start.15 = (bf16[256,1024]{1,0:T(8,128)(2,1)}, bf16[256,1024]{1,0:T(8,128)(2,1)}, u32[]{:S(2)}, u32[]{:S(2)}) collective-permute-start(bf16[256,1024]{1,0:T(8,128)(2,1)} %get-tuple-element.49), channel_id=1, source_target_pairs={{0,6},{2,0},{4,2},{6,4},{1,7},{3,1},{5,3},{7,5},{8,14},{10,8},{12,... | collective-permute-start | bytes 1572872 | tf_op jit(solution)/shard_map/ppermute | solution.py:474
  75.9 0.7 copy-start.2
  78.2 7.6 %copy-start.4 = (bf16[128,2048]{1,0:T(8,128)(2,1)}, bf16[128,2048]{1,0:T(8,128)(2,1)S(1)}, u32[]{:S(2)}) copy-start(bf16[128,2048]{1,0:T(8,128)(2,1)S(1)} %collective-permute-done.2.refs_4_) | copy-start | bytes 1572868
  78.2 17.2 %collective-permute-start.16 = (bf16[256,1024]{1,0:T(8,128)(2,1)}, bf16[256,1024]{1,0:T(8,128)(2,1)}, u32[]{:S(2)}, u32[]{:S(2)}) collective-permute-start(bf16[256,1024]{1,0:T(8,128)(2,1)} %get-tuple-element.51), channel_id=1, source_target_pairs={{0,4},{2,6},{4,0},{6,2},{1,5},{3,7},{5,1},{7,3},{8,12},{10,14},{12... | collective-permute-start | bytes 1572872 | tf_op jit(solution)/shard_map/ppermute | solution.py:474
  82.3 23.9 %collective-permute-start.17 = (bf16[256,1024]{1,0:T(8,128)(2,1)}, bf16[256,1024]{1,0:T(8,128)(2,1)}, u32[]{:S(2)}, u32[]{:S(2)}) collective-permute-start(bf16[256,1024]{1,0:T(8,128)(2,1)} %get-tuple-element.48), channel_id=1, source_target_pairs={{0,2},{2,4},{4,6},{6,0},{1,3},{3,5},{5,7},{7,1},{8,10},{10,12},{12... | collective-permute-start | bytes 1572872 | tf_op jit(solution)/shard_map/ppermute | solution.py:474
  82.3 37.7 %collective-permute-start.8 = (bf16[128,2048]{1,0:T(8,128)(2,1)S(1)}, bf16[128,2048]{1,0:T(8,128)(2,1)S(1)}, u32[]{:S(2)}, u32[]{:S(2)}) collective-permute-start(bf16[128,2048]{1,0:T(8,128)(2,1)S(1)} %collective-permute-done.2.refs_4_), channel_id=1, source_target_pairs={{0,2},{2,4},{4,6},{6,0},{1,3},{3,5},{5,7},{7,1},{8,10},{10,12},{12... | collective-permute-start | bytes 1572872 | tf_op jit(solution)/shard_map/ppermute | solution.py:439
  82.4 38.3 %collective-permute-start.9 = (bf16[128,2048]{1,0:T(8,128)(2,1)S(1)}, bf16[128,2048]{1,0:T(8,128)(2,1)S(1)}, u32[]{:S(2)}, u32[]{:S(2)}) collective-permute-start(bf16[128,2048]{1,0:T(8,128)(2,1)S(1)} %collective-permute-done.1.refs_3_), channel_id=1, source_target_pairs={{0,6},{2,0},{4,2},{6,4},{1,7},{3,1},{5,3},{7,5},{8,14},{10,8},{12,... | collective-permute-start | bytes 1572872 | tf_op jit(solution)/shard_map/ppermute | solution.py:435
  94.7 25.3 %collective-permute-start.6 = (bf16[3,128,512]{2,1,0:T(8,128)(2,1)}, bf16[3,128,512]{2,1,0:T(8,128)(2,1)S(1)}, u32[]{:S(2)}, u32[]{:S(2)}) collective-permute-start(bf16[3,128,512]{2,1,0:T(8,128)(2,1)} %bitcast.38), channel_id=1, source_target_pairs={{0,2},{2,4},{4,6},{6,0},{1,3},{3,5},{5,7},{7,1},{8,10},{10,12},{12... | collective-permute-start | bytes 1179656 | tf_op jit(solution)/shard_map/ppermute | solution.py:439
  106.2 27.5 %collective-permute-start.18 = (bf16[256,1024]{1,0:T(8,128)(2,1)}, bf16[256,1024]{1,0:T(8,128)(2,1)}, u32[]{:S(2)}, u32[]{:S(2)}) collective-permute-start(bf16[256,1024]{1,0:T(8,128)(2,1)} %get-tuple-element.38.rest_0_), channel_id=1, source_target_pairs={{0,1},{1,0},{2,3},{3,2},{4,5},{5,4},{6,7},{7,6},{8,9},{9,8},{10,11... | collective-permute-start | bytes 1572872 | tf_op jit(solution)/shard_map/ppermute | solution.py:482
  106.2 29.1 %collective-permute-start.19 = (bf16[256,1024]{1,0:T(8,128)(2,1)}, bf16[256,1024]{1,0:T(8,128)(2,1)}, u32[]{:S(2)}, u32[]{:S(2)}) collective-permute-start(bf16[256,1024]{1,0:T(8,128)(2,1)} %collective-permute-done.15.rest_2_), channel_id=1, source_target_pairs={{0,1},{1,0},{2,3},{3,2},{4,5},{5,4},{6,7},{7,6},{8,9},{9,8},{10,11... | collective-permute-start | bytes 1572872 | tf_op jit(solution)/shard_map/ppermute | solution.py:482
  120.0 11.8 %copy-start.7 = (bf16[3,128,512]{2,1,0:T(8,128)(2,1)}, bf16[3,128,512]{2,1,0:T(8,128)(2,1)S(1)}, u32[]{:S(2)}) copy-start(bf16[3,128,512]{2,1,0:T(8,128)(2,1)S(1)} %collective-permute-done.6.n3) | copy-start | bytes 1179652
  120.0 15.8 %collective-permute-start.20 = (bf16[256,1024]{1,0:T(8,128)(2,1)}, bf16[256,1024]{1,0:T(8,128)(2,1)}, u32[]{:S(2)}, u32[]{:S(2)}) collective-permute-start(bf16[256,1024]{1,0:T(8,128)(2,1)} %collective-permute-done.16.rest_4_), channel_id=1, source_target_pairs={{0,1},{1,0},{2,3},{3,2},{4,5},{5,4},{6,7},{7,6},{8,9},{9,8},{10,11... | collective-permute-start | bytes 1572872 | tf_op jit(solution)/shard_map/ppermute | solution.py:482
  120.0 0.8 copy-start.5
  120.0 11.8 %collective-permute-start.7 = (bf16[3,128,512]{2,1,0:T(8,128)(2,1)}, bf16[3,128,512]{2,1,0:T(8,128)(2,1)S(1)}, u32[]{:S(2)}, u32[]{:S(2)}) collective-permute-start(bf16[3,128,512]{2,1,0:T(8,128)(2,1)} %bitcast.39), channel_id=1, source_target_pairs={{0,6},{2,0},{4,2},{6,4},{1,7},{3,1},{5,3},{7,5},{8,14},{10,8},{12,... | collective-permute-start | bytes 1179656 | tf_op jit(solution)/shard_map/ppermute | solution.py:435
  120.7 0.8 copy-start.6
  120.7 17.7 %collective-permute-start.21 = (bf16[256,1024]{1,0:T(8,128)(2,1)}, bf16[256,1024]{1,0:T(8,128)(2,1)S(1)}, u32[]{:S(2)}, u32[]{:S(2)}) collective-permute-start(bf16[256,1024]{1,0:T(8,128)(2,1)} %collective-permute-done.17.rest_6_), channel_id=1, source_target_pairs={{0,1},{1,0},{2,3},{3,2},{4,5},{5,4},{6,7},{7,6},{8,9},{9,8},{10,11... | collective-permute-start | bytes 1572872 | tf_op jit(solution)/shard_map/ppermute | solution.py:482
  131.8 14.8 %copy-start.11 = (bf16[3,128,512]{2,1,0:T(8,128)(2,1)}, bf16[3,128,512]{2,1,0:T(8,128)(2,1)S(1)}, u32[]{:S(2)}) copy-start(bf16[3,128,512]{2,1,0:T(8,128)(2,1)S(1)} %collective-permute-done.7.n1) | copy-start | bytes 1179652
  131.8 14.7 %collective-permute-start.11 = (bf16[2,128,512]{2,1,0:T(8,128)(2,1)S(1)}, bf16[2,128,512]{2,1,0:T(8,128)(2,1)S(1)}, u32[]{:S(2)}, u32[]{:S(2)}) collective-permute-start(bf16[2,128,512]{2,1,0:T(8,128)(2,1)S(1)} %slice.14), channel_id=1, source_target_pairs={{0,2},{2,4},{4,6},{6,0},{1,3},{3,5},{5,7},{7,1},{8,10},{10,12},{12... | collective-permute-start | bytes 786440 | tf_op jit(solution)/shard_map/ppermute | solution.py:439
  133.7 7.0 %collective-permute-start.10 = (bf16[128,512]{1,0:T(8,128)(2,1)}, bf16[128,512]{1,0:T(8,128)(2,1)S(1)}, u32[]{:S(2)}, u32[]{:S(2)}) collective-permute-start(bf16[128,512]{1,0:T(8,128)(2,1)} %hidden_units.3.f0), channel_id=1, source_target_pairs={{0,6},{2,0},{4,2},{6,4},{1,7},{3,1},{5,3},{7,5},{8,14},{10,8},{12,... | collective-permute-start | bytes 393224 | tf_op jit(solution)/shard_map/ppermute | solution.py:435
  135.2 9.9 %collective-permute-start.13 = (bf16[128,512]{1,0:T(8,128)(2,1)}, bf16[128,512]{1,0:T(8,128)(2,1)S(1)}, u32[]{:S(2)}, u32[]{:S(2)}) collective-permute-start(bf16[128,512]{1,0:T(8,128)(2,1)} %hidden_units.3.f0), channel_id=1, source_target_pairs={{0,4},{2,6},{4,0},{6,2},{1,5},{3,7},{5,1},{7,3},{8,12},{10,14},{12... | collective-permute-start | bytes 393224 | tf_op jit(solution)/shard_map/ppermute | solution.py:500
  135.8 8.4 %collective-permute-start.12 = (bf16[1,128,512]{2,1,0:T(8,128)(2,1)S(1)}, bf16[1,128,512]{2,1,0:T(8,128)(2,1)S(1)}, u32[]{:S(2)}, u32[]{:S(2)}) collective-permute-start(bf16[1,128,512]{2,1,0:T(8,128)(2,1)S(1)} %slice.15), channel_id=1, source_target_pairs={{0,6},{2,0},{4,2},{6,4},{1,7},{3,1},{5,3},{7,5},{8,14},{10,8},{12,... | collective-permute-start | bytes 393224 | tf_op jit(solution)/shard_map/ppermute | solution.py:435
  138.5 8.1 %copy-start.13 = (bf16[256,1024]{1,0:T(8,128)(2,1)}, bf16[256,1024]{1,0:T(8,128)(2,1)S(1)}, u32[]{:S(2)}) copy-start(bf16[256,1024]{1,0:T(8,128)(2,1)S(1)} %collective-permute-done.21.rest_7_) | copy-start | bytes 1572868
  138.5 8.1 %collective-permute-start.14 = (bf16[128,512]{1,0:T(8,128)(2,1)}, bf16[128,512]{1,0:T(8,128)(2,1)S(1)}, u32[]{:S(2)}, u32[]{:S(2)}) collective-permute-start(bf16[128,512]{1,0:T(8,128)(2,1)} %hidden_units.3.f0), channel_id=1, source_target_pairs={{0,2},{2,4},{4,6},{6,0},{1,3},{3,5},{5,7},{7,1},{8,10},{10,12},{12... | collective-permute-start | bytes 393224 | tf_op jit(solution)/shard_map/ppermute | solution.py:439
  140.7 5.9 %copy-start.15 = (bf16[128,512]{1,0:T(8,128)(2,1)}, bf16[128,512]{1,0:T(8,128)(2,1)S(1)}, u32[]{:S(2)}) copy-start(bf16[128,512]{1,0:T(8,128)(2,1)S(1)} %collective-permute-done.10.f1) | copy-start | bytes 393220
  144.3 2.3 %copy-start.17 = (bf16[1,128,512]{2,1,0:T(8,128)(2,1)}, bf16[1,128,512]{2,1,0:T(8,128)(2,1)S(1)}, u32[]{:S(2)}) copy-start(bf16[1,128,512]{2,1,0:T(8,128)(2,1)S(1)} %collective-permute-done.12.n2b) | copy-start | bytes 393220
  145.1 1.5 copy-start.16
  146.5 0.6 copy-start.18
  146.5 0.7 copy-start.14
  153.7 6.2 %copy-start.12 = (f32[256,2]{0,1:T(2,128)S(1)}, f32[256,2]{0,1:T(2,128)}, u32[]{:S(2)}) copy-start(f32[256,2]{0,1:T(2,128)} %param.21) | copy-start | bytes 6148
  153.8 36.5 %all-to-all-start.2 = ((bf16[32,16,1152]{2,1,0:T(8,128)(2,1)}), bf16[32,16,1152]{2,1,0:T(8,128)(2,1)S(1)}, u32[]{:S(2)}, u32[]{:S(2)}) async-start(bf16[32,16,1152]{2,1,0:T(8,128)(2,1)} %bitcast.36), calls=%async_computation.2 | async-start | bytes 2359296 | tf_op jit(solution)/shard_map/all_to_all | solution.py:163
  190.3 1.0 copy-start.1
  193.8 6.3 %collective-permute-start.22 = (bf16[32,1024]{1,0:T(8,128)(2,1)}, bf16[32,1024]{1,0:T(8,128)(2,1)S(1)}, u32[]{:S(2)}, u32[]{:S(2)}) collective-permute-start(bf16[32,1024]{1,0:T(8,128)(2,1)} %get-tuple-element.45), channel_id=1, source_target_pairs={{0,6},{2,0},{4,2},{6,4},{1,7},{3,1},{5,3},{7,5},{8,14},{10,8},{12,... | collective-permute-start | bytes 196616 | tf_op jit(solution)/shard_map/ppermute | solution.py:512
  194.1 6.0 %collective-permute-start.23 = (bf16[32,1024]{1,0:T(8,128)(2,1)}, bf16[32,1024]{1,0:T(8,128)(2,1)S(1)}, u32[]{:S(2)}, u32[]{:S(2)}) collective-permute-start(bf16[32,1024]{1,0:T(8,128)(2,1)} %get-tuple-element.46), channel_id=1, source_target_pairs={{0,4},{2,6},{4,0},{6,2},{1,5},{3,7},{5,1},{7,3},{8,12},{10,14},{12... | collective-permute-start | bytes 196616 | tf_op jit(solution)/shard_map/ppermute | solution.py:512
  195.4 5.7 %collective-permute-start.24 = (bf16[32,1024]{1,0:T(8,128)(2,1)}, bf16[32,1024]{1,0:T(8,128)(2,1)S(1)}, u32[]{:S(2)}, u32[]{:S(2)}) collective-permute-start(bf16[32,1024]{1,0:T(8,128)(2,1)} %get-tuple-element.47), channel_id=1, source_target_pairs={{0,2},{2,4},{4,6},{6,0},{1,3},{3,5},{5,7},{7,1},{8,10},{10,12},{12... | collective-permute-start | bytes 196616 | tf_op jit(solution)/shard_map/ppermute | solution.py:512
  200.1 1.0 copy-start.8
  200.2 1.0 copy-start.9
  201.1 0.6 copy-start.10

commit v4 on v3

--- a/solution.py
+++ b/solution.py
@@ -184,7 +184,9 @@
     return contract(wide, pick, 1, 0)[0:2].astype(jnp.int32)
 
 
-def dispatch_kernel(idx_ref, rows_ref, gain_ref, pick_ref, out_ref, slot_ref, *, part, experts):
+def dispatch_kernel(
+    idx_ref, rows_ref, gain_ref, pick_ref, first_ref, second_ref, slot_ref, *, part, experts
+):
     total = pick_ref.shape[1]
     pick = pick_ref[...]
     first = pick[0:1]
@@ -205,18 +207,19 @@
     mean = jnp.mean(values * values, axis=-1, keepdims=True)
     normed = (values * lax.rsqrt(mean + 1e-06) * gain_ref[...]).astype(BF16)
     own = own_columns(slots, [idx_ref[0] * part], part)
-    place = lax.broadcasted_iota(jnp.int32, (out_ref.shape[0], part), 0)
+    place = lax.broadcasted_iota(jnp.int32, (first_ref.shape[0], part), 0)
     target = (place // (2 * CAP)) * CAP + place % CAP
     chosen = (own[0:1] == target) | (own[1:2] == target)
-    half = out_ref.shape[1]
-    total_out = None
-    for h in range(2):
-        mine = chosen & (place // CAP % 2 == h)
-        piece = contract(
-            jnp.where(mine, 1.0, 0.0).astype(BF16), normed[:, h * half : (h + 1) * half], 1, 0
+    quarter = first_ref.shape[1]
+    masks = [
+        jnp.where(chosen & (place // CAP % 2 == h), 1.0, 0.0).astype(BF16) for h in range(2)
+    ]
+    for i, out_ref in enumerate((first_ref, second_ref)):
+        start = 2 * i * quarter
+        piece = contract(masks[0], normed[:, start : start + quarter], 1, 0) + contract(
+            masks[1], normed[:, start + quarter : start + 2 * quarter], 1, 0
         )
-        total_out = piece if total_out is None else total_out + piece
-    out_ref[...] = total_out.astype(BF16)
+        out_ref[...] = piece.astype(BF16)
 
 
 def dispatch(index, rows, gain, pick, part, experts):
@@ -232,44 +235,63 @@
                 pl.BlockSpec((2, total), lambda n, idx: (0, 0)),
             ],
             out_specs=[
-                pl.BlockSpec((experts * CAP * 2, width // 2), lambda n, idx: (0, 0)),
+                pl.BlockSpec((experts * CAP * 2, width // 4), lambda n, idx: (0, 0)),
+                pl.BlockSpec((experts * CAP * 2, width // 4), lambda n, idx: (0, 0)),
                 pl.BlockSpec((2, total), lambda n, idx: (0, 0)),
             ],
         ),
         out_shape=[
-            jax.ShapeDtypeStruct((experts * CAP * 2, width // 2), BF16),
+            jax.ShapeDtypeStruct((experts * CAP * 2, width // 4), BF16),
+            jax.ShapeDtypeStruct((experts * CAP * 2, width // 4), BF16),
             jax.ShapeDtypeStruct((2, total), jnp.int32),
         ],
         name="dispatch",
     )(index, rows, gain.reshape(1, width), pick.T)
 
 
-def hidden_kernel(*refs, parts):
-    xs = refs[:parts]
-    weights = refs[parts : parts + 8]
-    out_ref = refs[parts + 8]
-    acc = refs[parts + 9]
-    step = pl.program_id(0)
+def two_quarters(xs):
     rows = xs[0].shape[0]
     new = lax.broadcasted_iota(jnp.int32, (rows // 2, rows), 0)
     old = lax.broadcasted_iota(jnp.int32, (rows // 2, rows), 1)
     spread = (new // CAP) * (2 * CAP) + new % CAP
-    x = []
+    out = []
     for h in range(2):
         order = jnp.where(old == spread + h * CAP, 1.0, 0.0).astype(BF16)
-        x.append(
+        out.append(
             jnp.concatenate([contract(order, r[...], 1, 0).astype(BF16) for r in xs], axis=0)
         )
-
-    @pl.when(step == 0)
-    def _():
-        acc[...] = jnp.zeros_like(acc)
-
+    return out
+
+
+def add_products(acc, xs, weights):
+    x = two_quarters(xs)
     width = weights[0].shape[1]
     for j in range(4):
         acc[:, j * width : (j + 1) * width] += contract(x[0], weights[2 * j][...], 1, 0) + contract(
             x[1], weights[2 * j + 1][...], 1, 0
         )
+
+
+def first_half_kernel(*refs, parts):
+    acc = refs[parts + 8]
+
+    @pl.when(pl.program_id(0) == 0)
+    def _():
+        acc[...] = jnp.zeros_like(acc)
+
+    add_products(acc, refs[:parts], refs[parts : parts + 8])
+
+
+def hidden_kernel(*refs, parts):
+    start_ref, out_ref, acc = refs[parts + 8 : parts + 11]
+    step = pl.program_id(0)
+
+    @pl.when(step == 0)
+    def _():
+        acc[...] = start_ref[...]
+
+    add_products(acc, refs[:parts], refs[parts : parts + 8])
+    width = out_ref.shape[1] // 2
 
     @pl.when(step == pl.num_programs(0) - 1)
     def _():
@@ -280,32 +302,60 @@
             out_ref[:, j * width : (j + 1) * width] = value.astype(BF16)
 
 
-def hidden_units(xs, weights, ktile=512):
+def half_specs(xs, weights, half, ktile):
+    steps = xs[0].shape[1] // ktile
+    specs = [pl.BlockSpec((x.shape[0], ktile), lambda n: (0, n)) for x in xs]
+    doubled = []
+    for w in weights:
+        for quarter in (2 * half, 2 * half + 1):
+            doubled.append(w)
+            specs.append(
+                pl.BlockSpec(
+                    (ktile, w.shape[1]), lambda n, quarter=quarter: (n + quarter * steps, 0)
+                )
+            )
+    return steps, specs, doubled
+
+
+def half_cost(rows, weights, width):
+    return pl.CostEstimate(
+        flops=4 * rows * weights[0].shape[0] * width,
+        transcendentals=rows * width,
+        bytes_accessed=4 * weights[0].shape[0] * weights[0].shape[1] + 6 * rows * width,
+    )
+
+
+def first_half(xs, weights, ktile=256):
     rows = sum(x.shape[0] for x in xs) // 2
-    depth, width = weights[0].shape
-    steps = depth // 2 // ktile
-    specs, doubled = [], []
-    for w in weights:
-        doubled += [w, w]
-        specs += [
-            pl.BlockSpec((ktile, width), lambda n: (n, 0)),
-            pl.BlockSpec((ktile, width), lambda n: (n + steps, 0)),
-        ]
+    width = 4 * weights[0].shape[1]
+    steps, specs, doubled = half_specs(xs, weights, 0, ktile)
+    return pl.pallas_call(
+        functools.partial(first_half_kernel, parts=len(xs)),
+        grid=(steps,),
+        in_specs=specs,
+        out_specs=pl.BlockSpec((rows, width), lambda n: (0, 0)),
+        out_shape=jax.ShapeDtypeStruct((rows, width), F32),
+        compiler_params=pltpu.CompilerParams(dimension_semantics=("arbitrary",)),
+        cost_estimate=half_cost(rows, weights, width),
+        name="first_half",
+    )(*xs, *doubled)
+
+
+def hidden_units(xs, weights, start, block, ktile=256):
+    rows = sum(x.shape[0] for x in xs) // 2
+    width = 4 * weights[0].shape[1]
+    steps, specs, doubled = half_specs(xs, weights, 1, ktile)
     return pl.pallas_call(
         functools.partial(hidden_kernel, parts=len(xs)),
         grid=(steps,),
-        in_specs=[pl.BlockSpec((x.shape[0], ktile), lambda n: (0, n)) for x in xs] + specs,
-        out_specs=pl.BlockSpec((rows, 2 * width), lambda n: (0, 0)),
-        out_shape=jax.ShapeDtypeStruct((rows, 2 * width), BF16),
-        scratch_shapes=[pltpu.VMEM((rows, 4 * width), F32)],
+        in_specs=specs + [pl.BlockSpec((rows, width), lambda n: (block, 0))],
+        out_specs=pl.BlockSpec((rows, width // 2), lambda n: (0, 0)),
+        out_shape=jax.ShapeDtypeStruct((rows, width // 2), BF16),
+        scratch_shapes=[pltpu.VMEM((rows, width), F32)],
         compiler_params=pltpu.CompilerParams(dimension_semantics=("arbitrary",)),
-        cost_estimate=pl.CostEstimate(
-            flops=8 * rows * depth * width,
-            transcendentals=2 * rows * width,
-            bytes_accessed=8 * depth * width + 2 * rows * depth,
-        ),
+        cost_estimate=half_cost(rows, weights, width),
         name="hidden_units",
-    )(*xs, *doubled)
+    )(*xs, *doubled, start)
 
 
 def in_blocks(near, far, shift):
@@ -463,8 +513,10 @@
     swap = [(0, 1), (1, 0)]
 
     gate, up, down = gate_weight[0], up_weight[0], down_weight[0]
-    outgoing, slots = dispatch(index, routed_rows, pre_gain, expert_pick, part, experts)
-    arrived = exchange(outgoing.reshape(experts, 2 * CAP, width // 2))
+    out_a, out_b, slots = dispatch(index, routed_rows, pre_gain, expert_pick, part, experts)
+    rows_a = exchange(out_a.reshape(experts, 2 * CAP, width // 4)).reshape(out_a.shape)
+    rows_b = exchange(out_b.reshape(experts, 2 * CAP, width // 4)).reshape(out_b.shape)
+    right_a, left_a = from_right(rows_a), from_left(rows_a)
 
     weights = (gate, up, lax.ppermute(gate, "c", swap), lax.ppermute(up, "c", swap))
     cut = width // NY
@@ -476,25 +528,22 @@
         queries, key_vectors, value_vectors, decay_logit
     )
     mine, _ = lax.optimization_barrier((mine, local_state))
-    arrived, local_state = lax.optimization_barrier((arrived, local_state))
+    rows_b, local_state = lax.optimization_barrier((rows_b, local_state))
     downs = []
     for piece in mine:
         downs += [piece, lax.ppermute(piece, "c", swap)]
 
-    half = experts // 2
-    top = arrived[:half].reshape(-1, width // 2)
-    bottom = arrived[half:].reshape(-1, width // 2)
-    right_top, right_bottom = from_right(top), from_right(bottom)
-    left_top, left_bottom = from_left(top), from_left(bottom)
-    far_top, far_bottom = from_left(left_top), from_right(right_bottom)
+    far_a = from_left(left_a)
+    right_b, left_b = from_right(rows_b), from_left(rows_b)
+    far_b = from_right(right_b)
 
     chunk_states = exchange(local_state)
     before = prefix(chunk_states)
-    sides, before = lax.optimization_barrier(
-        ((right_top, right_bottom, left_top, left_bottom), before)
-    )
-    near = hidden_units([top, bottom, *sides], weights).reshape(3, -1, 2 * gate.shape[1])
-    far = hidden_units([far_top, far_bottom], weights)
+    right_b, left_b, before = lax.optimization_barrier((right_b, left_b, before))
+    summed = first_half([rows_a, right_a, left_a, far_a], weights)
+    near = hidden_units([rows_b, right_b, left_b], weights, summed, 0)
+    near = near.reshape(3, -1, 2 * gate.shape[1])
+    far = hidden_units([far_b], weights, summed, 3)
     near_left, near_right = from_left(near), from_right(near)
     far_left, far_right = from_left(far), from_right(far)
     far_far = lax.ppermute(far, "y", ring(NY, 2))

time: 204 us -> 203 us (level)
  waiting for transfers between devices: 99.4 us -> 85.5 us
  starting transfers between devices: 50.4 us -> 58.9 us
  Pallas kernels: 44.4 us -> 48.8 us
    ppermute x6, waiting for transfers between devices: 20.5 us -> 10.6 us  [from_right(): return lax.ppermute(x, 'y', ring(NY, -1))]
    pallas_call x0 -> x1, Pallas kernels: none -> 7.29 us  [first_half(): pl.pallas_call(functools.partial(first_half_kernel, parts=len(xs)), grid=...]
    ppermute x6, waiting for transfers between devices: 14.8 us -> 7.78 us  [from_left(): return lax.ppermute(x, 'y', ring(NY, 1))]
    ppermute x3, waiting for transfers between devices: 11.4 us -> 4.99 us  [on_device(): lax.ppermute(slices[-m % NY], 'y', ring(NY, -m))]
    all_to_all x3 -> x4, waiting for transfers between devices: 51 us -> 56.3 us  [exchange(): return lax.all_to_all(x, EP, split_axis=0, concat_axis=0, tiled=True)]
    all_to_all x3 -> x4, starting transfers between devices: 23.4 us -> 28.1 us  [exchange(): return lax.all_to_all(x, EP, split_axis=0, concat_axis=0, tiled=True)]
    ppermute x1, waiting for transfers between devices: 0.84 us -> 4.47 us  [on_device(): far_far = lax.ppermute(far, 'y', ring(NY, 2))]
    ppermute x6, starting transfers between devices: 12 us -> 14.8 us  [from_right(): return lax.ppermute(x, 'y', ring(NY, -1))]
  transfers between devices with their start and end apart: 28 -> 29, of which waited for: 13 -> 15; matrix products, arithmetic and copies ran while one was open for 2% -> 2% of each run, Pallas kernels for 15% -> 17%
where the time goes in v4:
time: 203 us; the launch traced here: 202 us
  waiting for transfers between devices  85.5 us (42%)
  starting transfers between devices  58.9 us (29%)
  Pallas kernels  48.8 us (24%)
  local copies, waits for them, and re-layouts  7.66 us (4%)
    all_to_all x4, waiting for transfers between devices, exchange(): return lax.all_to_all(x, EP, split_axis=0, concat_axis=0, tiled=True)  56.3 us
    all_to_all x4, starting transfers between devices, exchange(): return lax.all_to_all(x, EP, split_axis=0, concat_axis=0, tiled=True)  28.1 us
    ppermute x6, starting transfers between devices, from_right(): return lax.ppermute(x, 'y', ring(NY, -1))  14.8 us
    pallas_call x2, Pallas kernels, hidden_units(): pl.pallas_call(functools.partial(hidden_kernel, parts=len(xs)), grid=(ste...  12.4 us
    ppermute x6, waiting for transfers between devices, from_right(): return lax.ppermute(x, 'y', ring(NY, -1))  10.6 us
    pallas_call x1, Pallas kernels, attn_local(): pl.pallas_call(attn_local_kernel, grid=(rows // tile,), in_specs=[pl.Bloc...  9.49 us
    ppermute x6, waiting for transfers between devices, from_left(): return lax.ppermute(x, 'y', ring(NY, 1))  7.78 us
    pallas_call x1, Pallas kernels, first_half(): pl.pallas_call(functools.partial(first_half_kernel, parts=len(xs)), grid=...  7.29 us
  transfers between devices with their start and end apart: 29, of which 15 were waited for; matrix products, arithmetic and copies ran while one was open for 2% of the time, Pallas kernels for 17%

profile of v4, /device:TPU:2, one launch (start us, length us, event | category | flops | bytes accessed | tf_op | source)
XLA Modules:
  0.0 201.8 jit_solution(17594953872857500202)
XLA Ops:
  0.6 0.0 copy-start
  0.6 2.9 %dispatch.1 = (bf16[256,1024]{1,0:T(8,128)(2,1)}, bf16[256,1024]{1,0:T(8,128)(2,1)}, s32[2,256]{1,0:T(2,128)}) custom-call(s32[1]{0:T(128)} %bitcast.idx_ref, bf16[256,4096]{1,0:T(8,128)(2,1)} %rows_ref.1, f32[1,4096]{1,0:T(1,128)} %bitcast.49, s32[2,256]{1,0:T(2,128)} %bitcast.51), custom_call_target="tpu_custom_call" | custom-call | tf_op jit(solution)/shard_map/dispatch/pallas_call | solution.py:227
  3.6 11.6 %all-to-all-start.2 = ((bf16[32,8,1024]{2,1,0:T(8,128)(2,1)}), bf16[32,8,1024]{2,1,0:T(8,128)(2,1)S(1)}, u32[]{:S(2)}, u32[]{:S(2)}) async-start(bf16[32,8,1024]{2,1,0:T(8,128)(2,1)} %bitcast.47), calls=%async_computation.2 | async-start | bytes 1048576 | tf_op jit(solution)/shard_map/all_to_all | solution.py:163
  15.2 0.1 collective-permute-start.2
  15.3 0.5 collective-permute-start.3
  15.8 16.2 %all-to-all-done.2 = bf16[32,8,1024]{2,1,0:T(8,128)(2,1)S(1)} async-done(((bf16[32,8,1024]{2,1,0:T(8,128)(2,1)}), bf16[32,8,1024]{2,1,0:T(8,128)(2,1)S(1)}, u32[]{:S(2)}, u32[]{:S(2)}) %all-to-all-start.2) | async-done | bytes 524320 | tf_op jit(solution)/shard_map/all_to_all | solution.py:163
  32.0 5.6 %all-to-all-start = ((bf16[32,8,1024]{2,1,0:T(8,128)(2,1)}), bf16[32,8,1024]{2,1,0:T(8,128)(2,1)S(1)}, u32[]{:S(2)}, u32[]{:S(2)}) async-start(bf16[32,8,1024]{2,1,0:T(8,128)(2,1)} %bitcast.46), calls=%async_computation | async-start | bytes 1048576 | tf_op jit(solution)/shard_map/all_to_all | solution.py:163
  37.6 9.5 %attn_local.1 = (f32[1024,512]{1,0:T(8,128)}, bf16[1024,256]{1,0:T(8,128)(2,1)}, bf16[32,24,128]{2,1,0:T(8,128)(2,1)}) custom-call(bf16[1024,256]{1,0:T(8,128)(2,1)} %q_ref.1, bf16[1024,256]{1,0:T(8,128)(2,1)} %k_ref.1, bf16[1024,512]{1,0:T(8,128)(2,1)} %v_ref.1, f32[1024,256]{1,0:T(8,128)} %g_ref.1), custom_call_target="tpu_custom_call" | custom-call | flops 8000000000 | bytes 6000000 | tf_op jit(solution)/shard_map/attn_local/pallas_call | solution.py:91
  47.1 1.7 collective-permute-start.5
  48.8 4.8 %all-to-all-done = bf16[32,8,1024]{2,1,0:T(8,128)(2,1)S(1)} async-done(((bf16[32,8,1024]{2,1,0:T(8,128)(2,1)}), bf16[32,8,1024]{2,1,0:T(8,128)(2,1)S(1)}, u32[]{:S(2)}, u32[]{:S(2)}) %all-to-all-start) | async-done | bytes 524320 | tf_op jit(solution)/shard_map/all_to_all | solution.py:163
  53.6 3.0 %collective-permute-start = (bf16[256,1024]{1,0:T(8,128)(2,1)S(1)}, bf16[256,1024]{1,0:T(8,128)(2,1)S(1)}, u32[]{:S(2)}, u32[]{:S(2)}) collective-permute-start(bf16[256,1024]{1,0:T(8,128)(2,1)S(1)} %bitcast.43), channel_id=1, source_target_pairs={{0,6},{2,0},{4,2},{6,4},{1,7},{3,1},{5,3},{7,5},{8,14},{10,8},{12,... | collective-permute-start | bytes 1572872 | tf_op jit(solution)/shard_map/ppermute | solution.py:485
  56.6 6.7 %collective-permute-done.5.refs_2_ = bf16[256,1024]{1,0:T(8,128)(2,1)} collective-permute-done((bf16[256,1024]{1,0:T(8,128)(2,1)S(1)}, bf16[256,1024]{1,0:T(8,128)(2,1)}, u32[]{:S(2)}, u32[]{:S(2)}) %collective-permute-start.5) | collective-permute-done | bytes 524320 | tf_op jit(solution)/shard_map/ppermute | solution.py:489
  63.3 1.8 collective-permute-start.4
  65.1 3.8 %collective-permute-done.refs_1_ = bf16[256,1024]{1,0:T(8,128)(2,1)S(1)} collective-permute-done((bf16[256,1024]{1,0:T(8,128)(2,1)S(1)}, bf16[256,1024]{1,0:T(8,128)(2,1)S(1)}, u32[]{:S(2)}, u32[]{:S(2)}) %collective-permute-start) | collective-permute-done | bytes 524320 | tf_op jit(solution)/shard_map/ppermute | solution.py:485
  68.9 0.8 copy-done.13
  69.7 1.0 collective-permute-start.6
  70.8 5.1 %all-to-all-start.1 = ((bf16[32,24,128]{2,1,0:T(8,128)(2,1)}), bf16[32,24,128]{2,1,0:T(8,128)(2,1)S(1)}, u32[]{:S(2)}, u32[]{:S(2)}) async-start(bf16[32,24,128]{2,1,0:T(8,128)(2,1)} %get-tuple-element.29), calls=%async_computation.1 | async-start | bytes 393216 | tf_op jit(solution)/shard_map/all_to_all | solution.py:163
  75.9 2.9 %dynamic-slice_bitcast_fusion = (bf16[256,1024]{1,0:T(8,128)(2,1)}, bf16[256,1024]{1,0:T(8,128)(2,1)}, bf16[256,1024]{1,0:T(8,128)(2,1)}, bf16[256,1024]{1,0:T(8,128)(2,1)}) fusion(bf16[1,256,4096]{2,1,0:T(8,128)(2,1)} %param.24, s32[]{:T(128)S(6)} %select_n.15, s32[]{:T(128)S(6)} %select_n.13, s32[]{:T(128)S(6)} %select_n.12, s32[]{:T(128)S(6)} %select_n.14), kind=kLoop, calls=%fused_computation | loop fusion | bytes 4194320 | tf_op jit(solution)/shard_map/dynamic_slice | solution.py:524
  78.8 6.2 %all-to-all-done.1.in_ref = bf16[32,24,128]{2,1,0:T(8,128)(2,1)S(1)} async-done(((bf16[32,24,128]{2,1,0:T(8,128)(2,1)}), bf16[32,24,128]{2,1,0:T(8,128)(2,1)S(1)}, u32[]{:S(2)}, u32[]{:S(2)}) %all-to-all-start.1) | async-done | bytes 196640 | tf_op jit(solution)/shard_map/all_to_all | solution.py:163
  85.0 0.7 copy-done.2
  85.7 1.6 prefix.1
  87.4 0.0 collective-permute-done.1.refs_2_
  87.4 3.0 %collective-permute-start.15 = (bf16[256,1024]{1,0:T(8,128)(2,1)}, bf16[256,1024]{1,0:T(8,128)(2,1)S(1)}, u32[]{:S(2)}, u32[]{:S(2)}) collective-permute-start(bf16[256,1024]{1,0:T(8,128)(2,1)} %get-tuple-element.47), channel_id=1, source_target_pairs={{0,6},{2,0},{4,2},{6,4},{1,7},{3,1},{5,3},{7,5},{8,14},{10,8},{12,... | collective-permute-start | bytes 1572872 | tf_op jit(solution)/shard_map/ppermute | solution.py:526
  90.4 1.0 collective-permute-start.16
  91.4 1.3 collective-permute-start.17
  92.7 1.9 collective-permute-start.9
  94.6 7.3 %first_half.1.refs_11_.refs_9_ = f32[512,1024]{1,0:T(8,128)} custom-call(bf16[256,1024]{1,0:T(8,128)(2,1)} %bitcast.42, bf16[256,1024]{1,0:T(8,128)(2,1)} %collective-permute-done.4.refs_1_, bf16[256,1024]{1,0:T(8,128)(2,1)} %collective-permute-done.5.refs_2_, bf16[256,1024]{1,0:T(8,128)(2,1)} %collective-permute-done.6.refs_3_, bf16[4096,256]{1,0:T(8,128)(2,1)} %bitcast.23, ...), custom_call_target="tpu_custom_call" | custom-call | flops 8589934592 | bytes 7340032 | tf_op jit(solution)/shard_map/first_half/pallas_call | solution.py:332
  102.0 7.1 %hidden_units.2 = bf16[384,512]{1,0:T(8,128)(2,1)} custom-call(bf16[256,1024]{1,0:T(8,128)(2,1)} %bitcast.45, bf16[256,1024]{1,0:T(8,128)(2,1)} %copy-done.13, bf16[256,1024]{1,0:T(8,128)(2,1)} %collective-permute-done.1.refs_2_, bf16[4096,256]{1,0:T(8,128)(2,1)} %bitcast.25, bf16[4096,256]{1,0:T(8,128)(2,1)} %bitcast.26, bf16[4096,256]{1,0:T(8,128)(2,1)} %bitcast.33, ...), custom_call_target="tpu_custom_call" | custom-call | flops 6442450944 | bytes 6553600 | tf_op jit(solution)/shard_map/hidden_units/pallas_call | solution.py:348
  109.1 0.1 collective-permute-start.7
  109.2 4.3 %collective-permute-done.15.rest_2_ = bf16[256,1024]{1,0:T(8,128)(2,1)S(1)} collective-permute-done((bf16[256,1024]{1,0:T(8,128)(2,1)}, bf16[256,1024]{1,0:T(8,128)(2,1)S(1)}, u32[]{:S(2)}, u32[]{:S(2)}) %collective-permute-start.15) | collective-permute-done | bytes 524320 | tf_op jit(solution)/shard_map/ppermute | solution.py:526
  113.5 0.6 collective-permute-done.17.rest_6_
  114.2 0.5 collective-permute-start.19
  114.7 0.0 collective-permute-start.20
  114.7 6.1 %collective-permute-done.9.refs_0_ = bf16[256,1024]{1,0:T(8,128)(2,1)S(1)} collective-permute-done((bf16[256,1024]{1,0:T(8,128)(2,1)}, bf16[256,1024]{1,0:T(8,128)(2,1)S(1)}, u32[]{:S(2)}, u32[]{:S(2)}) %collective-permute-start.9) | collective-permute-done | bytes 524320 | tf_op jit(solution)/shard_map/ppermute | solution.py:485
  120.8 3.6 %collective-permute-start.8 = (bf16[3,128,512]{2,1,0:T(8,128)(2,1)}, bf16[3,128,512]{2,1,0:T(8,128)(2,1)S(1)}, u32[]{:S(2)}, u32[]{:S(2)}) collective-permute-start(bf16[3,128,512]{2,1,0:T(8,128)(2,1)} %bitcast.53), channel_id=1, source_target_pairs={{0,6},{2,0},{4,2},{6,4},{1,7},{3,1},{5,3},{7,5},{8,14},{10,8},{12,... | collective-permute-start | bytes 1179656 | tf_op jit(solution)/shard_map/ppermute | solution.py:485
  124.4 5.3 %hidden_units.3.f0 = bf16[128,512]{1,0:T(8,128)(2,1)} custom-call(bf16[256,1024]{1,0:T(8,128)(2,1)} %copy-done.3, bf16[4096,256]{1,0:T(8,128)(2,1)} %bitcast.27, bf16[4096,256]{1,0:T(8,128)(2,1)} %bitcast.28, bf16[4096,256]{1,0:T(8,128)(2,1)} %bitcast.35, bf16[4096,256]{1,0:T(8,128)(2,1)} %bitcast.36, ...), custom_call_target="tpu_custom_call" | custom-call | flops 2147483648 | bytes 4980736 | tf_op jit(solution)/shard_map/hidden_units/pallas_call | solution.py:348
  129.7 0.3 collective-permute-done.8.n1
  130.0 1.8 collective-permute-start.11
  131.9 1.9 collective-permute-start.10
  133.8 2.2 %collective-permute-start.13 = (bf16[128,512]{1,0:T(8,128)(2,1)}, bf16[128,512]{1,0:T(8,128)(2,1)S(1)}, u32[]{:S(2)}, u32[]{:S(2)}) collective-permute-start(bf16[128,512]{1,0:T(8,128)(2,1)} %hidden_units.3.f0), channel_id=1, source_target_pairs={{0,4},{2,6},{4,0},{6,2},{1,5},{3,7},{5,1},{7,3},{8,12},{10,14},{12... | collective-permute-start | bytes 393224 | tf_op jit(solution)/shard_map/ppermute | solution.py:549
  136.0 0.6 collective-permute-start.14
  136.7 2.6 %collective-permute-start.12 = (bf16[1,128,512]{2,1,0:T(8,128)(2,1)S(1)}, bf16[1,128,512]{2,1,0:T(8,128)(2,1)S(1)}, u32[]{:S(2)}, u32[]{:S(2)}) collective-permute-start(bf16[1,128,512]{2,1,0:T(8,128)(2,1)S(1)} %slice.7), channel_id=1, source_target_pairs={{0,6},{2,0},{4,2},{6,4},{1,7},{3,1},{5,3},{7,5},{8,14},{10,8},{12,... | collective-permute-start | bytes 393224 | tf_op jit(solution)/shard_map/ppermute | solution.py:485
  139.3 0.4 collective-permute-done.10.f1
  139.7 4.5 %collective-permute-done.13.f2 = bf16[128,512]{1,0:T(8,128)(2,1)S(1)} collective-permute-done((bf16[128,512]{1,0:T(8,128)(2,1)}, bf16[128,512]{1,0:T(8,128)(2,1)S(1)}, u32[]{:S(2)}, u32[]{:S(2)}) %collective-permute-start.13) | collective-permute-done | bytes 131104 | tf_op jit(solution)/shard_map/ppermute | solution.py:549
  144.1 1.1 collective-permute-done.14.f3
  145.2 0.0 copy-start.16
  145.3 0.6 copy-done.19
  145.9 0.0 copy-done.20
  145.9 0.1 copy-done.16
  146.0 6.4 %expert_down.1 = bf16[512,1152]{1,0:T(8,128)(2,1)} custom-call(bf16[3,128,512]{2,1,0:T(8,128)(2,1)} %bitcast.54, bf16[128,512]{1,0:T(8,128)(2,1)} %hidden_units.3.f0, bf16[3,128,512]{2,1,0:T(8,128)(2,1)} %copy-done.11, bf16[128,512]{1,0:T(8,128)(2,1)} %copy-done.17, bf16[2,128,512]{2,1,0:T(8,128)(2,1)} %copy-done.16, bf16[1,128,512]{2,1,0:T(8,128)(2,1)} %copy-done.20, ...), custom_call_target="tpu_custom_call" | custom-call | flops 2415919104 | bytes 8000000 | tf_op jit(solution)/shard_map/expert_down/pallas_call | solution.py:398
  152.5 0.0 copy-start.12
  152.5 5.8 %all-to-all-start.3 = ((bf16[32,16,1152]{2,1,0:T(8,128)(2,1)}), bf16[32,16,1152]{2,1,0:T(8,128)(2,1)S(1)}, u32[]{:S(2)}, u32[]{:S(2)}) async-start(bf16[32,16,1152]{2,1,0:T(8,128)(2,1)} %bitcast.39), calls=%async_computation.3 | async-start | bytes 2359296 | tf_op jit(solution)/shard_map/all_to_all | solution.py:163
  158.3 0.8 copy.15.weight_ref
  159.1 29.1 %all-to-all-done.3 = bf16[32,16,1152]{2,1,0:T(8,128)(2,1)S(1)} async-done(((bf16[32,16,1152]{2,1,0:T(8,128)(2,1)}), bf16[32,16,1152]{2,1,0:T(8,128)(2,1)S(1)}, u32[]{:S(2)}, u32[]{:S(2)}) %all-to-all-start.3) | async-done | bytes 1179680 | tf_op jit(solution)/shard_map/all_to_all | solution.py:163
  188.2 1.0 copy-done.1
  189.2 2.5 %combine.1 = (bf16[32,1024]{1,0:T(8,128)(2,1)}, bf16[32,1024]{1,0:T(8,128)(2,1)}, bf16[32,1024]{1,0:T(8,128)(2,1)}, bf16[32,1024]{1,0:T(8,128)(2,1)}) custom-call(s32[1]{0:T(128)} %bitcast.idx_ref, bf16[512,1152]{1,0:T(8,128)(2,1)} %bitcast.37, s32[2,256]{1,0:T(2,128)} %get-tuple-element.41.slot_ref, f32[256,2]{1,0:T(8,128)} %copy.15.weight_ref), custom_call_target="tpu_custom_call" | custom-call | tf_op jit(solution)/shard_map/combine/pallas_call | solution.py:439
  191.7 0.9 collective-permute-start.22
  192.7 0.2 collective-permute-start.23
  192.8 0.9 collective-permute-start.24
  193.8 4.3 %attn_out.1 = bf16[1024,512]{1,0:T(8,128)(2,1)} custom-call(f32[1024,512]{1,0:T(8,128)} %get-tuple-element.24.o_ref, bf16[1024,256]{1,0:T(8,128)(2,1)} %get-tuple-element.25.qc_ref, bf16[512,1152]{1,0:T(8,128)(2,1)} %bitcast.38, f32[1,256]{1,0:T(1,128)} %bitcast.55), custom_call_target="tpu_custom_call" | custom-call | flops 3000000000 | bytes 4000000 | tf_op jit(solution)/shard_map/attn_out/pallas_call | solution.py:135
  198.0 0.6 collective-permute-done.23.p2
  198.7 0.7 collective-permute-done.24.p3
  199.3 0.6 copy-done.10
  200.0 1.8 finish.1
  (50 shorter events, 0.1 us)
Async XLA Ops:
  0.6 14.6 %copy-start = (bf16[1,4096,256]{2,1,0:T(8,128)(2,1)S(1)}, bf16[1,4096,256]{2,1,0:T(8,128)(2,1)}, u32[]{:S(2)}) copy-start(bf16[1,4096,256]{2,1,0:T(8,128)(2,1)} %param.22) | copy-start | bytes 6291460
  3.6 28.5 %all-to-all-start.2 = ((bf16[32,8,1024]{2,1,0:T(8,128)(2,1)}), bf16[32,8,1024]{2,1,0:T(8,128)(2,1)S(1)}, u32[]{:S(2)}, u32[]{:S(2)}) async-start(bf16[32,8,1024]{2,1,0:T(8,128)(2,1)} %bitcast.47), calls=%async_computation.2 | async-start | bytes 1048576 | tf_op jit(solution)/shard_map/all_to_all | solution.py:163
  15.2 77.5 %collective-permute-start.2 = (bf16[4096,256]{1,0:T(8,128)(2,1)S(1)}, bf16[4096,256]{1,0:T(8,128)(2,1)}, u32[]{:S(2)}, u32[]{:S(2)}) collective-permute-start(bf16[4096,256]{1,0:T(8,128)(2,1)S(1)} %bitcast.29), channel_id=1, source_target_pairs={{0,1},{1,0},{2,3},{3,2},{4,5},{5,4},{6,7},{7,6},{8,9},{9,8},{10,11... | collective-permute-start | bytes 6291464 | tf_op jit(solution)/shard_map/ppermute | solution.py:521
  15.3 79.3 %collective-permute-start.3 = (bf16[4096,256]{1,0:T(8,128)(2,1)}, bf16[4096,256]{1,0:T(8,128)(2,1)}, u32[]{:S(2)}, u32[]{:S(2)}) collective-permute-start(bf16[4096,256]{1,0:T(8,128)(2,1)} %bitcast.30), channel_id=1, source_target_pairs={{0,1},{1,0},{2,3},{3,2},{4,5},{5,4},{6,7},{7,6},{8,9},{9,8},{10,11... | collective-permute-start | bytes 6291464 | tf_op jit(solution)/shard_map/ppermute | solution.py:521
  32.0 31.3 %copy-start.4 = (bf16[32,8,1024]{2,1,0:T(8,128)(2,1)}, bf16[32,8,1024]{2,1,0:T(8,128)(2,1)S(1)}, u32[]{:S(2)}) copy-start(bf16[32,8,1024]{2,1,0:T(8,128)(2,1)S(1)} %all-to-all-done.2) | copy-start | bytes 1572868
  32.0 21.5 %all-to-all-start = ((bf16[32,8,1024]{2,1,0:T(8,128)(2,1)}), bf16[32,8,1024]{2,1,0:T(8,128)(2,1)S(1)}, u32[]{:S(2)}, u32[]{:S(2)}) async-start(bf16[32,8,1024]{2,1,0:T(8,128)(2,1)} %bitcast.46), calls=%async_computation | async-start | bytes 1048576 | tf_op jit(solution)/shard_map/all_to_all | solution.py:163
  47.1 16.2 %collective-permute-start.5 = (bf16[256,1024]{1,0:T(8,128)(2,1)S(1)}, bf16[256,1024]{1,0:T(8,128)(2,1)}, u32[]{:S(2)}, u32[]{:S(2)}) collective-permute-start(bf16[256,1024]{1,0:T(8,128)(2,1)S(1)} %bitcast.40), channel_id=1, source_target_pairs={{0,2},{2,4},{4,6},{6,0},{1,3},{3,5},{5,7},{7,1},{8,10},{10,12},{12... | collective-permute-start | bytes 1572872 | tf_op jit(solution)/shard_map/ppermute | solution.py:489
  53.6 25.3 %copy-start.5 = (bf16[32,8,1024]{2,1,0:T(8,128)(2,1)}, bf16[32,8,1024]{2,1,0:T(8,128)(2,1)S(1)}, u32[]{:S(2)}) copy-start(bf16[32,8,1024]{2,1,0:T(8,128)(2,1)S(1)} %all-to-all-done) | copy-start | bytes 1572868
  53.6 15.3 %collective-permute-start = (bf16[256,1024]{1,0:T(8,128)(2,1)S(1)}, bf16[256,1024]{1,0:T(8,128)(2,1)S(1)}, u32[]{:S(2)}, u32[]{:S(2)}) collective-permute-start(bf16[256,1024]{1,0:T(8,128)(2,1)S(1)} %bitcast.43), channel_id=1, source_target_pairs={{0,6},{2,0},{4,2},{6,4},{1,7},{3,1},{5,3},{7,5},{8,14},{10,8},{12,... | collective-permute-start | bytes 1572872 | tf_op jit(solution)/shard_map/ppermute | solution.py:485
  56.6 30.8 %collective-permute-start.1 = (bf16[256,1024]{1,0:T(8,128)(2,1)S(1)}, bf16[256,1024]{1,0:T(8,128)(2,1)}, u32[]{:S(2)}, u32[]{:S(2)}) collective-permute-start(bf16[256,1024]{1,0:T(8,128)(2,1)S(1)} %bitcast.44), channel_id=1, source_target_pairs={{0,2},{2,4},{4,6},{6,0},{1,3},{3,5},{5,7},{7,1},{8,10},{10,12},{12... | collective-permute-start | bytes 1572872 | tf_op jit(solution)/shard_map/ppermute | solution.py:489
  63.3 27.1 %collective-permute-start.4 = (bf16[256,1024]{1,0:T(8,128)(2,1)S(1)}, bf16[256,1024]{1,0:T(8,128)(2,1)}, u32[]{:S(2)}, u32[]{:S(2)}) collective-permute-start(bf16[256,1024]{1,0:T(8,128)(2,1)S(1)} %bitcast.41), channel_id=1, source_target_pairs={{0,6},{2,0},{4,2},{6,4},{1,7},{3,1},{5,3},{7,5},{8,14},{10,8},{12,... | collective-permute-start | bytes 1572872 | tf_op jit(solution)/shard_map/ppermute | solution.py:485
  68.9 0.8 copy-start.13
  69.7 21.7 %collective-permute-start.6 = (bf16[256,1024]{1,0:T(8,128)(2,1)}, bf16[256,1024]{1,0:T(8,128)(2,1)}, u32[]{:S(2)}, u32[]{:S(2)}) collective-permute-start(bf16[256,1024]{1,0:T(8,128)(2,1)} %collective-permute-done.5.refs_2_), channel_id=1, source_target_pairs={{0,2},{2,4},{4,6},{6,0},{1,3},{3,5},{5,7},{7,1},{8,10},{10,12},{12... | collective-permute-start | bytes 1572872 | tf_op jit(solution)/shard_map/ppermute | solution.py:489
  70.8 14.3 %all-to-all-start.1 = ((bf16[32,24,128]{2,1,0:T(8,128)(2,1)}), bf16[32,24,128]{2,1,0:T(8,128)(2,1)S(1)}, u32[]{:S(2)}, u32[]{:S(2)}) async-start(bf16[32,24,128]{2,1,0:T(8,128)(2,1)} %get-tuple-element.29), calls=%async_computation.1 | async-start | bytes 393216 | tf_op jit(solution)/shard_map/all_to_all | solution.py:163
  85.0 0.7 copy-start.2
  87.4 26.2 %collective-permute-start.15 = (bf16[256,1024]{1,0:T(8,128)(2,1)}, bf16[256,1024]{1,0:T(8,128)(2,1)S(1)}, u32[]{:S(2)}, u32[]{:S(2)}) collective-permute-start(bf16[256,1024]{1,0:T(8,128)(2,1)} %get-tuple-element.47), channel_id=1, source_target_pairs={{0,6},{2,0},{4,2},{6,4},{1,7},{3,1},{5,3},{7,5},{8,14},{10,8},{12,... | collective-permute-start | bytes 1572872 | tf_op jit(solution)/shard_map/ppermute | solution.py:526
  90.4 23.2 %collective-permute-start.16 = (bf16[256,1024]{1,0:T(8,128)(2,1)}, bf16[256,1024]{1,0:T(8,128)(2,1)S(1)}, u32[]{:S(2)}, u32[]{:S(2)}) collective-permute-start(bf16[256,1024]{1,0:T(8,128)(2,1)} %get-tuple-element.49), channel_id=1, source_target_pairs={{0,4},{2,6},{4,0},{6,2},{1,5},{3,7},{5,1},{7,3},{8,12},{10,14},{12... | collective-permute-start | bytes 1572872 | tf_op jit(solution)/shard_map/ppermute | solution.py:526
  91.4 22.8 %collective-permute-start.17 = (bf16[256,1024]{1,0:T(8,128)(2,1)}, bf16[256,1024]{1,0:T(8,128)(2,1)}, u32[]{:S(2)}, u32[]{:S(2)}) collective-permute-start(bf16[256,1024]{1,0:T(8,128)(2,1)} %get-tuple-element.46), channel_id=1, source_target_pairs={{0,2},{2,4},{4,6},{6,0},{1,3},{3,5},{5,7},{7,1},{8,10},{10,12},{12... | collective-permute-start | bytes 1572872 | tf_op jit(solution)/shard_map/ppermute | solution.py:526
  92.7 28.0 %collective-permute-start.9 = (bf16[256,1024]{1,0:T(8,128)(2,1)}, bf16[256,1024]{1,0:T(8,128)(2,1)S(1)}, u32[]{:S(2)}, u32[]{:S(2)}) collective-permute-start(bf16[256,1024]{1,0:T(8,128)(2,1)} %copy-done.13), channel_id=1, source_target_pairs={{0,6},{2,0},{4,2},{6,4},{1,7},{3,1},{5,3},{7,5},{8,14},{10,8},{12,... | collective-permute-start | bytes 1572872 | tf_op jit(solution)/shard_map/ppermute | solution.py:485
  101.9 12.2 %copy-start.6 = (bf16[256,1024]{1,0:T(8,128)(2,1)S(1)}, bf16[256,1024]{1,0:T(8,128)(2,1)}, u32[]{:S(2)}) copy-start(bf16[256,1024]{1,0:T(8,128)(2,1)} %get-tuple-element.36.rest_0_) | copy-start | bytes 1572868
  109.1 15.3 %collective-permute-start.7 = (bf16[3,128,512]{2,1,0:T(8,128)(2,1)}, bf16[3,128,512]{2,1,0:T(8,128)(2,1)S(1)}, u32[]{:S(2)}, u32[]{:S(2)}) collective-permute-start(bf16[3,128,512]{2,1,0:T(8,128)(2,1)} %bitcast.52), channel_id=1, source_target_pairs={{0,2},{2,4},{4,6},{6,0},{1,3},{3,5},{5,7},{7,1},{8,10},{10,12},{12... | collective-permute-start | bytes 1179656 | tf_op jit(solution)/shard_map/ppermute | solution.py:489
  113.5 16.1 %copy-start.14 = (bf16[256,1024]{1,0:T(8,128)(2,1)}, bf16[256,1024]{1,0:T(8,128)(2,1)S(1)}, u32[]{:S(2)}) copy-start(bf16[256,1024]{1,0:T(8,128)(2,1)S(1)} %collective-permute-done.15.rest_2_) | copy-start | bytes 1572868
  113.5 16.1 %copy-start.15 = (bf16[256,1024]{1,0:T(8,128)(2,1)}, bf16[256,1024]{1,0:T(8,128)(2,1)S(1)}, u32[]{:S(2)}) copy-start(bf16[256,1024]{1,0:T(8,128)(2,1)S(1)} %collective-permute-done.16.rest_4_) | copy-start | bytes 1572868
  114.2 17.7 %collective-permute-start.18 = (bf16[256,1024]{1,0:T(8,128)(2,1)S(1)}, bf16[256,1024]{1,0:T(8,128)(2,1)}, u32[]{:S(2)}, u32[]{:S(2)}) collective-permute-start(bf16[256,1024]{1,0:T(8,128)(2,1)S(1)} %copy-done.6), channel_id=1, source_target_pairs={{0,1},{1,0},{2,3},{3,2},{4,5},{5,4},{6,7},{7,6},{8,9},{9,8},{10,11... | collective-permute-start | bytes 1572872 | tf_op jit(solution)/shard_map/ppermute | solution.py:534
  114.2 19.6 %collective-permute-start.19 = (bf16[256,1024]{1,0:T(8,128)(2,1)S(1)}, bf16[256,1024]{1,0:T(8,128)(2,1)}, u32[]{:S(2)}, u32[]{:S(2)}) collective-permute-start(bf16[256,1024]{1,0:T(8,128)(2,1)S(1)} %collective-permute-done.15.rest_2_), channel_id=1, source_target_pairs={{0,1},{1,0},{2,3},{3,2},{4,5},{5,4},{6,7},{7,6},{8,9},{9,8},{10,11... | collective-permute-start | bytes 1572872 | tf_op jit(solution)/shard_map/ppermute | solution.py:534
  114.7 21.3 %collective-permute-start.20 = (bf16[256,1024]{1,0:T(8,128)(2,1)S(1)}, bf16[256,1024]{1,0:T(8,128)(2,1)}, u32[]{:S(2)}, u32[]{:S(2)}) collective-permute-start(bf16[256,1024]{1,0:T(8,128)(2,1)S(1)} %collective-permute-done.16.rest_4_), channel_id=1, source_target_pairs={{0,1},{1,0},{2,3},{3,2},{4,5},{5,4},{6,7},{7,6},{8,9},{9,8},{10,11... | collective-permute-start | bytes 1572872 | tf_op jit(solution)/shard_map/ppermute | solution.py:534
  120.8 3.6 %copy-start.3 = (bf16[256,1024]{1,0:T(8,128)(2,1)}, bf16[256,1024]{1,0:T(8,128)(2,1)S(1)}, u32[]{:S(2)}) copy-start(bf16[256,1024]{1,0:T(8,128)(2,1)S(1)} %collective-permute-done.9.refs_0_) | copy-start | bytes 1572868
  120.8 9.2 %collective-permute-start.8 = (bf16[3,128,512]{2,1,0:T(8,128)(2,1)}, bf16[3,128,512]{2,1,0:T(8,128)(2,1)S(1)}, u32[]{:S(2)}, u32[]{:S(2)}) collective-permute-start(bf16[3,128,512]{2,1,0:T(8,128)(2,1)} %bitcast.53), channel_id=1, source_target_pairs={{0,6},{2,0},{4,2},{6,4},{1,7},{3,1},{5,3},{7,5},{8,14},{10,8},{12,... | collective-permute-start | bytes 1179656 | tf_op jit(solution)/shard_map/ppermute | solution.py:485
  124.4 5.6 %copy-start.7 = (bf16[3,128,512]{2,1,0:T(8,128)(2,1)}, bf16[3,128,512]{2,1,0:T(8,128)(2,1)S(1)}, u32[]{:S(2)}) copy-start(bf16[3,128,512]{2,1,0:T(8,128)(2,1)S(1)} %collective-permute-done.7.n3) | copy-start | bytes 1179652
  124.4 12.3 %collective-permute-start.21 = (bf16[256,1024]{1,0:T(8,128)(2,1)}, bf16[256,1024]{1,0:T(8,128)(2,1)}, u32[]{:S(2)}, u32[]{:S(2)}) collective-permute-start(bf16[256,1024]{1,0:T(8,128)(2,1)} %collective-permute-done.17.rest_6_), channel_id=1, source_target_pairs={{0,1},{1,0},{2,3},{3,2},{4,5},{5,4},{6,7},{7,6},{8,9},{9,8},{10,11... | collective-permute-start | bytes 1572872 | tf_op jit(solution)/shard_map/ppermute | solution.py:534
  130.0 15.3 %copy-start.11 = (bf16[3,128,512]{2,1,0:T(8,128)(2,1)}, bf16[3,128,512]{2,1,0:T(8,128)(2,1)S(1)}, u32[]{:S(2)}) copy-start(bf16[3,128,512]{2,1,0:T(8,128)(2,1)S(1)} %collective-permute-done.8.n1) | copy-start | bytes 1179652
  130.0 15.2 %collective-permute-start.11 = (bf16[2,128,512]{2,1,0:T(8,128)(2,1)S(1)}, bf16[2,128,512]{2,1,0:T(8,128)(2,1)S(1)}, u32[]{:S(2)}, u32[]{:S(2)}) collective-permute-start(bf16[2,128,512]{2,1,0:T(8,128)(2,1)S(1)} %slice.6), channel_id=1, source_target_pairs={{0,2},{2,4},{4,6},{6,0},{1,3},{3,5},{5,7},{7,1},{8,10},{10,12},{12... | collective-permute-start | bytes 786440 | tf_op jit(solution)/shard_map/ppermute | solution.py:489
  131.9 7.8 %collective-permute-start.10 = (bf16[128,512]{1,0:T(8,128)(2,1)}, bf16[128,512]{1,0:T(8,128)(2,1)S(1)}, u32[]{:S(2)}, u32[]{:S(2)}) collective-permute-start(bf16[128,512]{1,0:T(8,128)(2,1)} %hidden_units.3.f0), channel_id=1, source_target_pairs={{0,6},{2,0},{4,2},{6,4},{1,7},{3,1},{5,3},{7,5},{8,14},{10,8},{12,... | collective-permute-start | bytes 393224 | tf_op jit(solution)/shard_map/ppermute | solution.py:485
  133.8 10.4 %collective-permute-start.13 = (bf16[128,512]{1,0:T(8,128)(2,1)}, bf16[128,512]{1,0:T(8,128)(2,1)S(1)}, u32[]{:S(2)}, u32[]{:S(2)}) collective-permute-start(bf16[128,512]{1,0:T(8,128)(2,1)} %hidden_units.3.f0), channel_id=1, source_target_pairs={{0,4},{2,6},{4,0},{6,2},{1,5},{3,7},{5,1},{7,3},{8,12},{10,14},{12... | collective-permute-start | bytes 393224 | tf_op jit(solution)/shard_map/ppermute | solution.py:549
  136.0 9.2 %collective-permute-start.14 = (bf16[128,512]{1,0:T(8,128)(2,1)}, bf16[128,512]{1,0:T(8,128)(2,1)S(1)}, u32[]{:S(2)}, u32[]{:S(2)}) collective-permute-start(bf16[128,512]{1,0:T(8,128)(2,1)} %hidden_units.3.f0), channel_id=1, source_target_pairs={{0,2},{2,4},{4,6},{6,0},{1,3},{3,5},{5,7},{7,1},{8,10},{10,12},{12... | collective-permute-start | bytes 393224 | tf_op jit(solution)/shard_map/ppermute | solution.py:489
  136.7 8.6 %collective-permute-start.12 = (bf16[1,128,512]{2,1,0:T(8,128)(2,1)S(1)}, bf16[1,128,512]{2,1,0:T(8,128)(2,1)S(1)}, u32[]{:S(2)}, u32[]{:S(2)}) collective-permute-start(bf16[1,128,512]{2,1,0:T(8,128)(2,1)S(1)} %slice.7), channel_id=1, source_target_pairs={{0,6},{2,0},{4,2},{6,4},{1,7},{3,1},{5,3},{7,5},{8,14},{10,8},{12,... | collective-permute-start | bytes 393224 | tf_op jit(solution)/shard_map/ppermute | solution.py:485
  139.7 5.6 %copy-start.17 = (bf16[128,512]{1,0:T(8,128)(2,1)}, bf16[128,512]{1,0:T(8,128)(2,1)S(1)}, u32[]{:S(2)}) copy-start(bf16[128,512]{1,0:T(8,128)(2,1)S(1)} %collective-permute-done.10.f1) | copy-start | bytes 393220
  144.1 1.1 copy-start.18
  145.2 0.6 copy-start.19
  145.2 0.7 copy-start.20
  145.2 0.8 copy-start.16
  152.5 5.8 %copy-start.12 = (f32[256,2]{0,1:T(2,128)S(1)}, f32[256,2]{0,1:T(2,128)}, u32[]{:S(2)}) copy-start(f32[256,2]{0,1:T(2,128)} %param.21) | copy-start | bytes 6148
  152.5 35.7 %all-to-all-start.3 = ((bf16[32,16,1152]{2,1,0:T(8,128)(2,1)}), bf16[32,16,1152]{2,1,0:T(8,128)(2,1)S(1)}, u32[]{:S(2)}, u32[]{:S(2)}) async-start(bf16[32,16,1152]{2,1,0:T(8,128)(2,1)} %bitcast.39), calls=%async_computation.3 | async-start | bytes 2359296 | tf_op jit(solution)/shard_map/all_to_all | solution.py:163
  188.2 1.0 copy-start.1
  191.7 6.3 %collective-permute-start.22 = (bf16[32,1024]{1,0:T(8,128)(2,1)}, bf16[32,1024]{1,0:T(8,128)(2,1)S(1)}, u32[]{:S(2)}, u32[]{:S(2)}) collective-permute-start(bf16[32,1024]{1,0:T(8,128)(2,1)} %get-tuple-element.43), channel_id=1, source_target_pairs={{0,6},{2,0},{4,2},{6,4},{1,7},{3,1},{5,3},{7,5},{8,14},{10,8},{12,... | collective-permute-start | bytes 196616 | tf_op jit(solution)/shard_map/ppermute | solution.py:561
  192.7 6.0 %collective-permute-start.23 = (bf16[32,1024]{1,0:T(8,128)(2,1)}, bf16[32,1024]{1,0:T(8,128)(2,1)S(1)}, u32[]{:S(2)}, u32[]{:S(2)}) collective-permute-start(bf16[32,1024]{1,0:T(8,128)(2,1)} %get-tuple-element.44), channel_id=1, source_target_pairs={{0,4},{2,6},{4,0},{6,2},{1,5},{3,7},{5,1},{7,3},{8,12},{10,14},{12... | collective-permute-start | bytes 196616 | tf_op jit(solution)/shard_map/ppermute | solution.py:561
  192.8 6.5 %collective-permute-start.24 = (bf16[32,1024]{1,0:T(8,128)(2,1)}, bf16[32,1024]{1,0:T(8,128)(2,1)S(1)}, u32[]{:S(2)}, u32[]{:S(2)}) collective-permute-start(bf16[32,1024]{1,0:T(8,128)(2,1)} %get-tuple-element.45), channel_id=1, source_target_pairs={{0,2},{2,4},{4,6},{6,0},{1,3},{3,5},{5,7},{7,1},{8,10},{10,12},{12... | collective-permute-start | bytes 196616 | tf_op jit(solution)/shard_map/ppermute | solution.py:561
  198.0 1.3 copy-start.8
  198.7 0.7 copy-start.9
  199.3 0.6 copy-start.10
